TPU v7x, 512 devices: a whole 4x4x16 slice. The times are simulated.
512 devices in a mesh: sp: 64 (over z, y), tp: 8 (over x, core).
Axes of the slice: x: 4, y: 4, z: 16, core: 2. Of those that a mesh axis runs over, the one named last changes fastest.
Arguments:
- tokens: bfloat16 [8192, 1024], P('sp', 'tp'), may hold values from -6 to 6
- norm_gain: float32 [1024], P('tp'), may hold values from 0.1 to 1.9
- query_weight: bfloat16 [1024, 1024], P('sp', 'tp'), may hold values from -0.1875 to 0.1875
- key_weight: bfloat16 [1024, 512], P('sp', 'tp'), may hold values from -0.1875 to 0.1875
- value_weight: bfloat16 [1024, 512], P('sp', 'tp'), may hold values from -0.1875 to 0.1875
- conv_in_weight: bfloat16 [1024, 1024], P('sp', 'tp'), may hold values from -0.1875 to 0.1875
- pre_weight: bfloat16 [1024, 1024], P('sp', 'tp'), may hold values from -0.1875 to 0.1875
- post_weight: bfloat16 [1024, 1024], P('sp', 'tp'), may hold values from -0.1875 to 0.1875
- attn_gate_weight: bfloat16 [1024, 1024], P('sp', 'tp'), may hold values from -0.1875 to 0.1875
- conv_gate_weight: bfloat16 [1024, 1024], P('sp', 'tp'), may hold values from -0.1875 to 0.1875
- sink_logit: float32 [16], P('tp'), may hold values from 1 to 5
- conv_taps: float32 [3, 1024], P(None, 'tp'), may hold values from -3 to 3
- attn_out_weight: bfloat16 [1024, 1024], P('tp', 'sp'), may hold values from -1 to 1
- conv_out_weight: bfloat16 [1024, 1024], P('tp', 'sp'), may hold values from -0.1875 to 0.1875
Outputs:
- merged: bfloat16 [8192, 1024], P('sp', 'tp')
All inputs are finite; a program needn't handle non-finite values.
Results may differ from a plain program's by a relative error of at most 0.003.
Values may be sent and summed in bfloat16 or wider, within the bound.
No kernel may reach another device: no remote copies, remote signals or barrier semaphores. Data moves between devices by JAX's collectives and lax.ppermute only.
A program may use at most 64 MiB of HBM per device.

v0:
```python
import jax
import jax.numpy as jnp
from jax import lax
from jax.sharding import Mesh
from jax.sharding import PartitionSpec as P

HEAD_DIM = 64
WINDOW = 64
TP = ("tp_0", "tp_1")


epsilon = 1e-06
negative = -1e30


def gathered_total(shard, axis):
    blocks = lax.all_gather(shard, axis)
    return blocks.sum(axis=0)


def joined_along(blocks, dim):
    blocks = jnp.moveaxis(blocks, 0, dim)
    lengths = blocks.shape
    return blocks.reshape(*lengths[:dim], lengths[dim] * lengths[dim + 1], *lengths[dim + 2 :])


def gather_packed(arrays, axis, dims):
    flat = jnp.concatenate([a.reshape(-1) for a in arrays])
    lines, at, finished = lax.all_gather(flat, axis), 0, []
    for a, dim in zip(arrays, dims):
        blocks = lines[:, at : at + a.size].reshape(-1, *a.shape)
        finished.append(joined_along(blocks, dim))
        at += a.size
    return tuple(finished)


def gather_axes(shard, axes, dim):
    for axis in reversed(axes):
        shard = lax.all_gather(shard, axis, axis=dim, tiled=True)
    return shard


def folded(shard, axes, dim, update, carry):
    everything = jax.tree.map(lambda part: gather_axes(part, axes, dim), shard)
    return update(carry, everything, jnp.int32(0))


def shortened(shard):
    def short(part):
        return part.astype(jnp.bfloat16) if part.dtype == jnp.float32 else part

    return jax.tree.map(short, shard)


def padded_2(shard, sides, width, wrap):
    for axis, dim in sides:
        devices, length = lax.axis_size(axis), shard.shape[dim]
        up = [(i, (i + 1) % devices) for i in range(devices if wrap else devices - 1)]
        down = [(j, i) for i, j in up]
        last = lax.slice_in_dim(shard, length - width, length, axis=dim)
        first = lax.slice_in_dim(shard, 0, width, axis=dim)
        before = lax.ppermute(last, axis, up)
        after = lax.ppermute(first, axis, down)
        shard = jnp.concatenate([before, shard, after], axis=dim)
    return shard


def scattered(portion, width, axis):
    count = width * lax.axis_size(axis)
    return lax.psum_scatter(portion(jnp.int32(0), count), axis, scatter_dimension=0, tiled=True)


def window_mix(queries, key_rows, value_rows, sink_cols, first, seq_total):
    score_scale = queries.shape[-1] ** (-0.5)
    scores = (
        jnp.einsum("qhgd,khd->hgqk", queries, key_rows, preferred_element_type=jnp.float32)
        * score_scale
    )
    qpos = first + jnp.arange(queries.shape[0], dtype=jnp.int32)
    kpos = first - WINDOW + jnp.arange(key_rows.shape[0], dtype=jnp.int32)
    allowed = (
        (jnp.abs(qpos[:, None] - kpos[None, :]) <= WINDOW)
        & (kpos >= 0)[None, :]
        & (kpos < seq_total)[None, :]
    )
    scores = jnp.where(allowed, scores, negative)
    column = jnp.broadcast_to(sink_cols[:, :, None, None], scores.shape[:-1] + (1,))
    weights_soft = jax.nn.softmax(jnp.concatenate([scores, column], axis=-1), axis=-1)[..., :-1]
    return jnp.einsum(
        "hgqk,khd->qhgd",
        weights_soft,
        value_rows.astype(jnp.float32),
        precision=lax.Precision.HIGHEST,
    )


def short_conv(padded, conv_taps):
    return (
        conv_taps[0][None, :] * padded[:-2]
        + conv_taps[1][None, :] * padded[1:-1]
        + conv_taps[2][None, :] * padded[2:]
    )


def on_device(
    tokens,
    norm_gain,
    query_weight,
    key_weight,
    value_weight,
    conv_in_weight,
    pre_weight,
    post_weight,
    attn_gate_weight,
    conv_gate_weight,
    sink_logit,
    conv_taps,
    attn_out_weight,
    conv_out_weight,
):
    tok_rows = tokens.shape[0]
    widened = tokens.astype(jnp.float32)
    row_sums = gathered_total(jnp.sum(widened * widened, axis=1), TP)
    features = tokens.shape[1] * lax.axis_size(TP)
    normed = (
        widened * lax.rsqrt(row_sums[:, None] / features + epsilon) * norm_gain[None, :]
    ).astype(jnp.bfloat16)
    collected = gather_packed(
        (
            query_weight,
            key_weight,
            value_weight,
            conv_in_weight,
            pre_weight,
            post_weight,
            attn_gate_weight,
            conv_gate_weight,
        ),
        "sp",
        (0, 0, 0, 0, 0, 0, 0, 0),
    )
    stacked = jnp.concatenate(collected, axis=1)

    def add_rows(carry_sum, segment, first):
        rows_here = lax.dynamic_slice_in_dim(stacked, first, segment.shape[1], 0)
        return carry_sum + jnp.dot(segment, rows_here, preferred_element_type=jnp.float32)

    projected = folded(
        normed, TP, 1, add_rows, jnp.zeros((tok_rows, stacked.shape[1]), jnp.float32)
    )
    pieces = []
    offset = 0
    for weight in collected:
        pieces.append(projected[:, offset : offset + weight.shape[1]])
        offset = offset + weight.shape[1]
    queries, key_rows, value_rows, conv_in, pre_gate, post_gate = [
        part_rows.astype(jnp.bfloat16) for part_rows in pieces[:6]
    ]
    attn_gate = pieces[6]
    conv_gate = pieces[7]
    conv_mix = (pre_gate.astype(jnp.float32) * conv_in.astype(jnp.float32)).astype(jnp.bfloat16)
    kv_width = key_rows.shape[1]
    padded = padded_2(
        shortened(jnp.concatenate([key_rows, value_rows, conv_mix], axis=1)),
        (("sp", 0),),
        WINDOW,
        False,
    )
    key_pad = padded[:, :kv_width]
    value_pad = padded[:, kv_width : 2 * kv_width]
    conv_pad = padded[WINDOW - 1 : WINDOW + tok_rows + 1, 2 * kv_width :]
    kv_local = kv_width // HEAD_DIM
    group_size = queries.shape[1] // kv_width
    first_row = lax.axis_index("sp") * tok_rows
    attended = window_mix(
        queries.reshape(tok_rows, kv_local, group_size, HEAD_DIM),
        key_pad.reshape(-1, kv_local, HEAD_DIM),
        value_pad.reshape(-1, kv_local, HEAD_DIM),
        sink_logit.reshape(kv_local, group_size),
        first_row,
        tok_rows * lax.axis_size("sp"),
    )
    attended = attended.reshape(tok_rows, -1).astype(jnp.bfloat16)
    conv_out = (
        post_gate.astype(jnp.float32) * short_conv(conv_pad.astype(jnp.float32), conv_taps)
    ).astype(jnp.bfloat16)
    attn_full, conv_full = gather_packed((attn_out_weight, conv_out_weight), "sp", (1, 1))

    def attn_term(first, number):
        columns = lax.dynamic_slice_in_dim(attn_full, first, number, 1)
        return jnp.dot(attended, columns, preferred_element_type=jnp.float32).T

    def conv_term(first, number):
        columns = lax.dynamic_slice_in_dim(conv_full, first, number, 1)
        return jnp.dot(conv_out, columns, preferred_element_type=jnp.float32).T

    out_rows = attn_gate.shape[1]

    def both_terms(first, number):
        return jnp.concatenate([attn_term(first, number), conv_term(first, number)], axis=1)

    summed = scattered(both_terms, out_rows, TP)
    branch_attn = summed[:, :tok_rows].T
    branch_conv = summed[:, tok_rows:].T
    return (
        jax.nn.sigmoid(attn_gate) * branch_attn + jax.nn.sigmoid(conv_gate) * branch_conv
    ).astype(jnp.bfloat16)


def solution(mesh):
    finer = Mesh(mesh.devices.reshape(mesh.shape["sp"], 4, 2), ("sp", "tp_0", "tp_1"))
    return jax.shard_map(
        on_device,
        mesh=finer,
        in_specs=(
            P("sp", TP),
            P(TP),
            P("sp", TP),
            P("sp", TP),
            P("sp", TP),
            P("sp", TP),
            P("sp", TP),
            P("sp", TP),
            P("sp", TP),
            P("sp", TP),
            P(TP),
            P(None, TP),
            P(TP, "sp"),
            P(TP, "sp"),
        ),
        out_specs=P("sp", TP),
        check_vma=False,
    )
```

profile of v0, /device:TPU:1, one launch (start us, length us, event | category | flops | bytes accessed | tf_op | source)
XLA Modules:
  0.0 228.6 jit_solution(1627320652116977208)
XLA Ops:
  6.5 0.0 all-gather.6.cloned.1.call-start
  6.5 0.7 constant_dynamic-update-slice_fusion.7
  7.3 0.8 reshape.161
  8.0 0.8 reshape.162
  8.8 0.7 constant_dynamic-update-slice_fusion.4
  9.5 0.7 constant_dynamic-update-slice_fusion.3
  10.2 0.7 constant_dynamic-update-slice_fusion.2
  10.9 0.7 constant_dynamic-update-slice_fusion.1
  11.6 0.7 constant_dynamic-update-slice_fusion
  12.2 0.6 copy-done.8
  12.9 0.0 all-gather.6.cloned.1.call-update
  12.9 0.0 reduce-scatter.2.cloned.1.call-start
  12.9 0.8 copy.37
  13.7 0.1 reshape.168
  13.8 0.8 copy.38
  14.6 0.1 reshape.169
  14.7 84.0 %all-gather.2 = bf16[262144]{0:T(1024)(128)(2,1)S(1)} all-gather(bf16[4096]{0:T(1024)(128)(2,1)S(1)} %pad_maximum_fusion.3), channel_id=4, replica_groups=mesh['sp'=64,'tp_0'=4,'tp_1'=2] {'sp'}, dimensions={0}, use_global_device_ids=true | all-gather | bytes 532480 | tf_op jit(solution)/shard_map/all_gather | solution.py:29
  98.7 0.2 reshape.178
  99.0 0.1 fusion.8
  99.1 34.9 %all-gather.3 = f32[8,1,128]{2,1,0:T(1,128)S(1)} all-gather(f32[1,1,128]{2,1,0:T(1,128)S(1)} %bitcast.76), channel_id=2, replica_groups=mesh['sp'=64,'tp_0'=4,'tp_1'=2] {'tp_0','tp_1'}, dimensions={0}, use_global_device_ids=true | all-gather | bytes 4608 | tf_op jit(solution)/shard_map/all_gather | solution.py:17
  134.1 0.1 fusion.10
  134.2 1.9 all_gather.26
  136.0 11.0 %all_gather.27 = bf16[128,1024]{1,0:T(8,128)(2,1)} all-gather(bf16[128,256]{1,0:T(8,128)(2,1)S(1)} %all_gather.26), channel_id=1, replica_groups=mesh['sp'=64,'tp_0'=4,'tp_1'=2] {'tp_0'}, dimensions={1}, use_global_device_ids=true | all-gather | bytes 327680 | tf_op jit(solution)/shard_map/all_gather | solution.py:39
  147.0 0.8 fusion.7
  147.8 0.8 fusion.37
  148.6 0.6 all-gather.6.cloned.1.call-done
  149.3 2.6 %reshape.177 = bf16[64,14336]{1,0:T(8,128)(2,1)S(1)} reshape(bf16[917504]{0:T(1024)(128)(2,1)} %all-gather.6.cloned.1.call-done) | data formatting | bytes 3670016 | tf_op jit(solution)/shard_map/all_gather | solution.py:29
  151.9 0.2 fusion.35
  152.1 0.7 fusion.36
  152.8 0.8 reshape_reshape.24
  153.6 0.8 reshape_reshape.27
  154.4 0.8 reshape_reshape.28
  155.2 0.1 reshape_reshape.29
  155.4 0.8 reshape_reshape.30
  156.2 0.8 reshape_reshape.31
  157.0 0.0 copy-done.6
  157.0 0.2 reshape_reshape.25
  157.2 0.9 reshape_reshape.26
  158.1 0.0 copy-done.5
  158.1 2.3 concatenate.34
  160.4 0.0 copy-start.10
  160.5 1.2 fusion.39
  161.7 0.0 copy-start.9
  161.8 2.4 %collective-permute-start = (bf16[64,256]{1,0:T(8,128)(2,1)S(1)}, bf16[64,256]{1,0:T(8,128)(2,1)S(1)}, u32[]{:S(2)}, u32[]{:S(2)}) collective-permute-start(bf16[64,256]{1,0:T(8,128)(2,1)S(1)} %get-tuple-element.19), channel_id=1, source_target_pairs={{0,8},{8,16},{16,24},{24,32},{32,40},{40,48},{48,56},{56,64},{64,7... | collective-permute-start | bytes 98312 | tf_op jit(solution)/shard_map/ppermute | solution.py:62
  164.1 1.3 collective-permute-start.1
  165.5 0.0 copy-start.12
  165.5 0.3 copy.39
  165.8 0.6 copy.40
  166.4 0.3 copy.45
  166.6 0.6 copy.46
  167.2 0.1 copy.41
  167.4 0.0 collective-permute-done
  167.4 1.4 collective-permute-done.1
  168.8 0.2 fusion.40
  169.0 0.1 broadcast_maximum_fusion
  169.1 0.1 broadcast_in_dim.14
  169.2 0.1 fusion.34
  169.2 0.3 convolution_convert_fusion
  169.5 0.3 fusion.41
  169.8 0.2 fusion.26
  170.1 1.0 pad_maximum_fusion
  171.1 0.0 reduce-scatter.2.cloned.1.call-update
  171.1 49.0 %reduce-scatter.2.cloned.1.call-done = f32[128,256]{0,1:T(8,128)} async-done(((f32[1024,256]{0,1:T(8,128)}), f32[128,256]{0,1:T(8,128)}) %reduce-scatter.2.cloned.1.call-update) | async-done | bytes 131088 | tf_op jit(solution)/shard_map/reduce_scatter | solution.py:70
  220.2 1.6 fusion.13
  (34 shorter events, 0.2 us)
Async XLA Ops:
  6.5 92.4 %copy-start.7 = (bf16[128,128]{1,0:T(8,128)(2,1)S(1)}, bf16[128,128]{1,0:T(8,128)(2,1)}, u32[]{:S(2)}) copy-start(bf16[128,128]{1,0:T(8,128)(2,1)} %param.14) | copy-start | bytes 98308
  6.5 127.5 %copy-start.11 = (f32[128]{0:T(128)S(1)}, f32[128]{0:T(128)}, u32[]{:S(2)}) copy-start(f32[128]{0:T(128)} %param.15) | copy-start | bytes 1540
  6.5 142.7 %all-gather.6.cloned.1.call-start = ((), (), s32[]{:S(2)}) async-start(), calls=%async_computation.2 | async-start | bytes 1863680 | tf_op jit(solution)/shard_map/all_gather | solution.py:29
  12.2 0.6 copy-start.8
  12.9 207.3 %reduce-scatter.2.cloned.1.call-start = ((), (), s32[]{:S(2)}) async-start(), calls=%async_computation.1 | async-start | bytes 1179648 | tf_op jit(solution)/shard_map/reduce_scatter | solution.py:70
  152.8 4.3 %copy-start.6 = (bf16[64,1024]{1,0:T(8,128)(2,1)S(1)}, bf16[64,1024]{1,0:T(8,128)(2,1)}, u32[]{:S(2)}) copy-start(bf16[64,1024]{1,0:T(8,128)(2,1)} %get-tuple-element.12) | copy-start | bytes 393220
  153.6 4.5 %copy-start.3 = (bf16[1024,128]{1,0:T(8,128)(2,1)S(1)}, bf16[1024,128]{1,0:T(8,128)(2,1)}, u32[]{:S(2)}) copy-start(bf16[1024,128]{1,0:T(8,128)(2,1)} %reshape_reshape.24) | copy-start | bytes 786436
  154.4 3.7 %copy-start.4 = (bf16[1024,128]{1,0:T(8,128)(2,1)S(1)}, bf16[1024,128]{1,0:T(8,128)(2,1)}, u32[]{:S(2)}) copy-start(bf16[1024,128]{1,0:T(8,128)(2,1)} %reshape_reshape.27) | copy-start | bytes 786436
  155.2 2.9 %copy-start.5 = (bf16[1024,128]{1,0:T(8,128)(2,1)S(1)}, bf16[1024,128]{1,0:T(8,128)(2,1)}, u32[]{:S(2)}) copy-start(bf16[1024,128]{1,0:T(8,128)(2,1)} %reshape_reshape.28) | copy-start | bytes 786436
  158.1 2.3 copy-start.2
  160.4 5.0 %copy-start.10 = (f32[3,128]{1,0:T(4,128)S(1)}, f32[3,128]{1,0:T(4,128)}, u32[]{:S(2)}) copy-start(f32[3,128]{1,0:T(4,128)} %param.25) | copy-start | bytes 4612
  160.4 5.0 %copy-start.1 = (bf16[64,2048]{1,0:T(8,128)(2,1)S(1)}, bf16[64,2048]{1,0:T(8,128)(2,1)}, u32[]{:S(2)}) copy-start(bf16[64,2048]{1,0:T(8,128)(2,1)} %get-tuple-element.13) | copy-start | bytes 786436
  160.4 5.9 %copy-start = (bf16[64,2048]{1,0:T(8,128)(2,1)S(1)}, bf16[64,2048]{1,0:T(8,128)(2,1)}, u32[]{:S(2)}) copy-start(bf16[64,2048]{1,0:T(8,128)(2,1)} %get-tuple-element.14) | copy-start | bytes 786436
  161.7 7.1 %copy-start.9 = (pred[128,256]{0,1:T(8,128)(4,1)S(1)}, pred[128,256]{0,1:T(8,128)(4,1)}, u32[]{:S(2)}) copy-start(pred[128,256]{0,1:T(8,128)(4,1)} %fusion.7) | copy-start | bytes 98308
  161.8 5.6 %collective-permute-start = (bf16[64,256]{1,0:T(8,128)(2,1)S(1)}, bf16[64,256]{1,0:T(8,128)(2,1)S(1)}, u32[]{:S(2)}, u32[]{:S(2)}) collective-permute-start(bf16[64,256]{1,0:T(8,128)(2,1)S(1)} %get-tuple-element.19), channel_id=1, source_target_pairs={{0,8},{8,16},{16,24},{24,32},{32,40},{40,48},{48,56},{56,64},{64,7... | collective-permute-start | bytes 98312 | tf_op jit(solution)/shard_map/ppermute | solution.py:62
  164.1 4.7 %collective-permute-start.1 = (bf16[64,256]{1,0:T(8,128)(2,1)S(1)}, bf16[64,256]{1,0:T(8,128)(2,1)S(1)}, u32[]{:S(2)}, u32[]{:S(2)}) collective-permute-start(bf16[64,256]{1,0:T(8,128)(2,1)S(1)} %get-tuple-element.20), channel_id=1, source_target_pairs={{8,0},{16,8},{24,16},{32,24},{40,32},{48,40},{56,48},{64,56},{72,6... | collective-permute-start | bytes 98312 | tf_op jit(solution)/shard_map/ppermute | solution.py:63
  165.5 3.6 %copy-start.12 = (f32[2]{0:T(128)S(1)}, f32[2]{0:T(128)}, u32[]{:S(2)}) copy-start(f32[2]{0:T(128)} %param.24) | copy-start | bytes 28
Sparse Core Ops, SparseCore 0:
  13.0 136.2 all-gather.5
  171.3 48.8 reduce-scatter.1
where the time goes:
time: 230 us; the launch traced here: 229 us
  blocking collectives  132 us (57%)
  waiting for transfers between devices  51.1 us (22%)
  local copies, waits for them, and re-layouts  22.2 us (10%)
  between operations  13.7 us (6%)
  other arithmetic  3.86 us (2%)
  starting transfers between devices  3.71 us (2%)
    all_gather x1, blocking collectives, gather_packed(): lines, at, finished = (lax.all_gather(flat, axis), 0, [])  84 us
    reduce_scatter x1, waiting for transfers between devices, scattered(): lax.psum_scatter(portion(jnp.int32(0), count), axis, scatter_dimension=0,...  49 us
    all_gather x1, blocking collectives, gathered_total(): blocks = lax.all_gather(shard, axis)  34.9 us
    all_gather x2, blocking collectives, gather_axes(): shard = lax.all_gather(shard, axis, axis=dim, tiled=True)  12.8 us
    unnamed x35, local copies, waits for them, and re-layouts  5.75 us
    another operation x8, local copies, waits for them, and re-layouts, joined_along(): blocks.reshape(*lengths[:dim], lengths[dim] * lengths[dim + 1], *lengths[...  5.34 us
  transfers between devices with their start and end apart: 4, of which 3 were waited for; matrix products, arithmetic and copies ran while one was open for 3% of the time, Pallas kernels for 0%

commit v1 on v0

v1 whole, which is shorter than its diff:
```python
import functools

import jax
import jax.numpy as jnp
from jax import lax
from jax.experimental import pallas as pl
from jax.experimental.pallas import tpu as pltpu
from jax.sharding import Mesh
from jax.sharding import PartitionSpec as P

ZN, YN, XN, CN = 16, 4, 4, 2
TPN = XN * CN
PLANE = YN * TPN
HALF = 64
WINDOW = 64
LANES = 128
TOK = 128
ROWS = YN * TOK + 2 * WINDOW
SLOT = TOK + WINDOW
FEATURES = TPN * LANES
EPSILON = 1e-06
NEGATIVE = -1e30
F32 = jnp.float32
BF16 = jnp.bfloat16


def nt_dot(a, b):
    return lax.dot_general(a, b, (((1,), (1,)), ((), ())), preferred_element_type=F32)


def nn_dot(a, b):
    return jnp.dot(a, b, preferred_element_type=F32)


def turned(block):
    return jnp.concatenate([block[:, HALF:], block[:, :HALF]], axis=1)


def pack_kernel(tok, q, k, v, ci, pre, post, ag, cg, wa, wc, wy_out, halo_out):
    y = lax.axis_index("y")
    for role in range(YN):
        half = slice(HALF * (role % 2), HALF * (role % 2) + HALF)
        first = (q[:, half], k[...], v[...]) if role < 2 else (ci[:, half], pre[:, half], post[:, half])
        out_weight = wa if role < 2 else wc
        columns = first + (ag[:, :HALF], ag[:, HALF:], cg[:, :HALF], cg[:, HALF:], out_weight[:, half])
        for pair in range(4):
            wy_out[role, 16 * pair : 16 * pair + 16, :] = jnp.concatenate(columns[2 * pair : 2 * pair + 2], axis=1)
    halo_out[...] = jnp.where(y == YN - 1, tok[TOK - WINDOW :, :], tok[:WINDOW, :])


def spread_kernel(tok, halo, gain, out):
    y = lax.axis_index("y")
    g = gain[...]
    high = g.astype(BF16)
    rest = g - high.astype(F32)
    middle = rest.astype(BF16)
    low = (rest - middle.astype(F32)).astype(BF16)
    row = lax.broadcasted_iota(jnp.int32, (WINDOW, LANES), 0)
    parts = [jnp.broadcast_to(part.astype(F32), (WINDOW, LANES)) for part in (high, middle, low)]
    gains = jnp.where(row == 0, parts[0], jnp.where(row == 1, parts[1], jnp.where(row == 2, parts[2], 0.0)))
    slot = jnp.where(y == 1, gains.astype(BF16), halo[...])
    block = tok[...]
    for peer in range(PLANE):
        out[peer, :TOK, :] = block
        out[peer, TOK:, :] = slot


def mix_kernel(t, w, taps, sink, out, own, n_scr, p_scr):
    y = lax.axis_index("y")
    z = lax.axis_index("z")
    gains = []
    for tp in range(TPN):
        r = t[TPN + tp, TOK : TOK + 16, :].astype(F32)
        gains.append(r[0:1] + r[1:2] + r[2:3])
    segments = [(0, 0, TOK, WINDOW)]
    segments += [(WINDOW + TOK * b, b, 0, TOK) for b in range(YN)]
    segments += [(WINDOW + TOK * YN, YN - 1, TOK, WINDOW)]
    for at, b, start, count in segments:
        total = jnp.zeros((count, LANES), F32)
        for tp in range(TPN):
            x = t[b * TPN + tp, start : start + count, :].astype(F32)
            total = total + x * x
        scale = lax.rsqrt(jnp.sum(total, axis=1, keepdims=True) / FEATURES + EPSILON)
        for tp in range(TPN):
            x = t[b * TPN + tp, start : start + count, :].astype(F32)
            n_scr[at : at + count, LANES * tp : LANES * (tp + 1)] = (x * scale * gains[tp]).astype(BF16)
    own[...] = n_scr[pl.ds(pl.multiple_of(WINDOW + TOK * y, WINDOW), TOK), :]
    weight = jnp.concatenate(
        [w[:, :, 16 * pair : 16 * pair + 16, :].reshape(FEATURES, LANES) for pair in range(2)], axis=1
    )
    p_scr[...] = nn_dot(n_scr[...], weight)
    left = lax.broadcasted_iota(jnp.int32, (TOK, LANES), 1) < HALF

    def send(b, mixed):
        for tp in range(TPN):
            columns = w[2 * tp : 2 * tp + 2, :, 48:64, :].reshape(LANES, LANES)
            out[b * TPN + tp] = jnp.where(left, mixed, columns)

    @pl.when(y < 2)
    def _():
        logit = jnp.where(y == 0, sink[0], sink[1])
        span = TOK + 2 * WINDOW
        i = lax.broadcasted_iota(jnp.int32, (TOK, span), 0)
        j = lax.broadcasted_iota(jnp.int32, (TOK, span), 1)
        near = jnp.abs(i + WINDOW - j) <= WINDOW
        for b in range(YN):
            q = p_scr[WINDOW + TOK * b : WINDOW + TOK * (b + 1), :HALF].astype(BF16)
            k = p_scr[TOK * b : TOK * b + span, HALF:LANES].astype(BF16)
            v = p_scr[TOK * b : TOK * b + span, LANES:].astype(BF16)
            scores = nt_dot(q, k) * (HALF**-0.5)
            key = (z * YN + b) * TOK - WINDOW + j
            allowed = near & (key >= 0) & (key < ZN * YN * TOK)
            scores = jnp.where(allowed, scores, NEGATIVE)
            top = jnp.maximum(jnp.max(scores, axis=1, keepdims=True), logit)
            e = jnp.exp(scores - top)
            share = jnp.sum(e, axis=1, keepdims=True) + jnp.exp(logit - top)
            e = e / share
            high = e.astype(BF16)
            low = (e - high.astype(F32)).astype(BF16)
            send(b, (nn_dot(high, v) + nn_dot(low, v)).astype(BF16))

    @pl.when(y >= 2)
    def _():
        t3 = jnp.where(y == YN - 1, turned(taps[...]), taps[...])
        c = p_scr[:, :LANES].astype(BF16).astype(F32)
        p_scr[:, :LANES] = (c * turned(c)).astype(BF16).astype(F32)
        for b in range(YN):
            at = WINDOW + TOK * b
            before = p_scr[at - 1 : at - 1 + TOK, :LANES]
            here = p_scr[at : at + TOK, :LANES]
            after = p_scr[at + 1 : at + 1 + TOK, :LANES]
            post = p_scr[at : at + TOK, LANES:].astype(BF16).astype(F32)
            send(b, (post * (t3[0:1] * before + t3[1:2] * here + t3[2:3] * after)).astype(BF16))


def gate_kernel(own, w, out):
    weight = jnp.concatenate(
        [w[:, :, 16 * pair : 16 * pair + 16, :].reshape(FEATURES, LANES) for pair in range(1, 4)], axis=1
    )
    g = nn_dot(own[...], weight)
    out[...] = jax.nn.sigmoid(g[:, HALF : HALF + 2 * LANES])


def final_kernel(m, gates, out):
    left = lax.broadcasted_iota(jnp.int32, (TOK, LANES), 1) < HALF
    branches = []
    for branch in range(2):
        mixed, columns = [], []
        for tp in range(TPN):
            a = m[(2 * branch) * TPN + tp]
            b = m[(2 * branch + 1) * TPN + tp]
            mixed.append(jnp.where(left, a, turned(b)))
            columns.append(jnp.where(left, turned(a), b))
        branches.append(nt_dot(jnp.concatenate(mixed, axis=1), jnp.concatenate(columns, axis=1)))
    out[...] = (gates[:, :LANES] * branches[0] + gates[:, LANES:] * branches[1]).astype(BF16)


VM = pl.BlockSpec(memory_space=pltpu.VMEM)
SM = pl.BlockSpec(memory_space=pltpu.SMEM)


def shaped(shape, kind=BF16):
    return jax.ShapeDtypeStruct(shape, kind)


def on_device(tok, gain, q, k, v, ci, pre, post, ag, cg, sink, taps, wa, wc):
    plane = ("y", "x", "c")
    wy, halo = pl.pallas_call(
        pack_kernel,
        out_shape=(shaped((YN, 64, LANES)), shaped((WINDOW, LANES))),
        in_specs=[VM] * 11,
        out_specs=(VM, VM),
        name="pack",
    )(tok, q, k, v, ci, pre, post, ag, cg, wa.T, wc.T)
    edges = [(YN * z + YN - 1, YN * z + YN) for z in range(ZN - 1)]
    halo = lax.ppermute(halo, ("z", "y"), edges + [(b, a) for a, b in edges])
    wy = lax.all_to_all(wy, "y", 0, 0, tiled=True)
    spread = pl.pallas_call(
        spread_kernel,
        out_shape=shaped((PLANE, SLOT, LANES)),
        in_specs=[VM] * 3,
        out_specs=VM,
        name="spread",
    )(tok, halo, gain.reshape(1, LANES))
    gathered_tok = lax.all_to_all(spread, plane, 0, 0, tiled=True)
    w = lax.all_gather(wy.reshape(YN * 64, LANES), "z", axis=0, tiled=True).reshape(ZN, YN, 64, LANES)
    message, own = pl.pallas_call(
        mix_kernel,
        out_shape=(shaped((PLANE, TOK, LANES)), shaped((TOK, FEATURES))),
        in_specs=[VM, VM, VM, SM],
        out_specs=(VM, VM),
        scratch_shapes=[pltpu.VMEM((ROWS, FEATURES), BF16), pltpu.VMEM((ROWS, 2 * LANES), F32)],
        name="mix",
    )(gathered_tok, w, taps, sink)
    message = lax.all_to_all(message, plane, 0, 0, tiled=True)
    gates = pl.pallas_call(
        gate_kernel,
        out_shape=shaped((TOK, 2 * LANES), F32),
        in_specs=[VM] * 2,
        out_specs=VM,
        name="gate",
    )(own, w)
    return pl.pallas_call(
        final_kernel,
        out_shape=shaped((TOK, LANES)),
        in_specs=[VM] * 2,
        out_specs=VM,
        name="final",
    )(message, gates)


def solution(mesh):
    finer = Mesh(mesh.devices.reshape(ZN, YN, XN, CN), ("z", "y", "x", "c"))
    sp, tp = ("z", "y"), ("x", "c")
    rows = P(sp, tp)
    columns = P(tp, sp)
    return jax.shard_map(
        on_device,
        mesh=finer,
        in_specs=(rows, P(tp)) + (rows,) * 8 + (P(tp), P(None, tp), columns, columns),
        out_specs=rows,
        check_vma=False,
    )
```

time: 230 us -> 132 us (0.57)
  blocking collectives: 132 us -> 49.5 us
  local copies, waits for them, and re-layouts: 22.2 us -> 1.56 us
  Pallas kernels: 0 us -> 13.6 us
  waiting for transfers between devices: 51.1 us -> 37.7 us
  starting transfers between devices: 3.71 us -> 15.9 us
  other arithmetic: 3.86 us -> 0 us
    all_gather x4 -> x0, blocking collectives: 132 us -> none  [the longest x1 84 us: gather_packed(): lines, at, finished = (lax.all_gather(flat, axis), 0, [])]
    all_to_all x0 -> x2, blocking collectives: none -> 49.5 us  [the longest x1 39.9 us: on_device(): gathered_tok = lax.all_to_all(spread, plane, 0, 0, tiled=True)]
    reduce_scatter x1 -> x0, waiting for transfers between devices: 49 us -> none  [scattered(): lax.psum_scatter(portion(jnp.int32(0), count), axis, scatter_dimension=0,...]
    all_gather x1, waiting for transfers between devices: 0.63 us -> 22.4 us  [on_device(): lax.all_gather(wy.reshape(YN * 64, LANES), 'z', axis=0, tiled=True)]
    all_to_all x0 -> x1, waiting for transfers between devices: none -> 15.3 us  [on_device(): message = lax.all_to_all(message, plane, 0, 0, tiled=True)]
    all_to_all x0 -> x1, starting transfers between devices: none -> 15.3 us  [on_device(): message = lax.all_to_all(message, plane, 0, 0, tiled=True)]
    pallas_call x0 -> x5, Pallas kernels: none -> 13.6 us  [the longest x1 5.09 us: on_device(): pl.pallas_call(mix_kernel, out_shape=(shaped((PLANE, TOK, LANES)), shaped...]
    another operation x8 -> x0, local copies, waits for them, and re-layouts: 5.34 us -> none  [joined_along(): blocks.reshape(*lengths[:dim], lengths[dim] * lengths[dim + 1], *lengths[...]
  transfers between devices with their start and end apart: 4 -> 3, of which waited for: 3 -> 2; matrix products, arithmetic and copies ran while one was open for 3% -> 0% of each run, Pallas kernels for 0% -> 4%
where the time goes in v1:
time: 132 us
  blocking collectives  49.5 us (38%)
  waiting for transfers between devices  37.7 us (29%)
  starting transfers between devices  15.9 us (12%)
  Pallas kernels  13.6 us (10%)
  between operations  13.4 us (10%)
  local copies, waits for them, and re-layouts  1.56 us (1%)
    all_to_all x1, blocking collectives, on_device(): gathered_tok = lax.all_to_all(spread, plane, 0, 0, tiled=True)  39.9 us
    all_gather x1, waiting for transfers between devices, on_device(): lax.all_gather(wy.reshape(YN * 64, LANES), 'z', axis=0, tiled=True)  22.4 us
    all_to_all x1, waiting for transfers between devices, on_device(): message = lax.all_to_all(message, plane, 0, 0, tiled=True)  15.3 us
    all_to_all x1, starting transfers between devices, on_device(): message = lax.all_to_all(message, plane, 0, 0, tiled=True)  15.3 us
    all_to_all x1, blocking collectives, on_device(): wy = lax.all_to_all(wy, 'y', 0, 0, tiled=True)  9.59 us
    pallas_call x1, Pallas kernels, on_device(): pl.pallas_call(mix_kernel, out_shape=(shaped((PLANE, TOK, LANES)), shaped...  5.09 us
  transfers between devices with their start and end apart: 3, of which 2 were waited for; matrix products, arithmetic and copies ran while one was open for 0% of the time, Pallas kernels for 4%

profile of v1, /device:TPU:1, one launch (start us, length us, event | category | flops | bytes accessed | tf_op | source)
XLA Modules:
  0.0 131.8 jit_solution(4521212893068621841)
XLA Ops:
  6.5 0.0 all-gather.2.cloned.1.call-start
  6.5 1.6 %pack.1 = (bf16[4,64,128]{2,1,0:T(8,128)(2,1)}, bf16[64,128]{1,0:T(8,128)(2,1)}) custom-call(bf16[128,128]{1,0:T(8,128)(2,1)} %tok.3, bf16[16,128]{1,0:T(8,128)(2,1)} %q.1, bf16[16,64]{1,0:T(8,128)(2,1)} %k.1, bf16[16,64]{1,0:T(8,128)(2,1)} %v.1, bf16[16,128]{1,0:T(8,128)(2,1)} %ci.1, bf16[16,128]{1,0:T(8,128)(2,1)} %pre.1, bf16[16,128]{1,0:T(8,128)(2,1)} %post.1, ...), custom_call_target="tpu_custom_call" | custom-call | tf_op jit(solution)/shard_map/pack/pallas_call | solution.py:168
  8.1 9.6 %all_to_all.15 = bf16[4,64,128]{2,1,0:T(8,128)(2,1)} all-to-all(bf16[4,64,128]{2,1,0:T(8,128)(2,1)} %get-tuple-element.10), channel_id=1, replica_groups=mesh['z'=16,'y'=4,'x'=4,'c'=2] {'y'}, dimensions={0} | all-to-all | bytes 131072 | tf_op jit(solution)/shard_map/all_to_all | solution.py:177
  17.7 0.0 all-gather.2.cloned.1.call-update
  17.7 0.7 collective-permute-start
  18.4 0.0 collective-permute-done.halo
  18.4 0.0 copy-start.1
  18.4 0.6 copy-done.1
  19.0 2.3 %spread.1 = bf16[32,192,128]{2,1,0:T(8,128)(2,1)} custom-call(bf16[128,128]{1,0:T(8,128)(2,1)} %tok.3, bf16[64,128]{1,0:T(8,128)(2,1)} %copy-done.1, f32[1,128]{1,0:T(1,128)} %bitcast.10), custom_call_target="tpu_custom_call" | custom-call | tf_op jit(solution)/shard_map/spread/pallas_call | solution.py:178
  21.3 39.9 %all_to_all.16.t = bf16[32,192,128]{2,1,0:T(8,128)(2,1)} all-to-all(bf16[32,192,128]{2,1,0:T(8,128)(2,1)} %spread.1), channel_id=1, replica_groups=mesh['z'=16,'y'=4,'x'=4,'c'=2] {'y','x','c'}, dimensions={0} | all-to-all | bytes 3145728 | tf_op jit(solution)/shard_map/all_to_all | solution.py:185
  61.2 22.4 %all-gather.2.cloned.1.call-done = bf16[4096,128]{1,0:T(8,128)(2,1)} async-done(((bf16[256,128]{1,0:T(8,128)(2,1)}), bf16[4096,128]{1,0:T(8,128)(2,1)}) %all-gather.2.cloned.1.call-update) | async-done | bytes 1048592 | tf_op jit(solution)/shard_map/all_gather | solution.py:186
  83.6 5.1 %mix.1 = (bf16[32,128,128]{2,1,0:T(8,128)(2,1)}, bf16[128,1024]{1,0:T(8,128)(2,1)}) custom-call(bf16[32,192,128]{2,1,0:T(8,128)(2,1)} %all_to_all.16.t, bf16[16,4,64,128]{3,2,1,0:T(8,128)(2,1)} %bitcast.5, f32[3,128]{1,0:T(4,128)} %taps.1, f32[2]{0:T(128)} %sink.1), custom_call_target="tpu_custom_call" | custom-call | tf_op jit(solution)/shard_map/mix/pallas_call | solution.py:187
  88.7 15.3 %all-to-all-start.2 = ((bf16[32,128,128]{2,1,0:T(8,128)(2,1)}), bf16[32,128,128]{2,1,0:T(8,128)(2,1)S(1)}, u32[]{:S(2)}, u32[]{:S(2)}) async-start(bf16[32,128,128]{2,1,0:T(8,128)(2,1)} %get-tuple-element.11), calls=%async_computation.2 | async-start | bytes 2097152 | tf_op jit(solution)/shard_map/all_to_all | solution.py:195
  104.0 2.4 %gate.1.gates = f32[128,256]{1,0:T(8,128)} custom-call(bf16[128,1024]{1,0:T(8,128)(2,1)} %get-tuple-element.12.own, bf16[16,4,64,128]{3,2,1,0:T(8,128)(2,1)} %bitcast.6), custom_call_target="tpu_custom_call" | custom-call | tf_op jit(solution)/shard_map/gate/pallas_call | solution.py:196
  106.3 15.3 %all-to-all-done.2.m = bf16[32,128,128]{2,1,0:T(8,128)(2,1)S(1)} async-done(((bf16[32,128,128]{2,1,0:T(8,128)(2,1)}), bf16[32,128,128]{2,1,0:T(8,128)(2,1)S(1)}, u32[]{:S(2)}, u32[]{:S(2)}) %all-to-all-start.2) | async-done | bytes 1048608 | tf_op jit(solution)/shard_map/all_to_all | solution.py:195
  121.7 0.0 copy-start
  121.7 1.0 copy-done
  122.6 2.3 %final.1 = bf16[128,128]{1,0:T(8,128)(2,1)} custom-call(bf16[32,128,128]{2,1,0:T(8,128)(2,1)} %copy-done, f32[128,256]{1,0:T(8,128)} %gate.1.gates), custom_call_target="tpu_custom_call" | custom-call | tf_op jit(solution)/shard_map/final/pallas_call | solution.py:203
Async XLA Ops:
  6.5 77.1 %all-gather.2.cloned.1.call-start = ((), (), s32[]{:S(2)}) async-start(), calls=%async_computation.3 | async-start | bytes 1114112 | tf_op jit(solution)/shard_map/all_gather | solution.py:186
  17.7 0.7 collective-permute-start
  18.4 0.6 copy-start.1
  88.7 32.9 %all-to-all-start.2 = ((bf16[32,128,128]{2,1,0:T(8,128)(2,1)}), bf16[32,128,128]{2,1,0:T(8,128)(2,1)S(1)}, u32[]{:S(2)}, u32[]{:S(2)}) async-start(bf16[32,128,128]{2,1,0:T(8,128)(2,1)} %get-tuple-element.11), calls=%async_computation.2 | async-start | bytes 2097152 | tf_op jit(solution)/shard_map/all_to_all | solution.py:195
  121.7 1.0 copy-start
Sparse Core Ops, SparseCore 0:
  17.8 65.7 all-gather.1

commit v2 on v1

v2 whole, which is shorter than its diff:
```python
import jax
import jax.numpy as jnp
from jax import lax
from jax.experimental import pallas as pl
from jax.experimental.pallas import tpu as pltpu
from jax.sharding import Mesh
from jax.sharding import PartitionSpec as P


ZN, YN, XN, CN = 16, 4, 4, 2
TPN = XN * CN
PLANE = YN * TPN
HALF = 64
WINDOW = 64
LANES = 128
TOK = 128
ROWS = YN * TOK + 2 * WINDOW
SLOT = TOK + WINDOW
FEATURES = TPN * LANES
EPSILON = 1e-06
NEGATIVE = -1e30
F32 = jnp.float32
BF16 = jnp.bfloat16


def nt_dot(a, b):
    return lax.dot_general(a, b, (((1,), (1,)), ((), ())), preferred_element_type=F32)


def nn_dot(a, b):
    return jnp.dot(a, b, preferred_element_type=F32)


def turned(block):
    return jnp.concatenate([block[:, HALF:], block[:, :HALF]], axis=1)


def pack_kernel(tok, gain, q, k, v, ci, pre, post, ag, cg, wa, wc, wy_out, halo_out, base_out):
    y = lax.axis_index("y")
    for role in range(YN):
        half = slice(HALF * (role % 2), HALF * (role % 2) + HALF)
        first = (q, k, v) if role < 2 else (ci, pre, post)
        first = [block[:, half] if block.shape[1] == LANES else block[...] for block in first]
        gate, out_weight = (ag, wa) if role < 2 else (cg, wc)
        wy_out[role, 0:16, :] = jnp.concatenate(first[:2], axis=1)
        wy_out[role, 16:32, :] = jnp.concatenate([first[2], gate[:, half]], axis=1)
        rows = out_weight[:, half].astype(F32)
        wy_out[role, 32:40, :] = jnp.concatenate([rows[:8], rows[8:]], axis=1).astype(BF16)
    halo_out[...] = jnp.where(y == YN - 1, tok[TOK - WINDOW :, :], tok[:WINDOW, :])
    g = gain[...]
    high = g.astype(BF16)
    rest = g - high.astype(F32)
    middle = rest.astype(BF16)
    low = (rest - middle.astype(F32)).astype(BF16)
    row = lax.broadcasted_iota(jnp.int32, (WINDOW, LANES), 0)
    parts = [jnp.broadcast_to(part.astype(F32), (WINDOW, LANES)) for part in (high, middle, low)]
    gains = jnp.where(row == 0, parts[0], jnp.where(row == 1, parts[1], jnp.where(row == 2, parts[2], 0.0)))
    base_out[:TOK, :] = tok[...]
    base_out[TOK:, :] = gains.astype(BF16)


def spread_kernel(base, halo, out):
    y = lax.axis_index("y")
    slot = jnp.where(y == 1, base[TOK:, :], halo[...])
    block = base[:TOK, :]
    for peer in range(PLANE):
        out[peer, :TOK, :] = block
        out[peer, TOK:, :] = slot


def mix_kernel(t, w, taps, sink, out, gates, n_scr, p_scr):
    y = lax.axis_index("y")
    z = lax.axis_index("z")
    gains = []
    for tp in range(TPN):
        r = t[TPN + tp, TOK : TOK + 16, :].astype(F32)
        gains.append(r[0:1] + r[1:2] + r[2:3])
    segments = [(0, 0, TOK, WINDOW)]
    segments += [(WINDOW + TOK * b, b, 0, TOK) for b in range(YN)]
    segments += [(WINDOW + TOK * YN, YN - 1, TOK, WINDOW)]
    for at, b, start, count in segments:
        total = jnp.zeros((count, LANES), F32)
        for tp in range(TPN):
            x = t[b * TPN + tp, start : start + count, :].astype(F32)
            total = total + x * x
        scale = lax.rsqrt(jnp.sum(total, axis=1, keepdims=True) / FEATURES + EPSILON)
        for tp in range(TPN):
            x = t[b * TPN + tp, start : start + count, :].astype(F32)
            n_scr[at : at + count, LANES * tp : LANES * (tp + 1)] = (x * scale * gains[tp]).astype(BF16)
    weight = jnp.concatenate(
        [w[:, :, 16 * pair : 16 * pair + 16, :].reshape(FEATURES, LANES) for pair in range(2)], axis=1
    )
    p_scr[...] = nn_dot(n_scr[...], weight)
    left = lax.broadcasted_iota(jnp.int32, (TOK, LANES), 1) < HALF
    for b in range(YN):
        at = WINDOW + TOK * b
        gates[b] = jnp.where(left[:HALF], turned(p_scr[at : at + HALF, LANES:]), p_scr[at + HALF : at + TOK, LANES:])

    def send(b, mixed):
        for tp in range(TPN):
            rows = w[2 * tp : 2 * tp + 2, :, 32:40, :].astype(F32).reshape(TPN, 8, LANES)
            rows = jnp.stack([turned(rows.reshape(HALF, LANES)).reshape(TPN, 8, LANES), rows], axis=1)
            out[b * TPN + tp] = jnp.where(left, mixed, rows.reshape(LANES, LANES).astype(BF16))

    @pl.when(y < 2)
    def _():
        logit = jnp.where(y == 0, sink[0], sink[1])
        span = TOK + 2 * WINDOW
        i = lax.broadcasted_iota(jnp.int32, (TOK, span), 0)
        j = lax.broadcasted_iota(jnp.int32, (TOK, span), 1)
        near = jnp.abs(i + WINDOW - j) <= WINDOW
        for b in range(YN):
            q = p_scr[WINDOW + TOK * b : WINDOW + TOK * (b + 1), :HALF].astype(BF16)
            k = p_scr[TOK * b : TOK * b + span, HALF:LANES].astype(BF16)
            v = p_scr[TOK * b : TOK * b + span, LANES:].astype(BF16)
            scores = nt_dot(q, k) * (HALF**-0.5)
            key = (z * YN + b) * TOK - WINDOW + j
            allowed = near & (key >= 0) & (key < ZN * YN * TOK)
            scores = jnp.where(allowed, scores, NEGATIVE)
            top = jnp.maximum(jnp.max(scores, axis=1, keepdims=True), logit)
            e = jnp.exp(scores - top)
            share = jnp.sum(e, axis=1, keepdims=True) + jnp.exp(logit - top)
            e = e / share
            high = e.astype(BF16)
            low = (e - high.astype(F32)).astype(BF16)
            send(b, (nn_dot(high, v) + nn_dot(low, v)).astype(BF16))

    @pl.when(y >= 2)
    def _():
        t3 = jnp.where(y == YN - 1, turned(taps[...]), taps[...])
        c = p_scr[:, :LANES].astype(BF16).astype(F32)
        p_scr[:, :LANES] = (c * turned(c)).astype(BF16).astype(F32)
        for b in range(YN):
            at = WINDOW + TOK * b
            before = p_scr[at - 1 : at - 1 + TOK, :LANES]
            here = p_scr[at : at + TOK, :LANES]
            after = p_scr[at + 1 : at + 1 + TOK, :LANES]
            post = p_scr[at : at + TOK, LANES:].astype(BF16).astype(F32)
            send(b, (post * (t3[0:1] * before + t3[1:2] * here + t3[2:3] * after)).astype(BF16))


def joined(a, b, left):
    return jnp.where(left, a, turned(b)), jnp.where(left, turned(a), b)


def gate_kernel(g, out):
    y = lax.axis_index("y")
    left = lax.broadcasted_iota(jnp.int32, (HALF, LANES), 1) < HALF
    for branch in range(2):
        both = joined(g[2 * branch, y], g[2 * branch + 1, y], left)
        out[branch] = jax.nn.sigmoid(jnp.concatenate(both, axis=0))


def final_kernel(m, gates, out):
    left = lax.broadcasted_iota(jnp.int32, (TOK, LANES), 1) < HALF
    total = jnp.zeros((TOK, LANES), F32)
    for branch in range(2):
        mixed, columns = [], []
        for tp in range(TPN):
            both = joined(m[(2 * branch) * TPN + tp], m[(2 * branch + 1) * TPN + tp], left)
            mixed.append(both[0])
            columns.append(both[1])
        value = nt_dot(jnp.concatenate(mixed, axis=1), jnp.concatenate(columns, axis=1))
        total = total + gates[branch] * value
    out[...] = total.astype(BF16)


VM = pl.BlockSpec(memory_space=pltpu.VMEM)
SM = pl.BlockSpec(memory_space=pltpu.SMEM)


def shaped(shape, kind=BF16):
    return jax.ShapeDtypeStruct(shape, kind)


def call(kernel, outs, args, specs=None, scratch=(), limit=8):
    return pl.pallas_call(
        kernel,
        out_shape=outs,
        in_specs=specs or [VM] * len(args),
        out_specs=jax.tree.map(lambda _: VM, outs),
        scratch_shapes=list(scratch),
        compiler_params=pltpu.CompilerParams(vmem_limit_bytes=limit * 2**20),
    )(*args)


def on_device(tok, gain, q, k, v, ci, pre, post, ag, cg, sink, taps, wa, wc):
    plane = ("y", "x", "c")
    wy, halo, base = call(
        pack_kernel,
        (shaped((YN, 40, LANES)), shaped((WINDOW, LANES)), shaped((SLOT, LANES))),
        (tok, gain.reshape(1, LANES), q, k, v, ci, pre, post, ag, cg, wa.T, wc.T),
        limit=60,
    )
    edges = [(YN * z + YN - 1, YN * z + YN) for z in range(ZN - 1)]
    halo = lax.ppermute(halo, ("z", "y"), edges + [(b, a) for a, b in edges])
    wy = lax.all_to_all(wy, "y", 0, 0, tiled=True)
    spread = call(spread_kernel, shaped((PLANE, SLOT, LANES)), (base, halo))
    gathered_tok = lax.all_to_all(spread, plane, 0, 0, tiled=True)
    w = lax.all_gather(wy.reshape(YN * 40, LANES), "z", axis=0, tiled=True).reshape(ZN, YN, 40, LANES)
    message, gates = call(
        mix_kernel,
        (shaped((PLANE, TOK, LANES)), shaped((YN, HALF, LANES), F32)),
        (gathered_tok, w, taps, sink),
        [VM, VM, VM, SM],
        [pltpu.VMEM((ROWS, FEATURES), BF16), pltpu.VMEM((ROWS, 2 * LANES), F32)],
        20,
    )
    message = lax.all_to_all(message, plane, 0, 0, tiled=True)
    gates = lax.all_gather(gates, "y")
    gates = call(gate_kernel, shaped((2, TOK, LANES), F32), (gates,))
    return call(final_kernel, shaped((TOK, LANES)), (message, gates))


def solution(mesh):
    finer = Mesh(mesh.devices.reshape(ZN, YN, XN, CN), ("z", "y", "x", "c"))
    sp, tp = ("z", "y"), ("x", "c")
    rows = P(sp, tp)
    columns = P(tp, sp)
    return jax.shard_map(
        on_device,
        mesh=finer,
        in_specs=(rows, P(tp)) + (rows,) * 8 + (P(tp), P(None, tp), columns, columns),
        out_specs=rows,
        check_vma=False,
    )
```

time: 132 us -> 98.7 us (0.75)
  the two profiles are of different devices: /device:TPU:1 before, /device:TPU:6 now
where the time goes in v2:
time: 98.7 us; the launch traced here: 98.2 us
  blocking collectives  61 us (62%)
  starting transfers between devices  25.7 us (26%)
  Pallas kernels  8.08 us (8%)
  waiting for transfers between devices  2.52 us (3%)
    all_gather x1, blocking collectives, on_device(): lax.all_gather(wy.reshape(YN * 40, LANES), 'z', axis=0, tiled=True)  37.5 us
    all_gather x1, blocking collectives, on_device(): gates = lax.all_gather(gates, 'y')  23.5 us
    all_to_all x1, starting transfers between devices, on_device(): gathered_tok = lax.all_to_all(spread, plane, 0, 0, tiled=True)  14.2 us
    pallas_call x5, Pallas kernels, call(): pl.pallas_call(kernel, out_shape=outs, in_specs=specs or [VM] * len(args)...  8.08 us
    all_to_all x1, starting transfers between devices, on_device(): message = lax.all_to_all(message, plane, 0, 0, tiled=True)  6.44 us
    all_to_all x1, starting transfers between devices, on_device(): wy = lax.all_to_all(wy, 'y', 0, 0, tiled=True)  4.46 us
    all_to_all x1, waiting for transfers between devices, on_device(): wy = lax.all_to_all(wy, 'y', 0, 0, tiled=True)  2.51 us
  transfers between devices with their start and end apart: 4, of which 1 were waited for; matrix products, arithmetic and copies ran while one was open for 0% of the time, Pallas kernels for 2%

profile of v2, /device:TPU:6, one launch (start us, length us, event | category | flops | bytes accessed | tf_op | source)
XLA Modules:
  0.0 98.2 jit_solution(13327270378893045730)
XLA Ops:
  0.0 1.6 %shard_map.136 = (bf16[4,40,128]{2,1,0:T(8,128)(2,1)}, bf16[64,128]{1,0:T(8,128)(2,1)}, bf16[192,128]{1,0:T(8,128)(2,1)}) custom-call(bf16[128,128]{1,0:T(8,128)(2,1)} %tok.1, f32[1,128]{1,0:T(1,128)} %bitcast.11, bf16[16,128]{1,0:T(8,128)(2,1)} %q.1, bf16[16,64]{1,0:T(8,128)(2,1)} %k.1, bf16[16,64]{1,0:T(8,128)(2,1)} %v.1, bf16[16,128]{1,0:T(8,128)(2,1)} %ci.1, ...), custom_call_target="tpu_custom_call" | custom-call | tf_op jit(solution)/shard_map/pallas_call | solution.py:177
  1.6 4.5 %all-to-all-start.1 = ((bf16[4,40,128]{2,1,0:T(8,128)(2,1)}), bf16[4,40,128]{2,1,0:T(8,128)(2,1)S(1)}, u32[]{:S(2)}, u32[]{:S(2)}) async-start(bf16[4,40,128]{2,1,0:T(8,128)(2,1)} %get-tuple-element.12), calls=%async_computation.1 | async-start | bytes 81920 | tf_op jit(solution)/shard_map/all_to_all | solution.py:197
  6.0 0.7 collective-permute-start
  6.7 0.0 collective-permute-done.halo
  6.7 0.0 copy-start
  6.7 0.8 copy-done
  7.5 1.5 %shard_map.137 = bf16[32,192,128]{2,1,0:T(8,128)(2,1)} custom-call(bf16[192,128]{1,0:T(8,128)(2,1)S(1)} %copy-done, bf16[64,128]{1,0:T(8,128)(2,1)S(1)} %collective-permute-done.halo), custom_call_target="tpu_custom_call" | custom-call | tf_op jit(solution)/shard_map/pallas_call | solution.py:177
  9.0 0.0 copy-start.1
  9.0 0.0 copy-start.2
  9.0 2.5 %all-to-all-done.1 = bf16[4,40,128]{2,1,0:T(8,128)(2,1)S(1)} async-done(((bf16[4,40,128]{2,1,0:T(8,128)(2,1)}), bf16[4,40,128]{2,1,0:T(8,128)(2,1)S(1)}, u32[]{:S(2)}, u32[]{:S(2)}) %all-to-all-start.1) | async-done | bytes 40992 | tf_op jit(solution)/shard_map/all_to_all | solution.py:197
  11.5 14.2 %all-to-all-start = ((bf16[32,192,128]{2,1,0:T(8,128)(2,1)}), bf16[32,192,128]{2,1,0:T(8,128)(2,1)S(1)}, u32[]{:S(2)}, u32[]{:S(2)}) async-start(bf16[32,192,128]{2,1,0:T(8,128)(2,1)} %shard_map.137), calls=%async_computation | async-start | bytes 3145728 | tf_op jit(solution)/shard_map/all_to_all | solution.py:199
  25.7 37.5 %all_gather.9 = bf16[2560,128]{1,0:T(8,128)(2,1)S(1)} all-gather(bf16[160,128]{1,0:T(8,128)(2,1)S(1)} %bitcast.8), channel_id=1, replica_groups=mesh['z'=16,'y'=4,'x'=4,'c'=2] {'z'}, dimensions={0}, use_global_device_ids=true | all-gather | bytes 696320 | tf_op jit(solution)/shard_map/all_gather | solution.py:200
  63.2 0.0 all-to-all-done.t
  63.2 0.0 copy-done.1
  63.2 0.0 copy-done.2
  63.2 3.8 %shard_map.138 = (bf16[32,128,128]{2,1,0:T(8,128)(2,1)}, f32[4,64,128]{2,1,0:T(8,128)S(1)}) custom-call(bf16[32,192,128]{2,1,0:T(8,128)(2,1)S(1)} %all-to-all-done.t, bf16[16,4,40,128]{3,2,1,0:T(8,128)(2,1)S(1)} %bitcast.6, f32[3,128]{1,0:T(4,128)S(1)} %copy-done.1, f32[2]{0:T(128)S(1)} %copy-done.2), custom_call_target="tpu_custom_call" | custom-call | tf_op jit(solution)/shard_map/pallas_call | solution.py:177
  67.0 6.4 %all-to-all-start.2 = ((bf16[32,128,128]{2,1,0:T(8,128)(2,1)}), bf16[32,128,128]{2,1,0:T(8,128)(2,1)S(1)}, u32[]{:S(2)}, u32[]{:S(2)}) async-start(bf16[32,128,128]{2,1,0:T(8,128)(2,1)} %get-tuple-element.13), calls=%async_computation.2 | async-start | bytes 2097152 | tf_op jit(solution)/shard_map/all_to_all | solution.py:209
  73.5 23.5 %all-gather = f32[16,64,128]{2,1,0:T(8,128)S(1)} all-gather(f32[4,64,128]{2,1,0:T(8,128)S(1)} %get-tuple-element.14), channel_id=2, replica_groups=mesh['z'=16,'y'=4,'x'=4,'c'=2] {'y'}, dimensions={0}, use_global_device_ids=true | all-gather | bytes 655360 | tf_op jit(solution)/shard_map/all_gather | solution.py:210
  97.0 0.1 shard_map.139.gates
  97.1 0.0 all-to-all-done.2.m
  97.1 1.1 %shard_map.140 = bf16[128,128]{1,0:T(8,128)(2,1)} custom-call(bf16[32,128,128]{2,1,0:T(8,128)(2,1)S(1)} %all-to-all-done.2.m, f32[2,128,128]{2,1,0:T(8,128)S(1)} %shard_map.139.gates), custom_call_target="tpu_custom_call" | custom-call | tf_op jit(solution)/shard_map/pallas_call | solution.py:177
Async XLA Ops:
  1.6 10.0 %all-to-all-start.1 = ((bf16[4,40,128]{2,1,0:T(8,128)(2,1)}), bf16[4,40,128]{2,1,0:T(8,128)(2,1)S(1)}, u32[]{:S(2)}, u32[]{:S(2)}) async-start(bf16[4,40,128]{2,1,0:T(8,128)(2,1)} %get-tuple-element.12), calls=%async_computation.1 | async-start | bytes 81920 | tf_op jit(solution)/shard_map/all_to_all | solution.py:197
  6.0 0.7 collective-permute-start
  6.7 0.8 copy-start
  9.0 54.2 %copy-start.1 = (f32[3,128]{1,0:T(4,128)S(1)}, f32[3,128]{1,0:T(4,128)}, u32[]{:S(2)}) copy-start(f32[3,128]{1,0:T(4,128)} %taps.1) | copy-start | bytes 4612
  9.0 54.2 %copy-start.2 = (f32[2]{0:T(128)S(1)}, f32[2]{0:T(128)}, u32[]{:S(2)}) copy-start(f32[2]{0:T(128)} %sink.1) | copy-start | bytes 28
  11.5 51.7 %all-to-all-start = ((bf16[32,192,128]{2,1,0:T(8,128)(2,1)}), bf16[32,192,128]{2,1,0:T(8,128)(2,1)S(1)}, u32[]{:S(2)}, u32[]{:S(2)}) async-start(bf16[32,192,128]{2,1,0:T(8,128)(2,1)} %shard_map.137), calls=%async_computation | async-start | bytes 3145728 | tf_op jit(solution)/shard_map/all_to_all | solution.py:199
  67.0 30.1 %all-to-all-start.2 = ((bf16[32,128,128]{2,1,0:T(8,128)(2,1)}), bf16[32,128,128]{2,1,0:T(8,128)(2,1)S(1)}, u32[]{:S(2)}, u32[]{:S(2)}) async-start(bf16[32,128,128]{2,1,0:T(8,128)(2,1)} %get-tuple-element.13), calls=%async_computation.2 | async-start | bytes 2097152 | tf_op jit(solution)/shard_map/all_to_all | solution.py:209

commit v3 on v2

v3 whole, which is shorter than its diff:
```python
import jax
import jax.numpy as jnp
from jax import lax
from jax.experimental import pallas as pl
from jax.experimental.pallas import tpu as pltpu
from jax.sharding import Mesh
from jax.sharding import PartitionSpec as P


ZN, YN, XN, CN = 16, 4, 4, 2
TPN = XN * CN
PLANE = YN * TPN
HALF = 64
WINDOW = 64
LANES = 128
TOK = 128
ROWS = YN * TOK
SLOT = TOK + 8
FEATURES = TPN * LANES
EPSILON = 1e-06
NEGATIVE = -1e30
F32 = jnp.float32
BF16 = jnp.bfloat16


def nt_dot(a, b):
    return lax.dot_general(a, b, (((1,), (1,)), ((), ())), preferred_element_type=F32)


def nn_dot(a, b):
    return jnp.dot(a, b, preferred_element_type=F32)


def turned(block):
    return jnp.concatenate([block[:, HALF:], block[:, :HALF]], axis=1)


def pack_kernel(q, k, v, ci, pre, post, ag, cg, wa, wc, wy_out):
    for role in range(YN):
        half = slice(HALF * (role % 2), HALF * (role % 2) + HALF)
        first = (q, k, v) if role < 2 else (ci, pre, post)
        first = [block[:, half] if block.shape[1] == LANES else block[...] for block in first]
        gate, out_weight = (ag, wa) if role < 2 else (cg, wc)
        wy_out[role, 0:16, :] = jnp.concatenate(first[:2], axis=1)
        wy_out[role, 16:32, :] = jnp.concatenate([first[2], gate[:, half]], axis=1)
        rows = out_weight[:, half].astype(F32)
        wy_out[role, 32:40, :] = jnp.concatenate([rows[:8], rows[8:]], axis=1).astype(BF16)


def spread_kernel(tok, gain, out):
    g = gain[...]
    high = g.astype(BF16)
    rest = g - high.astype(F32)
    middle = rest.astype(BF16)
    low = (rest - middle.astype(F32)).astype(BF16)
    row = lax.broadcasted_iota(jnp.int32, (8, LANES), 0)
    parts = [jnp.broadcast_to(part.astype(F32), (8, LANES)) for part in (high, middle, low)]
    gains = jnp.where(row == 0, parts[0], jnp.where(row == 1, parts[1], jnp.where(row == 2, parts[2], 0.0)))
    gains = gains.astype(BF16)
    block = tok[...]
    for peer in range(PLANE):
        out[peer, :TOK, :] = block
        out[peer, TOK:, :] = gains


def project_kernel(t, w, p, up, down, gate_0, gate_1, gate_2, gate_3, n_scr, g_scr):
    y = lax.axis_index("y")
    gains = []
    for tp in range(TPN):
        r = t[tp, TOK:, :].astype(F32)
        gains.append(r[0:1] + r[1:2] + r[2:3])
    for b in range(YN):
        total = jnp.zeros((TOK, LANES), F32)
        for tp in range(TPN):
            x = t[b * TPN + tp, :TOK, :].astype(F32)
            total = total + x * x
        scale = lax.rsqrt(jnp.sum(total, axis=1, keepdims=True) / FEATURES + EPSILON)
        for tp in range(TPN):
            x = t[b * TPN + tp, :TOK, :].astype(F32)
            n_scr[TOK * b : TOK * (b + 1), LANES * tp : LANES * (tp + 1)] = (x * scale * gains[tp]).astype(BF16)
    weight = jnp.concatenate(
        [w[:, :, 16 * pair : 16 * pair + 16, :].reshape(FEATURES, LANES) for pair in range(2)], axis=1
    )
    value = nn_dot(n_scr[...], weight)
    p[...] = value.astype(BF16)
    left = lax.broadcasted_iota(jnp.int32, (HALF, LANES), 1) < HALF
    for out, at in ((up, ROWS - WINDOW), (down, 0)):
        mixed = jnp.where(left & (y < 2), p[at : at + WINDOW, LANES:], p[at : at + WINDOW, :LANES])
        out[...] = mixed
    for b in range(YN):
        at = TOK * b
        g_scr[b] = jnp.where(left, turned(value[at : at + HALF, LANES:]), value[at + HALF : at + TOK, LANES:])
    for k, out in enumerate((gate_0, gate_1, gate_2, gate_3)):
        out[...] = g_scr[lax.rem(y + k, YN)]


def mix_kernel(p, before, after, w, taps, sink, out, c_scr):
    y = lax.axis_index("y")
    z = lax.axis_index("z")
    left = lax.broadcasted_iota(jnp.int32, (TOK, LANES), 1) < HALF

    def send(b, mixed):
        for tp in range(TPN):
            rows = w[2 * tp : 2 * tp + 2, :, 32:40, :].astype(F32).reshape(TPN, 8, LANES)
            rows = jnp.stack([turned(rows.reshape(HALF, LANES)).reshape(TPN, 8, LANES), rows], axis=1)
            out[b * TPN + tp] = jnp.where(left, mixed, rows.reshape(LANES, LANES).astype(BF16))

    @pl.when(y < 2)
    def _():
        logit = jnp.where(y == 0, sink[0], sink[1])
        span = TOK + 2 * WINDOW
        i = lax.broadcasted_iota(jnp.int32, (TOK, span), 0)
        j = lax.broadcasted_iota(jnp.int32, (TOK, span), 1)
        near = jnp.abs(i + WINDOW - j) <= WINDOW
        keys = jnp.concatenate([before[:, HALF:], p[:, HALF:LANES], after[:, HALF:]], axis=0)
        values = jnp.concatenate([before[...], p[:, LANES:], after[...]], axis=0)
        for b in range(YN):
            q = p[TOK * b : TOK * (b + 1), :HALF]
            k = keys[TOK * b : TOK * b + span]
            v = values[TOK * b : TOK * b + span]
            scores = nt_dot(q, k) * (HALF**-0.5)
            key = (z * YN + b) * TOK - WINDOW + j
            allowed = near & (key >= 0) & (key < ZN * YN * TOK)
            scores = jnp.where(allowed, scores, NEGATIVE)
            top = jnp.maximum(jnp.max(scores, axis=1, keepdims=True), logit)
            e = jnp.exp(scores - top)
            share = jnp.sum(e, axis=1, keepdims=True) + jnp.exp(logit - top)
            e = e / share
            high = e.astype(BF16)
            low = (e - high.astype(F32)).astype(BF16)
            send(b, (nn_dot(high, v) + nn_dot(low, v)).astype(BF16))

    @pl.when(y >= 2)
    def _():
        t3 = jnp.where(y == YN - 1, turned(taps[...]), taps[...])

        def gated(block):
            wide = block.astype(F32)
            return (wide * turned(wide)).astype(BF16).astype(F32)

        c_scr[:WINDOW] = gated(before[...])
        c_scr[WINDOW : WINDOW + ROWS] = gated(p[:, :LANES])
        c_scr[WINDOW + ROWS :] = gated(after[...])
        for b in range(YN):
            at = WINDOW + TOK * b
            last = c_scr[at - 1 : at - 1 + TOK]
            here = c_scr[at : at + TOK]
            coming = c_scr[at + 1 : at + 1 + TOK]
            post = p[TOK * b : TOK * (b + 1), LANES:].astype(F32)
            send(b, (post * (t3[0:1] * last + t3[1:2] * here + t3[2:3] * coming)).astype(BF16))


def joined(a, b, left):
    return jnp.where(left, a, turned(b)), jnp.where(left, turned(a), b)


def gate_kernel(g_0, g_1, g_2, g_3, out, g_scr):
    y = lax.axis_index("y")
    for k, g in enumerate((g_0, g_1, g_2, g_3)):
        g_scr[k] = g[...]
    left = lax.broadcasted_iota(jnp.int32, (HALF, LANES), 1) < HALF
    for branch in range(2):
        parts = [g_scr[lax.rem(y + YN - source, YN)] for source in (2 * branch, 2 * branch + 1)]
        out[branch] = jax.nn.sigmoid(jnp.concatenate(joined(*parts, left), axis=0))


def final_kernel(m, gates, out):
    left = lax.broadcasted_iota(jnp.int32, (TOK, LANES), 1) < HALF
    total = jnp.zeros((TOK, LANES), F32)
    for branch in range(2):
        mixed, columns = [], []
        for tp in range(TPN):
            both = joined(m[(2 * branch) * TPN + tp], m[(2 * branch + 1) * TPN + tp], left)
            mixed.append(both[0])
            columns.append(both[1])
        value = nt_dot(jnp.concatenate(mixed, axis=1), jnp.concatenate(columns, axis=1))
        total = total + gates[branch] * value
    out[...] = total.astype(BF16)


VM = pl.BlockSpec(memory_space=pltpu.VMEM)
SM = pl.BlockSpec(memory_space=pltpu.SMEM)


def shaped(shape, kind=BF16):
    return jax.ShapeDtypeStruct(shape, kind)


def call(kernel, outs, args, specs=None, scratch=(), limit=8):
    return pl.pallas_call(
        kernel,
        out_shape=outs,
        in_specs=specs or [VM] * len(args),
        out_specs=jax.tree.map(lambda _: VM, outs),
        scratch_shapes=list(scratch),
        compiler_params=pltpu.CompilerParams(vmem_limit_bytes=limit * 2**20),
    )(*args)


def on_device(tok, gain, q, k, v, ci, pre, post, ag, cg, sink, taps, wa, wc):
    plane = ("y", "x", "c")
    wy = call(pack_kernel, shaped((YN, 40, LANES)), (q, k, v, ci, pre, post, ag, cg, wa.T, wc.T), limit=60)
    wy = lax.all_to_all(wy, "y", 0, 0, tiled=True)
    spread = call(spread_kernel, shaped((PLANE, SLOT, LANES)), (tok, gain.reshape(1, LANES)), limit=60)
    gathered_tok = lax.all_to_all(spread, plane, 0, 0, tiled=True)
    w = lax.all_gather(wy.reshape(YN * 40, LANES), "z", axis=0, tiled=True).reshape(ZN, YN, 40, LANES)
    gate_shape = shaped((HALF, LANES), F32)
    p, up, down, *gates = call(
        project_kernel,
        (shaped((ROWS, 2 * LANES)),) + (shaped((WINDOW, LANES)),) * 2 + (gate_shape,) * 4,
        (gathered_tok, w),
        scratch=[pltpu.VMEM((ROWS, FEATURES), BF16), pltpu.VMEM((YN, HALF, LANES), F32)],
        limit=20,
    )
    before = lax.ppermute(up, "z", [(z, z + 1) for z in range(ZN - 1)])
    after = lax.ppermute(down, "z", [(z + 1, z) for z in range(ZN - 1)])
    for k in range(1, YN):
        gates[k] = lax.ppermute(gates[k], "y", [(y, (y + k) % YN) for y in range(YN)])
    message = call(
        mix_kernel,
        shaped((PLANE, TOK, LANES)),
        (p, before, after, w, taps, sink),
        [VM] * 5 + [SM],
        [pltpu.VMEM((ROWS + 2 * WINDOW, LANES), F32)],
        16,
    )
    message = lax.all_to_all(message, plane, 0, 0, tiled=True)
    gates = call(gate_kernel, shaped((2, TOK, LANES), F32), gates, scratch=[pltpu.VMEM((YN, HALF, LANES), F32)])
    return call(final_kernel, shaped((TOK, LANES)), (message, gates))


def solution(mesh):
    finer = Mesh(mesh.devices.reshape(ZN, YN, XN, CN), ("z", "y", "x", "c"))
    sp, tp = ("z", "y"), ("x", "c")
    rows = P(sp, tp)
    columns = P(tp, sp)
    return jax.shard_map(
        on_device,
        mesh=finer,
        in_specs=(rows, P(tp)) + (rows,) * 8 + (P(tp), P(None, tp), columns, columns),
        out_specs=rows,
        check_vma=False,
    )
```

time: 98.7 us -> 93.4 us (0.946)
  the two profiles are of different devices: /device:TPU:6 before, /device:TPU:1 now
where the time goes in v3:
time: 93.4 us; the launch traced here: 92.8 us
  starting transfers between devices  42.1 us (45%)
  blocking collectives  30.3 us (32%)
  waiting for transfers between devices  11.9 us (13%)
  Pallas kernels  8.46 us (9%)
    all_gather x1, blocking collectives, on_device(): lax.all_gather(wy.reshape(YN * 40, LANES), 'z', axis=0, tiled=True)  30.3 us
    all_to_all x1, starting transfers between devices, on_device(): message = lax.all_to_all(message, plane, 0, 0, tiled=True)  13.7 us
    ppermute x3, starting transfers between devices, on_device(): lax.ppermute(gates[k], 'y', [(y, (y + k) % YN) for y in range(YN)])  10.7 us
    all_to_all x1, starting transfers between devices, on_device(): gathered_tok = lax.all_to_all(spread, plane, 0, 0, tiled=True)  9.81 us
    pallas_call x6, Pallas kernels, call(): pl.pallas_call(kernel, out_shape=outs, in_specs=specs or [VM] * len(args)...  8.46 us
    all_to_all x1, starting transfers between devices, on_device(): wy = lax.all_to_all(wy, 'y', 0, 0, tiled=True)  5 us
    ppermute x3, waiting for transfers between devices, on_device(): lax.ppermute(gates[k], 'y', [(y, (y + k) % YN) for y in range(YN)])  4.61 us
    ppermute x1, waiting for transfers between devices, on_device(): after = lax.ppermute(down, 'z', [(z + 1, z) for z in range(ZN - 1)])  3.17 us
  transfers between devices with their start and end apart: 8, of which 6 were waited for; matrix products, arithmetic and copies ran while one was open for 0% of the time, Pallas kernels for 2%

profile of v3, /device:TPU:1, one launch (start us, length us, event | category | flops | bytes accessed | tf_op | source)
XLA Modules:
  0.0 92.8 jit_solution(10704434246243845326)
XLA Ops:
  0.0 1.5 %shard_map.137 = bf16[4,40,128]{2,1,0:T(8,128)(2,1)} custom-call(bf16[16,128]{1,0:T(8,128)(2,1)} %q.1, bf16[16,64]{1,0:T(8,128)(2,1)} %k.1, bf16[16,64]{1,0:T(8,128)(2,1)} %v.1, bf16[16,128]{1,0:T(8,128)(2,1)} %ci.1, bf16[16,128]{1,0:T(8,128)(2,1)} %pre.1, bf16[16,128]{1,0:T(8,128)(2,1)} %post.1, bf16[16,128]{1,0:T(8,128)(2,1)} %ag.1, bf16[16,128]{1,0:T(8,128)(2,1)} %cg.1, ...), custom_call_target="tpu_custom_call" | custom-call | tf_op jit(solution)/shard_map/pallas_call | solution.py:190
  1.5 5.0 %all-to-all-start.1 = ((bf16[4,40,128]{2,1,0:T(8,128)(2,1)}), bf16[4,40,128]{2,1,0:T(8,128)(2,1)S(1)}, u32[]{:S(2)}, u32[]{:S(2)}) async-start(bf16[4,40,128]{2,1,0:T(8,128)(2,1)} %shard_map.137), calls=%async_computation.1 | async-start | bytes 81920 | tf_op jit(solution)/shard_map/all_to_all | solution.py:203
  6.5 1.9 %shard_map.136 = bf16[32,136,128]{2,1,0:T(8,128)(2,1)} custom-call(bf16[128,128]{1,0:T(8,128)(2,1)} %tok.1, f32[1,128]{1,0:T(1,128)} %bitcast.10), custom_call_target="tpu_custom_call" | custom-call | tf_op jit(solution)/shard_map/pallas_call | solution.py:190
  8.4 2.4 %all-to-all-done.1 = bf16[4,40,128]{2,1,0:T(8,128)(2,1)S(1)} async-done(((bf16[4,40,128]{2,1,0:T(8,128)(2,1)}), bf16[4,40,128]{2,1,0:T(8,128)(2,1)S(1)}, u32[]{:S(2)}, u32[]{:S(2)}) %all-to-all-start.1) | async-done | bytes 40992 | tf_op jit(solution)/shard_map/all_to_all | solution.py:203
  10.9 9.8 %all-to-all-start = ((bf16[32,136,128]{2,1,0:T(8,128)(2,1)}), bf16[32,136,128]{2,1,0:T(8,128)(2,1)S(1)}, u32[]{:S(2)}, u32[]{:S(2)}) async-start(bf16[32,136,128]{2,1,0:T(8,128)(2,1)} %shard_map.136), calls=%async_computation | async-start | bytes 2228224 | tf_op jit(solution)/shard_map/all_to_all | solution.py:205
  20.7 0.0 copy-start
  20.7 0.0 copy-start.1
  20.7 30.3 %all_gather.3 = bf16[2560,128]{1,0:T(8,128)(2,1)S(1)} all-gather(bf16[160,128]{1,0:T(8,128)(2,1)S(1)} %bitcast.7), channel_id=1, replica_groups=mesh['z'=16,'y'=4,'x'=4,'c'=2] {'z'}, dimensions={0}, use_global_device_ids=true | all-gather | bytes 696320 | tf_op jit(solution)/shard_map/all_gather | solution.py:206
  51.0 0.0 all-to-all-done.t
  51.0 0.8 shard_map.138
  51.8 1.6 %collective-permute-start = (bf16[64,128]{1,0:T(8,128)(2,1)S(1)}, bf16[64,128]{1,0:T(8,128)(2,1)S(1)}, u32[]{:S(2)}, u32[]{:S(2)}) collective-permute-start(bf16[64,128]{1,0:T(8,128)(2,1)S(1)} %get-tuple-element.13), channel_id=1, source_target_pairs={{0,32},{32,64},{64,96},{96,128},{128,160},{160,192},{192,224},{224... | collective-permute-start | bytes 49160 | tf_op jit(solution)/shard_map/ppermute | solution.py:215
  53.5 1.3 %collective-permute-start.1 = (bf16[64,128]{1,0:T(8,128)(2,1)S(1)}, bf16[64,128]{1,0:T(8,128)(2,1)S(1)}, u32[]{:S(2)}, u32[]{:S(2)}) collective-permute-start(bf16[64,128]{1,0:T(8,128)(2,1)S(1)} %get-tuple-element.14), channel_id=1, source_target_pairs={{32,0},{64,32},{96,64},{128,96},{160,128},{192,160},{224,192},{256... | collective-permute-start | bytes 49160 | tf_op jit(solution)/shard_map/ppermute | solution.py:216
  54.8 0.0 collective-permute-done.before
  54.8 3.2 %collective-permute-done.1.after = bf16[64,128]{1,0:T(8,128)(2,1)S(1)} collective-permute-done((bf16[64,128]{1,0:T(8,128)(2,1)S(1)}, bf16[64,128]{1,0:T(8,128)(2,1)S(1)}, u32[]{:S(2)}, u32[]{:S(2)}) %collective-permute-start.1) | collective-permute-done | bytes 16416 | tf_op jit(solution)/shard_map/ppermute | solution.py:216
  58.0 0.0 copy-done
  58.0 0.0 copy-done.1
  58.0 3.0 %shard_map.139 = bf16[32,128,128]{2,1,0:T(8,128)(2,1)} custom-call(bf16[512,256]{1,0:T(8,128)(2,1)S(1)} %get-tuple-element.12.p, bf16[64,128]{1,0:T(8,128)(2,1)S(1)} %collective-permute-done.before, bf16[64,128]{1,0:T(8,128)(2,1)S(1)} %collective-permute-done.1.after, bf16[16,4,40,128]{3,2,1,0:T(8,128)(2,1)S(1)} %bitcast.6, f32[3,128]{1,0:T(4,128)S(1)} %copy-done, ...), custom_call_target="tpu_custom_call" | custom-call | tf_op jit(solution)/shard_map/pallas_call | solution.py:190
  61.0 13.7 %all-to-all-start.2 = ((bf16[32,128,128]{2,1,0:T(8,128)(2,1)}), bf16[32,128,128]{2,1,0:T(8,128)(2,1)S(1)}, u32[]{:S(2)}, u32[]{:S(2)}) async-start(bf16[32,128,128]{2,1,0:T(8,128)(2,1)} %shard_map.139), calls=%async_computation.2 | async-start | bytes 2097152 | tf_op jit(solution)/shard_map/all_to_all | solution.py:227
  74.7 3.3 %collective-permute-start.2 = (f32[64,128]{1,0:T(8,128)S(1)}, f32[64,128]{1,0:T(8,128)S(1)}, u32[]{:S(2)}, u32[]{:S(2)}) collective-permute-start(f32[64,128]{1,0:T(8,128)S(1)} %get-tuple-element.16), channel_id=1, source_target_pairs={{0,8},{8,16},{16,24},{24,0},{1,9},{9,17},{17,25},{25,1},{2,10},{10... | collective-permute-start | bytes 98312 | tf_op jit(solution)/shard_map/ppermute | solution.py:218
  78.0 4.3 %collective-permute-start.3 = (f32[64,128]{1,0:T(8,128)S(1)}, f32[64,128]{1,0:T(8,128)S(1)}, u32[]{:S(2)}, u32[]{:S(2)}) collective-permute-start(f32[64,128]{1,0:T(8,128)S(1)} %get-tuple-element.17), channel_id=1, source_target_pairs={{0,16},{8,24},{16,0},{24,8},{1,17},{9,25},{17,1},{25,9},{2,18},{10... | collective-permute-start | bytes 98312 | tf_op jit(solution)/shard_map/ppermute | solution.py:218
  82.3 3.0 %collective-permute-start.4 = (f32[64,128]{1,0:T(8,128)S(1)}, f32[64,128]{1,0:T(8,128)S(1)}, u32[]{:S(2)}, u32[]{:S(2)}) collective-permute-start(f32[64,128]{1,0:T(8,128)S(1)} %get-tuple-element.18), channel_id=1, source_target_pairs={{0,24},{8,0},{16,8},{24,16},{1,25},{9,1},{17,9},{25,17},{2,26},{10... | collective-permute-start | bytes 98312 | tf_op jit(solution)/shard_map/ppermute | solution.py:218
  85.4 0.7 collective-permute-done.2.g_1
  86.1 3.6 %collective-permute-done.3.g_2 = f32[64,128]{1,0:T(8,128)S(1)} collective-permute-done((f32[64,128]{1,0:T(8,128)S(1)}, f32[64,128]{1,0:T(8,128)S(1)}, u32[]{:S(2)}, u32[]{:S(2)}) %collective-permute-start.3) | collective-permute-done | bytes 32800 | tf_op jit(solution)/shard_map/ppermute | solution.py:218
  89.6 0.3 collective-permute-done.4.g_3
  90.0 0.1 shard_map.140.gates
  90.1 1.6 %all-to-all-done.2.m = bf16[32,128,128]{2,1,0:T(8,128)(2,1)S(1)} async-done(((bf16[32,128,128]{2,1,0:T(8,128)(2,1)}), bf16[32,128,128]{2,1,0:T(8,128)(2,1)S(1)}, u32[]{:S(2)}, u32[]{:S(2)}) %all-to-all-start.2) | async-done | bytes 1048608 | tf_op jit(solution)/shard_map/all_to_all | solution.py:227
  91.7 1.1 %shard_map.141 = bf16[128,128]{1,0:T(8,128)(2,1)} custom-call(bf16[32,128,128]{2,1,0:T(8,128)(2,1)S(1)} %all-to-all-done.2.m, f32[2,128,128]{2,1,0:T(8,128)S(1)} %shard_map.140.gates), custom_call_target="tpu_custom_call" | custom-call | tf_op jit(solution)/shard_map/pallas_call | solution.py:190
Async XLA Ops:
  1.5 9.3 %all-to-all-start.1 = ((bf16[4,40,128]{2,1,0:T(8,128)(2,1)}), bf16[4,40,128]{2,1,0:T(8,128)(2,1)S(1)}, u32[]{:S(2)}, u32[]{:S(2)}) async-start(bf16[4,40,128]{2,1,0:T(8,128)(2,1)} %shard_map.137), calls=%async_computation.1 | async-start | bytes 81920 | tf_op jit(solution)/shard_map/all_to_all | solution.py:203
  10.9 40.1 %all-to-all-start = ((bf16[32,136,128]{2,1,0:T(8,128)(2,1)}), bf16[32,136,128]{2,1,0:T(8,128)(2,1)S(1)}, u32[]{:S(2)}, u32[]{:S(2)}) async-start(bf16[32,136,128]{2,1,0:T(8,128)(2,1)} %shard_map.136), calls=%async_computation | async-start | bytes 2228224 | tf_op jit(solution)/shard_map/all_to_all | solution.py:205
  20.7 37.3 %copy-start = (f32[3,128]{1,0:T(4,128)S(1)}, f32[3,128]{1,0:T(4,128)}, u32[]{:S(2)}) copy-start(f32[3,128]{1,0:T(4,128)} %taps.1) | copy-start | bytes 4612
  20.7 37.3 %copy-start.1 = (f32[2]{0:T(128)S(1)}, f32[2]{0:T(128)}, u32[]{:S(2)}) copy-start(f32[2]{0:T(128)} %sink.1) | copy-start | bytes 28
  51.8 2.9 %collective-permute-start = (bf16[64,128]{1,0:T(8,128)(2,1)S(1)}, bf16[64,128]{1,0:T(8,128)(2,1)S(1)}, u32[]{:S(2)}, u32[]{:S(2)}) collective-permute-start(bf16[64,128]{1,0:T(8,128)(2,1)S(1)} %get-tuple-element.13), channel_id=1, source_target_pairs={{0,32},{32,64},{64,96},{96,128},{128,160},{160,192},{192,224},{224... | collective-permute-start | bytes 49160 | tf_op jit(solution)/shard_map/ppermute | solution.py:215
  53.5 4.5 %collective-permute-start.1 = (bf16[64,128]{1,0:T(8,128)(2,1)S(1)}, bf16[64,128]{1,0:T(8,128)(2,1)S(1)}, u32[]{:S(2)}, u32[]{:S(2)}) collective-permute-start(bf16[64,128]{1,0:T(8,128)(2,1)S(1)} %get-tuple-element.14), channel_id=1, source_target_pairs={{32,0},{64,32},{96,64},{128,96},{160,128},{192,160},{224,192},{256... | collective-permute-start | bytes 49160 | tf_op jit(solution)/shard_map/ppermute | solution.py:216
  61.0 30.8 %all-to-all-start.2 = ((bf16[32,128,128]{2,1,0:T(8,128)(2,1)}), bf16[32,128,128]{2,1,0:T(8,128)(2,1)S(1)}, u32[]{:S(2)}, u32[]{:S(2)}) async-start(bf16[32,128,128]{2,1,0:T(8,128)(2,1)} %shard_map.139), calls=%async_computation.2 | async-start | bytes 2097152 | tf_op jit(solution)/shard_map/all_to_all | solution.py:227
  74.7 11.4 %collective-permute-start.2 = (f32[64,128]{1,0:T(8,128)S(1)}, f32[64,128]{1,0:T(8,128)S(1)}, u32[]{:S(2)}, u32[]{:S(2)}) collective-permute-start(f32[64,128]{1,0:T(8,128)S(1)} %get-tuple-element.16), channel_id=1, source_target_pairs={{0,8},{8,16},{16,24},{24,0},{1,9},{9,17},{17,25},{25,1},{2,10},{10... | collective-permute-start | bytes 98312 | tf_op jit(solution)/shard_map/ppermute | solution.py:218
  78.0 11.7 %collective-permute-start.3 = (f32[64,128]{1,0:T(8,128)S(1)}, f32[64,128]{1,0:T(8,128)S(1)}, u32[]{:S(2)}, u32[]{:S(2)}) collective-permute-start(f32[64,128]{1,0:T(8,128)S(1)} %get-tuple-element.17), channel_id=1, source_target_pairs={{0,16},{8,24},{16,0},{24,8},{1,17},{9,25},{17,1},{25,9},{2,18},{10... | collective-permute-start | bytes 98312 | tf_op jit(solution)/shard_map/ppermute | solution.py:218
  82.3 7.7 %collective-permute-start.4 = (f32[64,128]{1,0:T(8,128)S(1)}, f32[64,128]{1,0:T(8,128)S(1)}, u32[]{:S(2)}, u32[]{:S(2)}) collective-permute-start(f32[64,128]{1,0:T(8,128)S(1)} %get-tuple-element.18), channel_id=1, source_target_pairs={{0,24},{8,0},{16,8},{24,16},{1,25},{9,1},{17,9},{25,17},{2,26},{10... | collective-permute-start | bytes 98312 | tf_op jit(solution)/shard_map/ppermute | solution.py:218

commit v4 on v2

--- a/solution.py
+++ b/solution.py
@@ -35,8 +35,7 @@
     return jnp.concatenate([block[:, HALF:], block[:, :HALF]], axis=1)
 
 
-def pack_kernel(tok, gain, q, k, v, ci, pre, post, ag, cg, wa, wc, wy_out, halo_out, base_out):
-    y = lax.axis_index("y")
+def pack_kernel(q, k, v, ci, pre, post, ag, cg, wa, wc, wy_out):
     for role in range(YN):
         half = slice(HALF * (role % 2), HALF * (role % 2) + HALF)
         first = (q, k, v) if role < 2 else (ci, pre, post)
@@ -46,34 +45,33 @@
         wy_out[role, 16:32, :] = jnp.concatenate([first[2], gate[:, half]], axis=1)
         rows = out_weight[:, half].astype(F32)
         wy_out[role, 32:40, :] = jnp.concatenate([rows[:8], rows[8:]], axis=1).astype(BF16)
-    halo_out[...] = jnp.where(y == YN - 1, tok[TOK - WINDOW :, :], tok[:WINDOW, :])
+
+
+def spread_kernel(tok, gain, edge, out):
+    y = lax.axis_index("y")
     g = gain[...]
     high = g.astype(BF16)
     rest = g - high.astype(F32)
     middle = rest.astype(BF16)
     low = (rest - middle.astype(F32)).astype(BF16)
-    row = lax.broadcasted_iota(jnp.int32, (WINDOW, LANES), 0)
-    parts = [jnp.broadcast_to(part.astype(F32), (WINDOW, LANES)) for part in (high, middle, low)]
+    row = lax.broadcasted_iota(jnp.int32, (8, LANES), 0)
+    parts = [jnp.broadcast_to(part.astype(F32), (8, LANES)) for part in (high, middle, low)]
     gains = jnp.where(row == 0, parts[0], jnp.where(row == 1, parts[1], jnp.where(row == 2, parts[2], 0.0)))
-    base_out[:TOK, :] = tok[...]
-    base_out[TOK:, :] = gains.astype(BF16)
-
-
-def spread_kernel(base, halo, out):
-    y = lax.axis_index("y")
-    slot = jnp.where(y == 1, base[TOK:, :], halo[...])
-    block = base[:TOK, :]
+    gains = gains.astype(BF16)
+    block = tok[...]
+    halo = jnp.where(y == YN - 1, edge[:WINDOW, :], edge[TOK - WINDOW :, :])
     for peer in range(PLANE):
         out[peer, :TOK, :] = block
-        out[peer, TOK:, :] = slot
-
-
-def mix_kernel(t, w, taps, sink, out, gates, n_scr, p_scr):
+        out[peer, TOK:SLOT, :] = halo
+        out[peer, SLOT:, :] = gains
+
+
+def mix_kernel(t, w, taps, sink, out, gate_0, gate_1, gate_2, gate_3, n_scr, p_scr, g_scr):
     y = lax.axis_index("y")
     z = lax.axis_index("z")
     gains = []
     for tp in range(TPN):
-        r = t[TPN + tp, TOK : TOK + 16, :].astype(F32)
+        r = t[tp, SLOT:, :].astype(F32)
         gains.append(r[0:1] + r[1:2] + r[2:3])
     segments = [(0, 0, TOK, WINDOW)]
     segments += [(WINDOW + TOK * b, b, 0, TOK) for b in range(YN)]
@@ -94,7 +92,9 @@
     left = lax.broadcasted_iota(jnp.int32, (TOK, LANES), 1) < HALF
     for b in range(YN):
         at = WINDOW + TOK * b
-        gates[b] = jnp.where(left[:HALF], turned(p_scr[at : at + HALF, LANES:]), p_scr[at + HALF : at + TOK, LANES:])
+        g_scr[b] = jnp.where(left[:HALF], turned(p_scr[at : at + HALF, LANES:]), p_scr[at + HALF : at + TOK, LANES:])
+    for k, gate in enumerate((gate_0, gate_1, gate_2, gate_3)):
+        gate[...] = g_scr[lax.rem(y + k, YN)]
 
     def send(b, mixed):
         for tp in range(TPN):
@@ -143,12 +143,14 @@
     return jnp.where(left, a, turned(b)), jnp.where(left, turned(a), b)
 
 
-def gate_kernel(g, out):
+def gate_kernel(g_0, g_1, g_2, g_3, out, g_scr):
     y = lax.axis_index("y")
+    for k, g in enumerate((g_0, g_1, g_2, g_3)):
+        g_scr[k] = g[...]
     left = lax.broadcasted_iota(jnp.int32, (HALF, LANES), 1) < HALF
     for branch in range(2):
-        both = joined(g[2 * branch, y], g[2 * branch + 1, y], left)
-        out[branch] = jax.nn.sigmoid(jnp.concatenate(both, axis=0))
+        parts = [g_scr[lax.rem(y + YN - source, YN)] for source in (2 * branch, 2 * branch + 1)]
+        out[branch] = jax.nn.sigmoid(jnp.concatenate(joined(*parts, left), axis=0))
 
 
 def final_kernel(m, gates, out):
@@ -186,29 +188,29 @@
 
 def on_device(tok, gain, q, k, v, ci, pre, post, ag, cg, sink, taps, wa, wc):
     plane = ("y", "x", "c")
-    wy, halo, base = call(
-        pack_kernel,
-        (shaped((YN, 40, LANES)), shaped((WINDOW, LANES)), shaped((SLOT, LANES))),
-        (tok, gain.reshape(1, LANES), q, k, v, ci, pre, post, ag, cg, wa.T, wc.T),
-        limit=60,
-    )
     edges = [(YN * z + YN - 1, YN * z + YN) for z in range(ZN - 1)]
-    halo = lax.ppermute(halo, ("z", "y"), edges + [(b, a) for a, b in edges])
+    edge = lax.ppermute(tok, ("z", "y"), edges + [(b, a) for a, b in edges])
+    wy = call(pack_kernel, shaped((YN, 40, LANES)), (q, k, v, ci, pre, post, ag, cg, wa.T, wc.T), limit=60)
     wy = lax.all_to_all(wy, "y", 0, 0, tiled=True)
-    spread = call(spread_kernel, shaped((PLANE, SLOT, LANES)), (base, halo))
+    spread = call(spread_kernel, shaped((PLANE, SLOT + 8, LANES)), (tok, gain.reshape(1, LANES), edge), limit=60)
     gathered_tok = lax.all_to_all(spread, plane, 0, 0, tiled=True)
     w = lax.all_gather(wy.reshape(YN * 40, LANES), "z", axis=0, tiled=True).reshape(ZN, YN, 40, LANES)
-    message, gates = call(
+    message, *gates = call(
         mix_kernel,
-        (shaped((PLANE, TOK, LANES)), shaped((YN, HALF, LANES), F32)),
+        (shaped((PLANE, TOK, LANES)),) + (shaped((HALF, LANES), F32),) * 4,
         (gathered_tok, w, taps, sink),
-        [VM, VM, VM, SM],
-        [pltpu.VMEM((ROWS, FEATURES), BF16), pltpu.VMEM((ROWS, 2 * LANES), F32)],
+        [VM] * 3 + [SM],
+        [
+            pltpu.VMEM((ROWS, FEATURES), BF16),
+            pltpu.VMEM((ROWS, 2 * LANES), F32),
+            pltpu.VMEM((YN, HALF, LANES), F32),
+        ],
         20,
     )
     message = lax.all_to_all(message, plane, 0, 0, tiled=True)
-    gates = lax.all_gather(gates, "y")
-    gates = call(gate_kernel, shaped((2, TOK, LANES), F32), (gates,))
+    for k in range(1, YN):
+        gates[k] = lax.ppermute(gates[k], "y", [(y, (y + k) % YN) for y in range(YN)])
+    gates = call(gate_kernel, shaped((2, TOK, LANES), F32), gates, scratch=[pltpu.VMEM((YN, HALF, LANES), F32)])
     return call(final_kernel, shaped((TOK, LANES)), (message, gates))
 
 

time: 98.7 us -> 90.5 us (0.917)
  the two profiles are of different devices: /device:TPU:6 before, /device:TPU:1 now
where the time goes in v4:
time: 90.5 us; the launch traced here: 89.9 us
  starting transfers between devices  38 us (42%)
  blocking collectives  34.6 us (38%)
  Pallas kernels  8.87 us (10%)
  waiting for transfers between devices  7.77 us (9%)
    all_gather x1, blocking collectives, on_device(): lax.all_gather(wy.reshape(YN * 40, LANES), 'z', axis=0, tiled=True)  34.6 us
    all_to_all x1, starting transfers between devices, on_device(): message = lax.all_to_all(message, plane, 0, 0, tiled=True)  11.9 us
    ppermute x3, starting transfers between devices, on_device(): lax.ppermute(gates[k], 'y', [(y, (y + k) % YN) for y in range(YN)])  10.7 us
    pallas_call x5, Pallas kernels, call(): pl.pallas_call(kernel, out_shape=outs, in_specs=specs or [VM] * len(args)...  8.87 us
    all_to_all x1, starting transfers between devices, on_device(): gathered_tok = lax.all_to_all(spread, plane, 0, 0, tiled=True)  7.49 us
    all_to_all x1, starting transfers between devices, on_device(): wy = lax.all_to_all(wy, 'y', 0, 0, tiled=True)  7.36 us
    ppermute x3, waiting for transfers between devices, on_device(): lax.ppermute(gates[k], 'y', [(y, (y + k) % YN) for y in range(YN)])  4.61 us
  transfers between devices with their start and end apart: 7, of which 5 were waited for; matrix products, arithmetic and copies ran while one was open for 0% of the time, Pallas kernels for 4%

profile of v4, /device:TPU:1, one launch (start us, length us, event | category | flops | bytes accessed | tf_op | source)
XLA Modules:
  0.0 89.9 jit_solution(5094281926891408965)
XLA Ops:
  0.0 0.7 collective-permute-start
  0.7 1.5 %shard_map.137 = bf16[4,40,128]{2,1,0:T(8,128)(2,1)} custom-call(bf16[16,128]{1,0:T(8,128)(2,1)} %q.1, bf16[16,64]{1,0:T(8,128)(2,1)} %k.1, bf16[16,64]{1,0:T(8,128)(2,1)} %v.1, bf16[16,128]{1,0:T(8,128)(2,1)} %ci.1, bf16[16,128]{1,0:T(8,128)(2,1)} %pre.1, bf16[16,128]{1,0:T(8,128)(2,1)} %post.1, bf16[16,128]{1,0:T(8,128)(2,1)} %ag.1, bf16[16,128]{1,0:T(8,128)(2,1)} %cg.1, ...), custom_call_target="tpu_custom_call" | custom-call | tf_op jit(solution)/shard_map/pallas_call | solution.py:179
  2.2 7.4 %all-to-all-start.1 = ((bf16[4,40,128]{2,1,0:T(8,128)(2,1)}), bf16[4,40,128]{2,1,0:T(8,128)(2,1)S(1)}, u32[]{:S(2)}, u32[]{:S(2)}) async-start(bf16[4,40,128]{2,1,0:T(8,128)(2,1)} %shard_map.137), calls=%async_computation.1 | async-start | bytes 81920 | tf_op jit(solution)/shard_map/all_to_all | solution.py:194
  9.5 0.0 collective-permute-done.edge
  9.5 0.0 copy-start.2
  9.5 0.6 copy-done.2
  10.2 2.2 %shard_map.136 = bf16[32,200,128]{2,1,0:T(8,128)(2,1)} custom-call(bf16[128,128]{1,0:T(8,128)(2,1)} %tok.1, f32[1,128]{1,0:T(1,128)} %bitcast.9, bf16[128,128]{1,0:T(8,128)(2,1)} %copy-done.2), custom_call_target="tpu_custom_call" | custom-call | tf_op jit(solution)/shard_map/pallas_call | solution.py:179
  12.4 0.0 copy-start
  12.4 0.0 copy-start.1
  12.4 1.5 %all-to-all-done.1 = bf16[4,40,128]{2,1,0:T(8,128)(2,1)S(1)} async-done(((bf16[4,40,128]{2,1,0:T(8,128)(2,1)}), bf16[4,40,128]{2,1,0:T(8,128)(2,1)S(1)}, u32[]{:S(2)}, u32[]{:S(2)}) %all-to-all-start.1) | async-done | bytes 40992 | tf_op jit(solution)/shard_map/all_to_all | solution.py:194
  13.9 7.5 %all-to-all-start = ((bf16[32,200,128]{2,1,0:T(8,128)(2,1)}), bf16[32,200,128]{2,1,0:T(8,128)(2,1)S(1)}, u32[]{:S(2)}, u32[]{:S(2)}) async-start(bf16[32,200,128]{2,1,0:T(8,128)(2,1)} %shard_map.136), calls=%async_computation | async-start | bytes 3276800 | tf_op jit(solution)/shard_map/all_to_all | solution.py:196
  21.4 34.6 %all_gather.3 = bf16[2560,128]{1,0:T(8,128)(2,1)S(1)} all-gather(bf16[160,128]{1,0:T(8,128)(2,1)S(1)} %bitcast.6), channel_id=1, replica_groups=mesh['z'=16,'y'=4,'x'=4,'c'=2] {'z'}, dimensions={0}, use_global_device_ids=true | all-gather | bytes 696320 | tf_op jit(solution)/shard_map/all_gather | solution.py:197
  56.0 0.0 all-to-all-done.t
  56.0 0.0 copy-done
  56.0 0.0 copy-done.1
  56.0 3.9 %shard_map.138 = (bf16[32,128,128]{2,1,0:T(8,128)(2,1)}, f32[64,128]{1,0:T(8,128)S(1)}, f32[64,128]{1,0:T(8,128)S(1)}, f32[64,128]{1,0:T(8,128)S(1)}, f32[64,128]{1,0:T(8,128)S(1)}) custom-call(bf16[32,200,128]{2,1,0:T(8,128)(2,1)S(1)} %all-to-all-done.t, bf16[16,4,40,128]{3,2,1,0:T(8,128)(2,1)S(1)} %bitcast.5, f32[3,128]{1,0:T(4,128)S(1)} %copy-done, ...), custom_call_target="tpu_custom_call" | custom-call | tf_op jit(solution)/shard_map/pallas_call | solution.py:179
  59.9 11.9 %all-to-all-start.2 = ((bf16[32,128,128]{2,1,0:T(8,128)(2,1)}), bf16[32,128,128]{2,1,0:T(8,128)(2,1)S(1)}, u32[]{:S(2)}, u32[]{:S(2)}) async-start(bf16[32,128,128]{2,1,0:T(8,128)(2,1)} %get-tuple-element.10), calls=%async_computation.2 | async-start | bytes 2097152 | tf_op jit(solution)/shard_map/all_to_all | solution.py:210
  71.8 3.3 %collective-permute-start.1 = (f32[64,128]{1,0:T(8,128)S(1)}, f32[64,128]{1,0:T(8,128)S(1)}, u32[]{:S(2)}, u32[]{:S(2)}) collective-permute-start(f32[64,128]{1,0:T(8,128)S(1)} %get-tuple-element.12), channel_id=1, source_target_pairs={{0,8},{8,16},{16,24},{24,0},{1,9},{9,17},{17,25},{25,1},{2,10},{10... | collective-permute-start | bytes 98312 | tf_op jit(solution)/shard_map/ppermute | solution.py:212
  75.1 4.3 %collective-permute-start.2 = (f32[64,128]{1,0:T(8,128)S(1)}, f32[64,128]{1,0:T(8,128)S(1)}, u32[]{:S(2)}, u32[]{:S(2)}) collective-permute-start(f32[64,128]{1,0:T(8,128)S(1)} %get-tuple-element.13), channel_id=1, source_target_pairs={{0,16},{8,24},{16,0},{24,8},{1,17},{9,25},{17,1},{25,9},{2,18},{10... | collective-permute-start | bytes 98312 | tf_op jit(solution)/shard_map/ppermute | solution.py:212
  79.4 3.0 %collective-permute-start.3 = (f32[64,128]{1,0:T(8,128)S(1)}, f32[64,128]{1,0:T(8,128)S(1)}, u32[]{:S(2)}, u32[]{:S(2)}) collective-permute-start(f32[64,128]{1,0:T(8,128)S(1)} %get-tuple-element.14), channel_id=1, source_target_pairs={{0,24},{8,0},{16,8},{24,16},{1,25},{9,1},{17,9},{25,17},{2,26},{10... | collective-permute-start | bytes 98312 | tf_op jit(solution)/shard_map/ppermute | solution.py:212
  82.5 0.7 collective-permute-done.1.g_1
  83.2 3.6 %collective-permute-done.2.g_2 = f32[64,128]{1,0:T(8,128)S(1)} collective-permute-done((f32[64,128]{1,0:T(8,128)S(1)}, f32[64,128]{1,0:T(8,128)S(1)}, u32[]{:S(2)}, u32[]{:S(2)}) %collective-permute-start.2) | collective-permute-done | bytes 32800 | tf_op jit(solution)/shard_map/ppermute | solution.py:212
  86.7 0.3 collective-permute-done.3.g_3
  87.1 0.1 shard_map.139.gates
  87.2 1.6 %all-to-all-done.2.m = bf16[32,128,128]{2,1,0:T(8,128)(2,1)S(1)} async-done(((bf16[32,128,128]{2,1,0:T(8,128)(2,1)}), bf16[32,128,128]{2,1,0:T(8,128)(2,1)S(1)}, u32[]{:S(2)}, u32[]{:S(2)}) %all-to-all-start.2) | async-done | bytes 1048608 | tf_op jit(solution)/shard_map/all_to_all | solution.py:210
  88.8 1.1 %shard_map.140 = bf16[128,128]{1,0:T(8,128)(2,1)} custom-call(bf16[32,128,128]{2,1,0:T(8,128)(2,1)S(1)} %all-to-all-done.2.m, f32[2,128,128]{2,1,0:T(8,128)S(1)} %shard_map.139.gates), custom_call_target="tpu_custom_call" | custom-call | tf_op jit(solution)/shard_map/pallas_call | solution.py:179
Async XLA Ops:
  0.0 9.5 %collective-permute-start = (bf16[128,128]{1,0:T(8,128)(2,1)}, bf16[128,128]{1,0:T(8,128)(2,1)S(1)}, u32[]{:S(2)}, u32[]{:S(2)}) collective-permute-start(bf16[128,128]{1,0:T(8,128)(2,1)} %tok.1), channel_id=1, source_target_pairs={{24,32},{56,64},{88,96},{120,128},{152,160},{184,192},{216,224},{2... | collective-permute-start | bytes 98312 | tf_op jit(solution)/shard_map/ppermute | solution.py:192
  2.2 11.7 %all-to-all-start.1 = ((bf16[4,40,128]{2,1,0:T(8,128)(2,1)}), bf16[4,40,128]{2,1,0:T(8,128)(2,1)S(1)}, u32[]{:S(2)}, u32[]{:S(2)}) async-start(bf16[4,40,128]{2,1,0:T(8,128)(2,1)} %shard_map.137), calls=%async_computation.1 | async-start | bytes 81920 | tf_op jit(solution)/shard_map/all_to_all | solution.py:194
  9.5 0.6 copy-start.2
  12.4 43.6 %copy-start = (f32[3,128]{1,0:T(4,128)S(1)}, f32[3,128]{1,0:T(4,128)}, u32[]{:S(2)}) copy-start(f32[3,128]{1,0:T(4,128)} %taps.1) | copy-start | bytes 4612
  12.4 43.6 %copy-start.1 = (f32[2]{0:T(128)S(1)}, f32[2]{0:T(128)}, u32[]{:S(2)}) copy-start(f32[2]{0:T(128)} %sink.1) | copy-start | bytes 28
  13.9 42.1 %all-to-all-start = ((bf16[32,200,128]{2,1,0:T(8,128)(2,1)}), bf16[32,200,128]{2,1,0:T(8,128)(2,1)S(1)}, u32[]{:S(2)}, u32[]{:S(2)}) async-start(bf16[32,200,128]{2,1,0:T(8,128)(2,1)} %shard_map.136), calls=%async_computation | async-start | bytes 3276800 | tf_op jit(solution)/shard_map/all_to_all | solution.py:196
  59.9 28.9 %all-to-all-start.2 = ((bf16[32,128,128]{2,1,0:T(8,128)(2,1)}), bf16[32,128,128]{2,1,0:T(8,128)(2,1)S(1)}, u32[]{:S(2)}, u32[]{:S(2)}) async-start(bf16[32,128,128]{2,1,0:T(8,128)(2,1)} %get-tuple-element.10), calls=%async_computation.2 | async-start | bytes 2097152 | tf_op jit(solution)/shard_map/all_to_all | solution.py:210
  71.8 11.4 %collective-permute-start.1 = (f32[64,128]{1,0:T(8,128)S(1)}, f32[64,128]{1,0:T(8,128)S(1)}, u32[]{:S(2)}, u32[]{:S(2)}) collective-permute-start(f32[64,128]{1,0:T(8,128)S(1)} %get-tuple-element.12), channel_id=1, source_target_pairs={{0,8},{8,16},{16,24},{24,0},{1,9},{9,17},{17,25},{25,1},{2,10},{10... | collective-permute-start | bytes 98312 | tf_op jit(solution)/shard_map/ppermute | solution.py:212
  75.1 11.7 %collective-permute-start.2 = (f32[64,128]{1,0:T(8,128)S(1)}, f32[64,128]{1,0:T(8,128)S(1)}, u32[]{:S(2)}, u32[]{:S(2)}) collective-permute-start(f32[64,128]{1,0:T(8,128)S(1)} %get-tuple-element.13), channel_id=1, source_target_pairs={{0,16},{8,24},{16,0},{24,8},{1,17},{9,25},{17,1},{25,9},{2,18},{10... | collective-permute-start | bytes 98312 | tf_op jit(solution)/shard_map/ppermute | solution.py:212
  79.4 7.7 %collective-permute-start.3 = (f32[64,128]{1,0:T(8,128)S(1)}, f32[64,128]{1,0:T(8,128)S(1)}, u32[]{:S(2)}, u32[]{:S(2)}) collective-permute-start(f32[64,128]{1,0:T(8,128)S(1)} %get-tuple-element.14), channel_id=1, source_target_pairs={{0,24},{8,0},{16,8},{24,16},{1,25},{9,1},{17,9},{25,17},{2,26},{10... | collective-permute-start | bytes 98312 | tf_op jit(solution)/shard_map/ppermute | solution.py:212

commit v5 on v4

--- a/solution.py
+++ b/solution.py
@@ -40,11 +40,10 @@
         half = slice(HALF * (role % 2), HALF * (role % 2) + HALF)
         first = (q, k, v) if role < 2 else (ci, pre, post)
         first = [block[:, half] if block.shape[1] == LANES else block[...] for block in first]
-        gate, out_weight = (ag, wa) if role < 2 else (cg, wc)
-        wy_out[role, 0:16, :] = jnp.concatenate(first[:2], axis=1)
-        wy_out[role, 16:32, :] = jnp.concatenate([first[2], gate[:, half]], axis=1)
-        rows = out_weight[:, half].astype(F32)
-        wy_out[role, 32:40, :] = jnp.concatenate([rows[:8], rows[8:]], axis=1).astype(BF16)
+        gate, out_weight = (cg if role % 2 else ag), (wa if role < 2 else wc)
+        columns = first + [gate[:, :HALF], gate[:, HALF:], out_weight[:, half]]
+        for pair in range(3):
+            wy_out[role, 16 * pair : 16 * pair + 16, :] = jnp.concatenate(columns[2 * pair : 2 * pair + 2], axis=1)
 
 
 def spread_kernel(tok, gain, edge, out):
@@ -66,7 +65,7 @@
         out[peer, SLOT:, :] = gains
 
 
-def mix_kernel(t, w, taps, sink, out, gate_0, gate_1, gate_2, gate_3, n_scr, p_scr, g_scr):
+def mix_kernel(t, w, taps, sink, out, gate_own, gate_pair, n_scr, p_scr):
     y = lax.axis_index("y")
     z = lax.axis_index("z")
     gains = []
@@ -85,22 +84,17 @@
         for tp in range(TPN):
             x = t[b * TPN + tp, start : start + count, :].astype(F32)
             n_scr[at : at + count, LANES * tp : LANES * (tp + 1)] = (x * scale * gains[tp]).astype(BF16)
-    weight = jnp.concatenate(
-        [w[:, :, 16 * pair : 16 * pair + 16, :].reshape(FEATURES, LANES) for pair in range(2)], axis=1
-    )
-    p_scr[...] = nn_dot(n_scr[...], weight)
+    blocks = [w[:, :, 16 * pair : 16 * pair + 16, :].reshape(FEATURES, LANES) for pair in range(3)]
+    p_scr[...] = nn_dot(n_scr[...], jnp.concatenate(blocks[:2], axis=1))
     left = lax.broadcasted_iota(jnp.int32, (TOK, LANES), 1) < HALF
-    for b in range(YN):
-        at = WINDOW + TOK * b
-        g_scr[b] = jnp.where(left[:HALF], turned(p_scr[at : at + HALF, LANES:]), p_scr[at + HALF : at + TOK, LANES:])
-    for k, gate in enumerate((gate_0, gate_1, gate_2, gate_3)):
-        gate[...] = g_scr[lax.rem(y + k, YN)]
+    for gate, owner in ((gate_own, y), (gate_pair, y + 1 - 2 * lax.rem(y, 2))):
+        rows = pl.ds(pl.multiple_of(WINDOW + TOK * owner, WINDOW), TOK)
+        gate[...] = turned(jnp.where(left, nn_dot(n_scr[rows, :], blocks[2]), p_scr[rows, LANES:]))
 
     def send(b, mixed):
         for tp in range(TPN):
-            rows = w[2 * tp : 2 * tp + 2, :, 32:40, :].astype(F32).reshape(TPN, 8, LANES)
-            rows = jnp.stack([turned(rows.reshape(HALF, LANES)).reshape(TPN, 8, LANES), rows], axis=1)
-            out[b * TPN + tp] = jnp.where(left, mixed, rows.reshape(LANES, LANES).astype(BF16))
+            columns = w[2 * tp : 2 * tp + 2, :, 32:48, :].reshape(LANES, LANES)
+            out[b * TPN + tp] = jnp.where(left, mixed, columns)
 
     @pl.when(y < 2)
     def _():
@@ -113,17 +107,18 @@
             q = p_scr[WINDOW + TOK * b : WINDOW + TOK * (b + 1), :HALF].astype(BF16)
             k = p_scr[TOK * b : TOK * b + span, HALF:LANES].astype(BF16)
             v = p_scr[TOK * b : TOK * b + span, LANES:].astype(BF16)
-            scores = nt_dot(q, k) * (HALF**-0.5)
-            key = (z * YN + b) * TOK - WINDOW + j
-            allowed = near & (key >= 0) & (key < ZN * YN * TOK)
-            scores = jnp.where(allowed, scores, NEGATIVE)
+            allowed = near
+            if b == 0:
+                allowed = near & (j >= jnp.where(z == 0, WINDOW, 0))
+            if b == YN - 1:
+                allowed = near & (j < jnp.where(z == ZN - 1, TOK + WINDOW, span))
+            scores = jnp.where(allowed, nt_dot(q, k) * (HALF**-0.5), NEGATIVE)
             top = jnp.maximum(jnp.max(scores, axis=1, keepdims=True), logit)
             e = jnp.exp(scores - top)
             share = jnp.sum(e, axis=1, keepdims=True) + jnp.exp(logit - top)
-            e = e / share
             high = e.astype(BF16)
             low = (e - high.astype(F32)).astype(BF16)
-            send(b, (nn_dot(high, v) + nn_dot(low, v)).astype(BF16))
+            send(b, ((nn_dot(high, v) + nn_dot(low, v)) * (1.0 / share)).astype(BF16))
 
     @pl.when(y >= 2)
     def _():
@@ -143,14 +138,10 @@
     return jnp.where(left, a, turned(b)), jnp.where(left, turned(a), b)
 
 
-def gate_kernel(g_0, g_1, g_2, g_3, out, g_scr):
-    y = lax.axis_index("y")
-    for k, g in enumerate((g_0, g_1, g_2, g_3)):
-        g_scr[k] = g[...]
-    left = lax.broadcasted_iota(jnp.int32, (HALF, LANES), 1) < HALF
-    for branch in range(2):
-        parts = [g_scr[lax.rem(y + YN - source, YN)] for source in (2 * branch, 2 * branch + 1)]
-        out[branch] = jax.nn.sigmoid(jnp.concatenate(joined(*parts, left), axis=0))
+def gate_kernel(own, pair, out):
+    even = lax.rem(lax.axis_index("y"), 2) == 0
+    out[0] = jax.nn.sigmoid(jnp.where(even, own[...], pair[...]))
+    out[1] = jax.nn.sigmoid(jnp.where(even, pair[...], own[...]))
 
 
 def final_kernel(m, gates, out):
@@ -189,28 +180,23 @@
 def on_device(tok, gain, q, k, v, ci, pre, post, ag, cg, sink, taps, wa, wc):
     plane = ("y", "x", "c")
     edges = [(YN * z + YN - 1, YN * z + YN) for z in range(ZN - 1)]
+    wy = call(pack_kernel, shaped((YN, 48, LANES)), (q, k, v, ci, pre, post, ag, cg, wa.T, wc.T), limit=60)
+    wy = lax.all_to_all(wy, "y", 0, 0, tiled=True)
     edge = lax.ppermute(tok, ("z", "y"), edges + [(b, a) for a, b in edges])
-    wy = call(pack_kernel, shaped((YN, 40, LANES)), (q, k, v, ci, pre, post, ag, cg, wa.T, wc.T), limit=60)
-    wy = lax.all_to_all(wy, "y", 0, 0, tiled=True)
     spread = call(spread_kernel, shaped((PLANE, SLOT + 8, LANES)), (tok, gain.reshape(1, LANES), edge), limit=60)
     gathered_tok = lax.all_to_all(spread, plane, 0, 0, tiled=True)
-    w = lax.all_gather(wy.reshape(YN * 40, LANES), "z", axis=0, tiled=True).reshape(ZN, YN, 40, LANES)
-    message, *gates = call(
+    w = lax.all_gather(wy.reshape(YN * 48, LANES), "z", axis=0, tiled=True).reshape(ZN, YN, 48, LANES)
+    message, own, pair = call(
         mix_kernel,
-        (shaped((PLANE, TOK, LANES)),) + (shaped((HALF, LANES), F32),) * 4,
+        (shaped((PLANE, TOK, LANES)),) + (shaped((TOK, LANES), F32),) * 2,
         (gathered_tok, w, taps, sink),
         [VM] * 3 + [SM],
-        [
-            pltpu.VMEM((ROWS, FEATURES), BF16),
-            pltpu.VMEM((ROWS, 2 * LANES), F32),
-            pltpu.VMEM((YN, HALF, LANES), F32),
-        ],
+        [pltpu.VMEM((ROWS, FEATURES), BF16), pltpu.VMEM((ROWS, 2 * LANES), F32)],
         20,
     )
     message = lax.all_to_all(message, plane, 0, 0, tiled=True)
-    for k in range(1, YN):
-        gates[k] = lax.ppermute(gates[k], "y", [(y, (y + k) % YN) for y in range(YN)])
-    gates = call(gate_kernel, shaped((2, TOK, LANES), F32), gates, scratch=[pltpu.VMEM((YN, HALF, LANES), F32)])
+    pair = lax.ppermute(pair, "y", [(y, y ^ 1) for y in range(YN)])
+    gates = call(gate_kernel, shaped((2, TOK, LANES), F32), (own, pair))
     return call(final_kernel, shaped((TOK, LANES)), (message, gates))
 
 

time: 90.5 us -> 95 us (1.050)
  waiting for transfers between devices: 7.77 us -> 14.7 us
  blocking collectives: 34.6 us -> 32.8 us
    all_to_all x1, starting transfers between devices: 7.49 us -> 16.4 us  [on_device(): gathered_tok = lax.all_to_all(spread, plane, 0, 0, tiled=True)]
    ppermute x3 -> x1, starting transfers between devices: 10.7 us -> 3.26 us  [on_device(): pair = lax.ppermute(pair, 'y', [(y, y ^ 1) for y in range(YN)])]
    ppermute x3 -> x1, waiting for transfers between devices: 4.61 us -> 8.44 us  [on_device(): pair = lax.ppermute(pair, 'y', [(y, y ^ 1) for y in range(YN)])]
    all_to_all x1, waiting for transfers between devices: 1.63 us -> 5.3 us  [on_device(): message = lax.all_to_all(message, plane, 0, 0, tiled=True)]
    all_to_all x1, starting transfers between devices: 7.36 us -> 5 us  [on_device(): wy = lax.all_to_all(wy, 'y', 0, 0, tiled=True)]
    all_gather x1, blocking collectives: 34.6 us -> 32.8 us  [on_device(): lax.all_gather(wy.reshape(YN * 48, LANES), 'z', axis=0, tiled=True)]
  transfers between devices with their start and end apart: 7 -> 5, of which waited for: 5 -> 3; matrix products, arithmetic and copies ran while one was open for 0% -> 0% of each run, Pallas kernels for 4% -> 2%
where the time goes in v5:
time: 95 us; the launch traced here: 94.4 us
  starting transfers between devices  37.6 us (40%)
  blocking collectives  32.8 us (35%)
  waiting for transfers between devices  14.7 us (15%)
  Pallas kernels  8.76 us (9%)
    all_gather x1, blocking collectives, on_device(): lax.all_gather(wy.reshape(YN * 48, LANES), 'z', axis=0, tiled=True)  32.8 us
    all_to_all x1, starting transfers between devices, on_device(): gathered_tok = lax.all_to_all(spread, plane, 0, 0, tiled=True)  16.4 us
    all_to_all x1, starting transfers between devices, on_device(): message = lax.all_to_all(message, plane, 0, 0, tiled=True)  12.2 us
    pallas_call x5, Pallas kernels, call(): pl.pallas_call(kernel, out_shape=outs, in_specs=specs or [VM] * len(args)...  8.76 us
    ppermute x1, waiting for transfers between devices, on_device(): pair = lax.ppermute(pair, 'y', [(y, y ^ 1) for y in range(YN)])  8.44 us
    all_to_all x1, waiting for transfers between devices, on_device(): message = lax.all_to_all(message, plane, 0, 0, tiled=True)  5.3 us
    all_to_all x1, starting transfers between devices, on_device(): wy = lax.all_to_all(wy, 'y', 0, 0, tiled=True)  5 us
    ppermute x1, starting transfers between devices, on_device(): pair = lax.ppermute(pair, 'y', [(y, y ^ 1) for y in range(YN)])  3.26 us
  transfers between devices with their start and end apart: 5, of which 3 were waited for; matrix products, arithmetic and copies ran while one was open for 0% of the time, Pallas kernels for 2%

profile of v5, /device:TPU:1, one launch (start us, length us, event | category | flops | bytes accessed | tf_op | source)
XLA Modules:
  0.0 94.4 jit_solution(9353901599783589961)
XLA Ops:
  0.0 1.5 %shard_map.137 = bf16[4,48,128]{2,1,0:T(8,128)(2,1)} custom-call(bf16[16,128]{1,0:T(8,128)(2,1)} %q.1, bf16[16,64]{1,0:T(8,128)(2,1)} %k.1, bf16[16,64]{1,0:T(8,128)(2,1)} %v.1, bf16[16,128]{1,0:T(8,128)(2,1)} %ci.1, bf16[16,128]{1,0:T(8,128)(2,1)} %pre.1, bf16[16,128]{1,0:T(8,128)(2,1)} %post.1, bf16[16,128]{1,0:T(8,128)(2,1)} %ag.1, bf16[16,128]{1,0:T(8,128)(2,1)} %cg.1, ...), custom_call_target="tpu_custom_call" | custom-call | tf_op jit(solution)/shard_map/pallas_call | solution.py:170
  1.5 5.0 %all-to-all-start.1 = ((bf16[4,48,128]{2,1,0:T(8,128)(2,1)}), bf16[4,48,128]{2,1,0:T(8,128)(2,1)S(1)}, u32[]{:S(2)}, u32[]{:S(2)}) async-start(bf16[4,48,128]{2,1,0:T(8,128)(2,1)} %shard_map.137), calls=%async_computation.1 | async-start | bytes 98304 | tf_op jit(solution)/shard_map/all_to_all | solution.py:184
  6.5 0.7 collective-permute-start
  7.2 0.0 collective-permute-done.edge
  7.2 0.0 copy-start.2
  7.2 0.6 copy-done.2
  7.8 2.2 %shard_map.136 = bf16[32,200,128]{2,1,0:T(8,128)(2,1)} custom-call(bf16[128,128]{1,0:T(8,128)(2,1)} %tok.1, f32[1,128]{1,0:T(1,128)} %bitcast.9, bf16[128,128]{1,0:T(8,128)(2,1)} %copy-done.2), custom_call_target="tpu_custom_call" | custom-call | tf_op jit(solution)/shard_map/pallas_call | solution.py:170
  10.0 0.0 copy-start
  10.0 0.0 copy-start.1
  10.0 0.9 all-to-all-done.1
  10.9 16.4 %all-to-all-start = ((bf16[32,200,128]{2,1,0:T(8,128)(2,1)}), bf16[32,200,128]{2,1,0:T(8,128)(2,1)S(1)}, u32[]{:S(2)}, u32[]{:S(2)}) async-start(bf16[32,200,128]{2,1,0:T(8,128)(2,1)} %shard_map.136), calls=%async_computation | async-start | bytes 3276800 | tf_op jit(solution)/shard_map/all_to_all | solution.py:187
  27.4 32.8 %all_gather.3 = bf16[3072,128]{1,0:T(8,128)(2,1)S(1)} all-gather(bf16[192,128]{1,0:T(8,128)(2,1)S(1)} %bitcast.6), channel_id=1, replica_groups=mesh['z'=16,'y'=4,'x'=4,'c'=2] {'z'}, dimensions={0}, use_global_device_ids=true | all-gather | bytes 835584 | tf_op jit(solution)/shard_map/all_gather | solution.py:188
  60.2 0.0 all-to-all-done.t
  60.2 0.0 copy-done
  60.2 0.0 copy-done.1
  60.2 3.9 %shard_map.138 = (bf16[32,128,128]{2,1,0:T(8,128)(2,1)}, f32[128,128]{1,0:T(8,128)S(1)}, f32[128,128]{1,0:T(8,128)S(1)}) custom-call(bf16[32,200,128]{2,1,0:T(8,128)(2,1)S(1)} %all-to-all-done.t, bf16[16,4,48,128]{3,2,1,0:T(8,128)(2,1)S(1)} %bitcast.5, f32[3,128]{1,0:T(4,128)S(1)} %copy-done, f32[2]{0:T(128)S(1)} %copy-done.1), custom_call_target="tpu_custom_call" | custom-call | tf_op jit(solution)/shard_map/pallas_call | solution.py:170
  64.1 12.2 %all-to-all-start.2 = ((bf16[32,128,128]{2,1,0:T(8,128)(2,1)}), bf16[32,128,128]{2,1,0:T(8,128)(2,1)S(1)}, u32[]{:S(2)}, u32[]{:S(2)}) async-start(bf16[32,128,128]{2,1,0:T(8,128)(2,1)} %get-tuple-element.8), calls=%async_computation.2 | async-start | bytes 2097152 | tf_op jit(solution)/shard_map/all_to_all | solution.py:197
  76.3 3.3 %collective-permute-start.1 = (f32[128,128]{1,0:T(8,128)S(1)}, f32[128,128]{1,0:T(8,128)S(1)}, u32[]{:S(2)}, u32[]{:S(2)}) collective-permute-start(f32[128,128]{1,0:T(8,128)S(1)} %get-tuple-element.10), channel_id=1, source_target_pairs={{0,8},{8,0},{16,24},{24,16},{1,9},{9,1},{17,25},{25,17},{2,10},{10... | collective-permute-start | bytes 196616 | tf_op jit(solution)/shard_map/ppermute | solution.py:198
  79.6 8.4 %collective-permute-done.1.pair = f32[128,128]{1,0:T(8,128)S(1)} collective-permute-done((f32[128,128]{1,0:T(8,128)S(1)}, f32[128,128]{1,0:T(8,128)S(1)}, u32[]{:S(2)}, u32[]{:S(2)}) %collective-permute-start.1) | collective-permute-done | bytes 65568 | tf_op jit(solution)/shard_map/ppermute | solution.py:198
  88.0 5.3 %all-to-all-done.2.m = bf16[32,128,128]{2,1,0:T(8,128)(2,1)S(1)} async-done(((bf16[32,128,128]{2,1,0:T(8,128)(2,1)}), bf16[32,128,128]{2,1,0:T(8,128)(2,1)S(1)}, u32[]{:S(2)}, u32[]{:S(2)}) %all-to-all-start.2) | async-done | bytes 1048608 | tf_op jit(solution)/shard_map/all_to_all | solution.py:197
  93.4 1.1 %shard_map.140 = bf16[128,128]{1,0:T(8,128)(2,1)} custom-call(bf16[32,128,128]{2,1,0:T(8,128)(2,1)S(1)} %all-to-all-done.2.m, f32[2,128,128]{2,1,0:T(8,128)S(1)} %shard_map.139.gates), custom_call_target="tpu_custom_call" | custom-call | tf_op jit(solution)/shard_map/pallas_call | solution.py:170
  (1 shorter events, 0.0 us)
Async XLA Ops:
  1.5 9.4 %all-to-all-start.1 = ((bf16[4,48,128]{2,1,0:T(8,128)(2,1)}), bf16[4,48,128]{2,1,0:T(8,128)(2,1)S(1)}, u32[]{:S(2)}, u32[]{:S(2)}) async-start(bf16[4,48,128]{2,1,0:T(8,128)(2,1)} %shard_map.137), calls=%async_computation.1 | async-start | bytes 98304 | tf_op jit(solution)/shard_map/all_to_all | solution.py:184
  6.5 0.7 collective-permute-start
  7.2 0.6 copy-start.2
  10.0 50.2 %copy-start = (f32[3,128]{1,0:T(4,128)S(1)}, f32[3,128]{1,0:T(4,128)}, u32[]{:S(2)}) copy-start(f32[3,128]{1,0:T(4,128)} %taps.1) | copy-start | bytes 4612
  10.0 50.2 %copy-start.1 = (f32[2]{0:T(128)S(1)}, f32[2]{0:T(128)}, u32[]{:S(2)}) copy-start(f32[2]{0:T(128)} %sink.1) | copy-start | bytes 28
  10.9 49.2 %all-to-all-start = ((bf16[32,200,128]{2,1,0:T(8,128)(2,1)}), bf16[32,200,128]{2,1,0:T(8,128)(2,1)S(1)}, u32[]{:S(2)}, u32[]{:S(2)}) async-start(bf16[32,200,128]{2,1,0:T(8,128)(2,1)} %shard_map.136), calls=%async_computation | async-start | bytes 3276800 | tf_op jit(solution)/shard_map/all_to_all | solution.py:187
  64.1 29.3 %all-to-all-start.2 = ((bf16[32,128,128]{2,1,0:T(8,128)(2,1)}), bf16[32,128,128]{2,1,0:T(8,128)(2,1)S(1)}, u32[]{:S(2)}, u32[]{:S(2)}) async-start(bf16[32,128,128]{2,1,0:T(8,128)(2,1)} %get-tuple-element.8), calls=%async_computation.2 | async-start | bytes 2097152 | tf_op jit(solution)/shard_map/all_to_all | solution.py:197
  76.3 11.7 %collective-permute-start.1 = (f32[128,128]{1,0:T(8,128)S(1)}, f32[128,128]{1,0:T(8,128)S(1)}, u32[]{:S(2)}, u32[]{:S(2)}) collective-permute-start(f32[128,128]{1,0:T(8,128)S(1)} %get-tuple-element.10), channel_id=1, source_target_pairs={{0,8},{8,0},{16,24},{24,16},{1,9},{9,1},{17,25},{25,17},{2,10},{10... | collective-permute-start | bytes 196616 | tf_op jit(solution)/shard_map/ppermute | solution.py:198

commit v6 on v4

--- a/solution.py
+++ b/solution.py
@@ -66,7 +66,7 @@
         out[peer, SLOT:, :] = gains
 
 
-def mix_kernel(t, w, taps, sink, out, gate_0, gate_1, gate_2, gate_3, n_scr, p_scr, g_scr):
+def mix_kernel(t, w, taps, sink, out, gate_0, gate_1, gate_2, gate_3, n_scr, p_scr, g_scr, w_scr, m_scr, sems):
     y = lax.axis_index("y")
     z = lax.axis_index("z")
     gains = []
@@ -96,15 +96,24 @@
     for k, gate in enumerate((gate_0, gate_1, gate_2, gate_3)):
         gate[...] = g_scr[lax.rem(y + k, YN)]
 
+    for tp in range(TPN):
+        rows = w[2 * tp : 2 * tp + 2, :, 32:40, :].astype(F32).reshape(TPN, 8, LANES)
+        rows = jnp.stack([turned(rows.reshape(HALF, LANES)).reshape(TPN, 8, LANES), rows], axis=1)
+        w_scr[tp] = rows.reshape(LANES, LANES).astype(BF16)
+
+    def outgoing(b):
+        part = pl.ds(b * TPN, TPN)
+        return pltpu.make_async_copy(m_scr.at[part], out.at[part], sems.at[b])
+
     def send(b, mixed):
         for tp in range(TPN):
-            rows = w[2 * tp : 2 * tp + 2, :, 32:40, :].astype(F32).reshape(TPN, 8, LANES)
-            rows = jnp.stack([turned(rows.reshape(HALF, LANES)).reshape(TPN, 8, LANES), rows], axis=1)
-            out[b * TPN + tp] = jnp.where(left, mixed, rows.reshape(LANES, LANES).astype(BF16))
+            m_scr[b * TPN + tp] = jnp.where(left, mixed, w_scr[tp])
+        outgoing(b).start()
 
     @pl.when(y < 2)
     def _():
-        logit = jnp.where(y == 0, sink[0], sink[1])
+        lane = lax.broadcasted_iota(jnp.int32, (1, 2), 1)
+        logit = jnp.sum(jnp.where(lane == y, sink[...], 0.0), axis=1, keepdims=True)
         span = TOK + 2 * WINDOW
         i = lax.broadcasted_iota(jnp.int32, (TOK, span), 0)
         j = lax.broadcasted_iota(jnp.int32, (TOK, span), 1)
@@ -114,16 +123,18 @@
             k = p_scr[TOK * b : TOK * b + span, HALF:LANES].astype(BF16)
             v = p_scr[TOK * b : TOK * b + span, LANES:].astype(BF16)
             scores = nt_dot(q, k) * (HALF**-0.5)
-            key = (z * YN + b) * TOK - WINDOW + j
-            allowed = near & (key >= 0) & (key < ZN * YN * TOK)
+            allowed = near
+            if b == 0:
+                allowed = near & (j >= jnp.where(z == 0, WINDOW, 0))
+            if b == YN - 1:
+                allowed = near & (j < jnp.where(z == ZN - 1, TOK + WINDOW, span))
             scores = jnp.where(allowed, scores, NEGATIVE)
             top = jnp.maximum(jnp.max(scores, axis=1, keepdims=True), logit)
             e = jnp.exp(scores - top)
             share = jnp.sum(e, axis=1, keepdims=True) + jnp.exp(logit - top)
-            e = e / share
             high = e.astype(BF16)
             low = (e - high.astype(F32)).astype(BF16)
-            send(b, (nn_dot(high, v) + nn_dot(low, v)).astype(BF16))
+            send(b, ((nn_dot(high, v) + nn_dot(low, v)) * (1.0 / share)).astype(BF16))
 
     @pl.when(y >= 2)
     def _():
@@ -138,6 +149,9 @@
             post = p_scr[at : at + TOK, LANES:].astype(BF16).astype(F32)
             send(b, (post * (t3[0:1] * before + t3[1:2] * here + t3[2:3] * after)).astype(BF16))
 
+    for b in range(YN):
+        outgoing(b).wait()
+
 
 def joined(a, b, left):
     return jnp.where(left, a, turned(b)), jnp.where(left, turned(a), b)
@@ -168,19 +182,21 @@
 
 
 VM = pl.BlockSpec(memory_space=pltpu.VMEM)
-SM = pl.BlockSpec(memory_space=pltpu.SMEM)
 
 
 def shaped(shape, kind=BF16):
     return jax.ShapeDtypeStruct(shape, kind)
 
 
-def call(kernel, outs, args, specs=None, scratch=(), limit=8):
+def call(kernel, outs, args, specs=None, scratch=(), limit=8, first=None):
+    out_specs = jax.tree.map(lambda _: VM, outs)
+    if first is not None:
+        out_specs = (first,) + out_specs[1:]
     return pl.pallas_call(
         kernel,
         out_shape=outs,
         in_specs=specs or [VM] * len(args),
-        out_specs=jax.tree.map(lambda _: VM, outs),
+        out_specs=out_specs,
         scratch_shapes=list(scratch),
         compiler_params=pltpu.CompilerParams(vmem_limit_bytes=limit * 2**20),
     )(*args)
@@ -198,14 +214,18 @@
     message, *gates = call(
         mix_kernel,
         (shaped((PLANE, TOK, LANES)),) + (shaped((HALF, LANES), F32),) * 4,
-        (gathered_tok, w, taps, sink),
-        [VM] * 3 + [SM],
+        (gathered_tok, w, taps, sink.reshape(1, 2)),
+        [VM] * 4,
         [
             pltpu.VMEM((ROWS, FEATURES), BF16),
             pltpu.VMEM((ROWS, 2 * LANES), F32),
             pltpu.VMEM((YN, HALF, LANES), F32),
+            pltpu.VMEM((TPN, LANES, LANES), BF16),
+            pltpu.VMEM((PLANE, TOK, LANES), BF16),
+            pltpu.SemaphoreType.DMA((YN,)),
         ],
         20,
+        first=pl.BlockSpec(memory_space=pl.ANY),
     )
     message = lax.all_to_all(message, plane, 0, 0, tiled=True)
     for k in range(1, YN):

time: 90.5 us -> 89.7 us (level)
  Pallas kernels: 8.87 us -> 7.95 us
    pallas_call x5, Pallas kernels: 8.87 us -> 7.95 us  [call(): pl.pallas_call(kernel, out_shape=outs, in_specs=specs or [VM] * len(args)...]
where the time goes in v6:
time: 89.7 us; the launch traced here: 89.1 us
  starting transfers between devices  38.1 us (42%)
  blocking collectives  34.6 us (39%)
  Pallas kernels  7.95 us (9%)
  waiting for transfers between devices  7.77 us (9%)
    all_gather x1, blocking collectives, on_device(): lax.all_gather(wy.reshape(YN * 40, LANES), 'z', axis=0, tiled=True)  34.6 us
    all_to_all x1, starting transfers between devices, on_device(): message = lax.all_to_all(message, plane, 0, 0, tiled=True)  11.9 us
    ppermute x3, starting transfers between devices, on_device(): lax.ppermute(gates[k], 'y', [(y, (y + k) % YN) for y in range(YN)])  10.7 us
    pallas_call x5, Pallas kernels, call(): pl.pallas_call(kernel, out_shape=outs, in_specs=specs or [VM] * len(args)...  7.95 us
    all_to_all x1, starting transfers between devices, on_device(): gathered_tok = lax.all_to_all(spread, plane, 0, 0, tiled=True)  7.49 us
    all_to_all x1, starting transfers between devices, on_device(): wy = lax.all_to_all(wy, 'y', 0, 0, tiled=True)  7.36 us
    ppermute x3, waiting for transfers between devices, on_device(): lax.ppermute(gates[k], 'y', [(y, (y + k) % YN) for y in range(YN)])  4.61 us
  transfers between devices with their start and end apart: 7, of which 5 were waited for; matrix products, arithmetic and copies ran while one was open for 0% of the time, Pallas kernels for 4%

profile of v6, /device:TPU:1, one launch (start us, length us, event | category | flops | bytes accessed | tf_op | source)
XLA Modules:
  0.0 89.1 jit_solution(8246942935634565183)
XLA Ops:
  0.0 0.7 collective-permute-start
  0.7 1.5 %shard_map.137 = bf16[4,40,128]{2,1,0:T(8,128)(2,1)} custom-call(bf16[16,128]{1,0:T(8,128)(2,1)} %q.1, bf16[16,64]{1,0:T(8,128)(2,1)} %k.1, bf16[16,64]{1,0:T(8,128)(2,1)} %v.1, bf16[16,128]{1,0:T(8,128)(2,1)} %ci.1, bf16[16,128]{1,0:T(8,128)(2,1)} %pre.1, bf16[16,128]{1,0:T(8,128)(2,1)} %post.1, bf16[16,128]{1,0:T(8,128)(2,1)} %ag.1, bf16[16,128]{1,0:T(8,128)(2,1)} %cg.1, ...), custom_call_target="tpu_custom_call" | custom-call | tf_op jit(solution)/shard_map/pallas_call | solution.py:195
  2.2 7.4 %all-to-all-start.1 = ((bf16[4,40,128]{2,1,0:T(8,128)(2,1)}), bf16[4,40,128]{2,1,0:T(8,128)(2,1)S(1)}, u32[]{:S(2)}, u32[]{:S(2)}) async-start(bf16[4,40,128]{2,1,0:T(8,128)(2,1)} %shard_map.137), calls=%async_computation.1 | async-start | bytes 81920 | tf_op jit(solution)/shard_map/all_to_all | solution.py:210
  9.5 0.0 collective-permute-done.edge
  9.5 0.0 copy-start.2
  9.5 0.6 copy-done.2
  10.2 2.2 %shard_map.136 = bf16[32,200,128]{2,1,0:T(8,128)(2,1)} custom-call(bf16[128,128]{1,0:T(8,128)(2,1)} %tok.1, f32[1,128]{1,0:T(1,128)} %bitcast.11, bf16[128,128]{1,0:T(8,128)(2,1)} %copy-done.2), custom_call_target="tpu_custom_call" | custom-call | tf_op jit(solution)/shard_map/pallas_call | solution.py:195
  12.4 0.0 copy-start
  12.4 0.0 copy-start.1
  12.4 1.5 %all-to-all-done.1 = bf16[4,40,128]{2,1,0:T(8,128)(2,1)S(1)} async-done(((bf16[4,40,128]{2,1,0:T(8,128)(2,1)}), bf16[4,40,128]{2,1,0:T(8,128)(2,1)S(1)}, u32[]{:S(2)}, u32[]{:S(2)}) %all-to-all-start.1) | async-done | bytes 40992 | tf_op jit(solution)/shard_map/all_to_all | solution.py:210
  13.9 7.5 %all-to-all-start = ((bf16[32,200,128]{2,1,0:T(8,128)(2,1)}), bf16[32,200,128]{2,1,0:T(8,128)(2,1)S(1)}, u32[]{:S(2)}, u32[]{:S(2)}) async-start(bf16[32,200,128]{2,1,0:T(8,128)(2,1)} %shard_map.136), calls=%async_computation | async-start | bytes 3276800 | tf_op jit(solution)/shard_map/all_to_all | solution.py:212
  21.4 34.6 %all_gather.3 = bf16[2560,128]{1,0:T(8,128)(2,1)S(1)} all-gather(bf16[160,128]{1,0:T(8,128)(2,1)S(1)} %bitcast.8), channel_id=1, replica_groups=mesh['z'=16,'y'=4,'x'=4,'c'=2] {'z'}, dimensions={0}, use_global_device_ids=true | all-gather | bytes 696320 | tf_op jit(solution)/shard_map/all_gather | solution.py:213
  56.0 0.0 all-to-all-done.t
  56.0 0.0 copy-done
  56.0 0.0 copy-done.1
  56.0 3.0 %shard_map.138 = (bf16[32,128,128]{2,1,0:T(8,128)(2,1)}, f32[64,128]{1,0:T(8,128)S(1)}, f32[64,128]{1,0:T(8,128)S(1)}, f32[64,128]{1,0:T(8,128)S(1)}, f32[64,128]{1,0:T(8,128)S(1)}) custom-call(bf16[32,200,128]{2,1,0:T(8,128)(2,1)S(1)} %all-to-all-done.t, bf16[16,4,40,128]{3,2,1,0:T(8,128)(2,1)S(1)} %bitcast.6, f32[3,128]{1,0:T(4,128)S(1)} %copy-done, ...), custom_call_target="tpu_custom_call" | custom-call | tf_op jit(solution)/shard_map/pallas_call | solution.py:195
  59.0 11.9 %all-to-all-start.2 = ((bf16[32,128,128]{2,1,0:T(8,128)(2,1)}), bf16[32,128,128]{2,1,0:T(8,128)(2,1)S(1)}, u32[]{:S(2)}, u32[]{:S(2)}) async-start(bf16[32,128,128]{2,1,0:T(8,128)(2,1)} %get-tuple-element.10), calls=%async_computation.2 | async-start | bytes 2097152 | tf_op jit(solution)/shard_map/all_to_all | solution.py:230
  71.0 3.3 %collective-permute-start.1 = (f32[64,128]{1,0:T(8,128)S(1)}, f32[64,128]{1,0:T(8,128)S(1)}, u32[]{:S(2)}, u32[]{:S(2)}) collective-permute-start(f32[64,128]{1,0:T(8,128)S(1)} %get-tuple-element.12), channel_id=1, source_target_pairs={{0,8},{8,16},{16,24},{24,0},{1,9},{9,17},{17,25},{25,1},{2,10},{10... | collective-permute-start | bytes 98312 | tf_op jit(solution)/shard_map/ppermute | solution.py:232
  74.2 4.3 %collective-permute-start.2 = (f32[64,128]{1,0:T(8,128)S(1)}, f32[64,128]{1,0:T(8,128)S(1)}, u32[]{:S(2)}, u32[]{:S(2)}) collective-permute-start(f32[64,128]{1,0:T(8,128)S(1)} %get-tuple-element.13), channel_id=1, source_target_pairs={{0,16},{8,24},{16,0},{24,8},{1,17},{9,25},{17,1},{25,9},{2,18},{10... | collective-permute-start | bytes 98312 | tf_op jit(solution)/shard_map/ppermute | solution.py:232
  78.6 3.0 %collective-permute-start.3 = (f32[64,128]{1,0:T(8,128)S(1)}, f32[64,128]{1,0:T(8,128)S(1)}, u32[]{:S(2)}, u32[]{:S(2)}) collective-permute-start(f32[64,128]{1,0:T(8,128)S(1)} %get-tuple-element.14), channel_id=1, source_target_pairs={{0,24},{8,0},{16,8},{24,16},{1,25},{9,1},{17,9},{25,17},{2,26},{10... | collective-permute-start | bytes 98312 | tf_op jit(solution)/shard_map/ppermute | solution.py:232
  81.6 0.7 collective-permute-done.1.g_1
  82.4 3.6 %collective-permute-done.2.g_2 = f32[64,128]{1,0:T(8,128)S(1)} collective-permute-done((f32[64,128]{1,0:T(8,128)S(1)}, f32[64,128]{1,0:T(8,128)S(1)}, u32[]{:S(2)}, u32[]{:S(2)}) %collective-permute-start.2) | collective-permute-done | bytes 32800 | tf_op jit(solution)/shard_map/ppermute | solution.py:232
  85.9 0.3 collective-permute-done.3.g_3
  86.3 0.1 shard_map.139.gates
  86.4 1.6 %all-to-all-done.2.m = bf16[32,128,128]{2,1,0:T(8,128)(2,1)S(1)} async-done(((bf16[32,128,128]{2,1,0:T(8,128)(2,1)}), bf16[32,128,128]{2,1,0:T(8,128)(2,1)S(1)}, u32[]{:S(2)}, u32[]{:S(2)}) %all-to-all-start.2) | async-done | bytes 1048608 | tf_op jit(solution)/shard_map/all_to_all | solution.py:230
  88.0 1.1 %shard_map.140 = bf16[128,128]{1,0:T(8,128)(2,1)} custom-call(bf16[32,128,128]{2,1,0:T(8,128)(2,1)S(1)} %all-to-all-done.2.m, f32[2,128,128]{2,1,0:T(8,128)S(1)} %shard_map.139.gates), custom_call_target="tpu_custom_call" | custom-call | tf_op jit(solution)/shard_map/pallas_call | solution.py:195
Async XLA Ops:
  0.0 9.5 %collective-permute-start = (bf16[128,128]{1,0:T(8,128)(2,1)}, bf16[128,128]{1,0:T(8,128)(2,1)S(1)}, u32[]{:S(2)}, u32[]{:S(2)}) collective-permute-start(bf16[128,128]{1,0:T(8,128)(2,1)} %tok.1), channel_id=1, source_target_pairs={{24,32},{56,64},{88,96},{120,128},{152,160},{184,192},{216,224},{2... | collective-permute-start | bytes 98312 | tf_op jit(solution)/shard_map/ppermute | solution.py:208
  2.2 11.7 %all-to-all-start.1 = ((bf16[4,40,128]{2,1,0:T(8,128)(2,1)}), bf16[4,40,128]{2,1,0:T(8,128)(2,1)S(1)}, u32[]{:S(2)}, u32[]{:S(2)}) async-start(bf16[4,40,128]{2,1,0:T(8,128)(2,1)} %shard_map.137), calls=%async_computation.1 | async-start | bytes 81920 | tf_op jit(solution)/shard_map/all_to_all | solution.py:210
  9.5 0.6 copy-start.2
  12.4 43.6 %copy-start = (f32[3,128]{1,0:T(4,128)S(1)}, f32[3,128]{1,0:T(4,128)}, u32[]{:S(2)}) copy-start(f32[3,128]{1,0:T(4,128)} %taps.1) | copy-start | bytes 4612
  12.4 43.6 %copy-start.1 = (f32[2]{0:T(128)S(1)}, f32[2]{0:T(128)}, u32[]{:S(2)}) copy-start(f32[2]{0:T(128)} %param.24) | copy-start | bytes 28
  13.9 42.1 %all-to-all-start = ((bf16[32,200,128]{2,1,0:T(8,128)(2,1)}), bf16[32,200,128]{2,1,0:T(8,128)(2,1)S(1)}, u32[]{:S(2)}, u32[]{:S(2)}) async-start(bf16[32,200,128]{2,1,0:T(8,128)(2,1)} %shard_map.136), calls=%async_computation | async-start | bytes 3276800 | tf_op jit(solution)/shard_map/all_to_all | solution.py:212
  59.0 29.0 %all-to-all-start.2 = ((bf16[32,128,128]{2,1,0:T(8,128)(2,1)}), bf16[32,128,128]{2,1,0:T(8,128)(2,1)S(1)}, u32[]{:S(2)}, u32[]{:S(2)}) async-start(bf16[32,128,128]{2,1,0:T(8,128)(2,1)} %get-tuple-element.10), calls=%async_computation.2 | async-start | bytes 2097152 | tf_op jit(solution)/shard_map/all_to_all | solution.py:230
  71.0 11.4 %collective-permute-start.1 = (f32[64,128]{1,0:T(8,128)S(1)}, f32[64,128]{1,0:T(8,128)S(1)}, u32[]{:S(2)}, u32[]{:S(2)}) collective-permute-start(f32[64,128]{1,0:T(8,128)S(1)} %get-tuple-element.12), channel_id=1, source_target_pairs={{0,8},{8,16},{16,24},{24,0},{1,9},{9,17},{17,25},{25,1},{2,10},{10... | collective-permute-start | bytes 98312 | tf_op jit(solution)/shard_map/ppermute | solution.py:232
  74.2 11.7 %collective-permute-start.2 = (f32[64,128]{1,0:T(8,128)S(1)}, f32[64,128]{1,0:T(8,128)S(1)}, u32[]{:S(2)}, u32[]{:S(2)}) collective-permute-start(f32[64,128]{1,0:T(8,128)S(1)} %get-tuple-element.13), channel_id=1, source_target_pairs={{0,16},{8,24},{16,0},{24,8},{1,17},{9,25},{17,1},{25,9},{2,18},{10... | collective-permute-start | bytes 98312 | tf_op jit(solution)/shard_map/ppermute | solution.py:232
  78.6 7.7 %collective-permute-start.3 = (f32[64,128]{1,0:T(8,128)S(1)}, f32[64,128]{1,0:T(8,128)S(1)}, u32[]{:S(2)}, u32[]{:S(2)}) collective-permute-start(f32[64,128]{1,0:T(8,128)S(1)} %get-tuple-element.14), channel_id=1, source_target_pairs={{0,24},{8,0},{16,8},{24,16},{1,25},{9,1},{17,9},{25,17},{2,26},{10... | collective-permute-start | bytes 98312 | tf_op jit(solution)/shard_map/ppermute | solution.py:232

commit v7 on v5

--- a/solution.py
+++ b/solution.py
@@ -65,7 +65,7 @@
         out[peer, SLOT:, :] = gains
 
 
-def mix_kernel(t, w, taps, sink, out, gate_own, gate_pair, n_scr, p_scr):
+def mix_kernel(t, w, taps, sink, keep, give, gate_own, gate_pair, n_scr, p_scr, m_scr):
     y = lax.axis_index("y")
     z = lax.axis_index("z")
     gains = []
@@ -92,32 +92,32 @@
         gate[...] = turned(jnp.where(left, nn_dot(n_scr[rows, :], blocks[2]), p_scr[rows, LANES:]))
 
     def send(b, mixed):
-        for tp in range(TPN):
-            columns = w[2 * tp : 2 * tp + 2, :, 32:48, :].reshape(LANES, LANES)
-            out[b * TPN + tp] = jnp.where(left, mixed, columns)
+        m_scr[TOK * b : TOK * (b + 1), :] = jnp.where(left, jnp.zeros_like(mixed), turned(mixed))
 
     @pl.when(y < 2)
     def _():
-        logit = jnp.where(y == 0, sink[0], sink[1])
+        lane = lax.broadcasted_iota(jnp.int32, (1, 2), 1)
+        logit = jnp.sum(jnp.where(lane == y, sink[...], 0.0), axis=1, keepdims=True)
         span = TOK + 2 * WINDOW
         i = lax.broadcasted_iota(jnp.int32, (TOK, span), 0)
         j = lax.broadcasted_iota(jnp.int32, (TOK, span), 1)
         near = jnp.abs(i + WINDOW - j) <= WINDOW
+        edge_low, edge_high = jnp.where(z == 0, WINDOW, 0), jnp.where(z == ZN - 1, TOK + WINDOW, span)
+        masks = [near & (j >= edge_low)] + [near] * (YN - 2) + [near & (j < edge_high)]
+        scores, tops, weights = [], [], []
         for b in range(YN):
             q = p_scr[WINDOW + TOK * b : WINDOW + TOK * (b + 1), :HALF].astype(BF16)
             k = p_scr[TOK * b : TOK * b + span, HALF:LANES].astype(BF16)
+            scores.append(jnp.where(masks[b], nt_dot(q, k) * (HALF**-0.5), NEGATIVE))
+        for b in range(YN):
+            tops.append(jnp.maximum(jnp.max(scores[b], axis=1, keepdims=True), logit))
+        for b in range(YN):
+            weights.append(jnp.exp(scores[b] - tops[b]))
+        for b in range(YN):
             v = p_scr[TOK * b : TOK * b + span, LANES:].astype(BF16)
-            allowed = near
-            if b == 0:
-                allowed = near & (j >= jnp.where(z == 0, WINDOW, 0))
-            if b == YN - 1:
-                allowed = near & (j < jnp.where(z == ZN - 1, TOK + WINDOW, span))
-            scores = jnp.where(allowed, nt_dot(q, k) * (HALF**-0.5), NEGATIVE)
-            top = jnp.maximum(jnp.max(scores, axis=1, keepdims=True), logit)
-            e = jnp.exp(scores - top)
-            share = jnp.sum(e, axis=1, keepdims=True) + jnp.exp(logit - top)
-            high = e.astype(BF16)
-            low = (e - high.astype(F32)).astype(BF16)
+            share = jnp.sum(weights[b], axis=1, keepdims=True) + jnp.exp(logit - tops[b])
+            high = weights[b].astype(BF16)
+            low = (weights[b] - high.astype(F32)).astype(BF16)
             send(b, ((nn_dot(high, v) + nn_dot(low, v)) * (1.0 / share)).astype(BF16))
 
     @pl.when(y >= 2)
@@ -133,9 +133,18 @@
             post = p_scr[at : at + TOK, LANES:].astype(BF16).astype(F32)
             send(b, (post * (t3[0:1] * before + t3[1:2] * here + t3[2:3] * after)).astype(BF16))
 
-
-def joined(a, b, left):
-    return jnp.where(left, a, turned(b)), jnp.where(left, turned(a), b)
+    first_core = lax.axis_index("c") == 0
+    for b in range(YN):
+        sums = nt_dot(m_scr[TOK * b : TOK * (b + 1), :], blocks[2])
+        for x in range(XN):
+            even = sums[:, 2 * LANES * x : 2 * LANES * x + LANES]
+            odd = sums[:, 2 * LANES * x + LANES : 2 * LANES * (x + 1)]
+            keep[XN * b + x] = jnp.where(first_core, even, odd)
+            give[XN * b + x] = jnp.where(first_core, odd, even).astype(BF16)
+
+
+def add_kernel(keep, came, out):
+    out[...] = (keep[...] + came[...].astype(F32)).astype(BF16)
 
 
 def gate_kernel(own, pair, out):
@@ -145,33 +154,31 @@
 
 
 def final_kernel(m, gates, out):
-    left = lax.broadcasted_iota(jnp.int32, (TOK, LANES), 1) < HALF
     total = jnp.zeros((TOK, LANES), F32)
     for branch in range(2):
-        mixed, columns = [], []
-        for tp in range(TPN):
-            both = joined(m[(2 * branch) * TPN + tp], m[(2 * branch + 1) * TPN + tp], left)
-            mixed.append(both[0])
-            columns.append(both[1])
-        value = nt_dot(jnp.concatenate(mixed, axis=1), jnp.concatenate(columns, axis=1))
+        value = m[2 * XN * branch].astype(F32)
+        for source in range(2 * XN * branch + 1, 2 * XN * (branch + 1)):
+            value = value + m[source].astype(F32)
         total = total + gates[branch] * value
     out[...] = total.astype(BF16)
 
 
 VM = pl.BlockSpec(memory_space=pltpu.VMEM)
-SM = pl.BlockSpec(memory_space=pltpu.SMEM)
 
 
 def shaped(shape, kind=BF16):
     return jax.ShapeDtypeStruct(shape, kind)
 
 
-def call(kernel, outs, args, specs=None, scratch=(), limit=8):
+def call(kernel, outs, args, specs=None, scratch=(), limit=8, first=None):
+    out_specs = jax.tree.map(lambda _: VM, outs)
+    if first is not None:
+        out_specs = (first,) + out_specs[1:]
     return pl.pallas_call(
         kernel,
         out_shape=outs,
         in_specs=specs or [VM] * len(args),
-        out_specs=jax.tree.map(lambda _: VM, outs),
+        out_specs=out_specs,
         scratch_shapes=list(scratch),
         compiler_params=pltpu.CompilerParams(vmem_limit_bytes=limit * 2**20),
     )(*args)
@@ -180,21 +187,27 @@
 def on_device(tok, gain, q, k, v, ci, pre, post, ag, cg, sink, taps, wa, wc):
     plane = ("y", "x", "c")
     edges = [(YN * z + YN - 1, YN * z + YN) for z in range(ZN - 1)]
+    edge = lax.ppermute(tok, ("z", "y"), edges + [(b, a) for a, b in edges])
     wy = call(pack_kernel, shaped((YN, 48, LANES)), (q, k, v, ci, pre, post, ag, cg, wa.T, wc.T), limit=60)
     wy = lax.all_to_all(wy, "y", 0, 0, tiled=True)
-    edge = lax.ppermute(tok, ("z", "y"), edges + [(b, a) for a, b in edges])
     spread = call(spread_kernel, shaped((PLANE, SLOT + 8, LANES)), (tok, gain.reshape(1, LANES), edge), limit=60)
     gathered_tok = lax.all_to_all(spread, plane, 0, 0, tiled=True)
     w = lax.all_gather(wy.reshape(YN * 48, LANES), "z", axis=0, tiled=True).reshape(ZN, YN, 48, LANES)
-    message, own, pair = call(
+    sums = (YN * XN, TOK, LANES)
+    keep, give, own, pair = call(
         mix_kernel,
-        (shaped((PLANE, TOK, LANES)),) + (shaped((TOK, LANES), F32),) * 2,
-        (gathered_tok, w, taps, sink),
-        [VM] * 3 + [SM],
-        [pltpu.VMEM((ROWS, FEATURES), BF16), pltpu.VMEM((ROWS, 2 * LANES), F32)],
-        20,
+        (shaped(sums, F32), shaped(sums)) + (shaped((TOK, LANES), F32),) * 2,
+        (gathered_tok, w, taps, sink.reshape(1, 2)),
+        scratch=[
+            pltpu.VMEM((ROWS, FEATURES), BF16),
+            pltpu.VMEM((ROWS, 2 * LANES), F32),
+            pltpu.VMEM((YN * TOK, LANES), BF16),
+        ],
+        limit=20,
     )
-    message = lax.all_to_all(message, plane, 0, 0, tiled=True)
+    came = lax.ppermute(give, "c", [(0, 1), (1, 0)])
+    message = call(add_kernel, shaped(sums), (keep, came))
+    message = lax.all_to_all(message, ("y", "x"), 0, 0, tiled=True)
     pair = lax.ppermute(pair, "y", [(y, y ^ 1) for y in range(YN)])
     gates = call(gate_kernel, shaped((2, TOK, LANES), F32), (own, pair))
     return call(final_kernel, shaped((TOK, LANES)), (message, gates))

time: 95 us -> 91.2 us (0.960)
  waiting for transfers between devices: 14.7 us -> 9.83 us
  starting transfers between devices: 37.6 us -> 39.5 us
  Pallas kernels: 8.76 us -> 7.76 us
    ppermute x0 -> x1, starting transfers between devices: none -> 7.88 us  [on_device(): came = lax.ppermute(give, 'c', [(0, 1), (1, 0)])]
    all_to_all x1, starting transfers between devices: 12.2 us -> 6.27 us  [on_device(): message = lax.all_to_all(message, ('y', 'x'), 0, 0, tiled=True)]
    all_to_all x1, waiting for transfers between devices: 5.3 us -> 1.26 us  [on_device(): message = lax.all_to_all(message, ('y', 'x'), 0, 0, tiled=True)]
    ppermute x1, waiting for transfers between devices: 8.44 us -> 6.15 us  [on_device(): pair = lax.ppermute(pair, 'y', [(y, y ^ 1) for y in range(YN)])]
    ppermute x0 -> x1, waiting for transfers between devices: none -> 1.51 us  [on_device(): came = lax.ppermute(give, 'c', [(0, 1), (1, 0)])]
    pallas_call x5 -> x6, Pallas kernels: 8.76 us -> 7.76 us  [call(): pl.pallas_call(kernel, out_shape=outs, in_specs=specs or [VM] * len(args)...]
  transfers between devices with their start and end apart: 5 -> 6, of which waited for: 3 -> 4; matrix products, arithmetic and copies ran while one was open for 0% -> 0% of each run, Pallas kernels for 2% -> 2%
where the time goes in v7:
time: 91.2 us; the launch traced here: 90.6 us
  starting transfers between devices  39.5 us (43%)
  blocking collectives  32.8 us (36%)
  waiting for transfers between devices  9.83 us (11%)
  Pallas kernels  7.76 us (9%)
    all_gather x1, blocking collectives, on_device(): lax.all_gather(wy.reshape(YN * 48, LANES), 'z', axis=0, tiled=True)  32.8 us
    all_to_all x1, starting transfers between devices, on_device(): gathered_tok = lax.all_to_all(spread, plane, 0, 0, tiled=True)  16.5 us
    ppermute x1, starting transfers between devices, on_device(): came = lax.ppermute(give, 'c', [(0, 1), (1, 0)])  7.88 us
    pallas_call x6, Pallas kernels, call(): pl.pallas_call(kernel, out_shape=outs, in_specs=specs or [VM] * len(args)...  7.76 us
    all_to_all x1, starting transfers between devices, on_device(): message = lax.all_to_all(message, ('y', 'x'), 0, 0, tiled=True)  6.27 us
    ppermute x1, waiting for transfers between devices, on_device(): pair = lax.ppermute(pair, 'y', [(y, y ^ 1) for y in range(YN)])  6.15 us
    all_to_all x1, starting transfers between devices, on_device(): wy = lax.all_to_all(wy, 'y', 0, 0, tiled=True)  5 us
    ppermute x1, starting transfers between devices, on_device(): pair = lax.ppermute(pair, 'y', [(y, y ^ 1) for y in range(YN)])  3.26 us
  transfers between devices with their start and end apart: 6, of which 4 were waited for; matrix products, arithmetic and copies ran while one was open for 0% of the time, Pallas kernels for 2%

profile of v7, /device:TPU:1, one launch (start us, length us, event | category | flops | bytes accessed | tf_op | source)
XLA Modules:
  0.0 90.6 jit_solution(10279323893953143076)
XLA Ops:
  0.0 1.5 %shard_map.137 = bf16[4,48,128]{2,1,0:T(8,128)(2,1)} custom-call(bf16[16,128]{1,0:T(8,128)(2,1)} %q.1, bf16[16,64]{1,0:T(8,128)(2,1)} %k.1, bf16[16,64]{1,0:T(8,128)(2,1)} %v.1, bf16[16,128]{1,0:T(8,128)(2,1)} %ci.1, bf16[16,128]{1,0:T(8,128)(2,1)} %pre.1, bf16[16,128]{1,0:T(8,128)(2,1)} %post.1, bf16[16,128]{1,0:T(8,128)(2,1)} %ag.1, bf16[16,128]{1,0:T(8,128)(2,1)} %cg.1, ...), custom_call_target="tpu_custom_call" | custom-call | tf_op jit(solution)/shard_map/pallas_call | solution.py:177
  1.5 5.0 %all-to-all-start.1 = ((bf16[4,48,128]{2,1,0:T(8,128)(2,1)}), bf16[4,48,128]{2,1,0:T(8,128)(2,1)S(1)}, u32[]{:S(2)}, u32[]{:S(2)}) async-start(bf16[4,48,128]{2,1,0:T(8,128)(2,1)} %shard_map.137), calls=%async_computation.1 | async-start | bytes 98304 | tf_op jit(solution)/shard_map/all_to_all | solution.py:192
  6.5 0.7 collective-permute-start
  7.2 0.0 collective-permute-done.edge
  7.2 0.0 copy-start.2
  7.2 0.6 copy-done.2
  7.8 2.2 %shard_map.136 = bf16[32,200,128]{2,1,0:T(8,128)(2,1)} custom-call(bf16[128,128]{1,0:T(8,128)(2,1)} %tok.1, f32[1,128]{1,0:T(1,128)} %bitcast.11, bf16[128,128]{1,0:T(8,128)(2,1)} %copy-done.2), custom_call_target="tpu_custom_call" | custom-call | tf_op jit(solution)/shard_map/pallas_call | solution.py:177
  10.0 0.0 copy-start
  10.0 0.0 copy-start.1
  10.0 0.9 all-to-all-done.1
  10.9 16.5 %all-to-all-start = ((bf16[32,200,128]{2,1,0:T(8,128)(2,1)}), bf16[32,200,128]{2,1,0:T(8,128)(2,1)S(1)}, u32[]{:S(2)}, u32[]{:S(2)}) async-start(bf16[32,200,128]{2,1,0:T(8,128)(2,1)} %shard_map.136), calls=%async_computation | async-start | bytes 3276800 | tf_op jit(solution)/shard_map/all_to_all | solution.py:194
  27.4 32.8 %all_gather.3 = bf16[3072,128]{1,0:T(8,128)(2,1)S(1)} all-gather(bf16[192,128]{1,0:T(8,128)(2,1)S(1)} %bitcast.8), channel_id=1, replica_groups=mesh['z'=16,'y'=4,'x'=4,'c'=2] {'z'}, dimensions={0}, use_global_device_ids=true | all-gather | bytes 835584 | tf_op jit(solution)/shard_map/all_gather | solution.py:195
  60.2 0.0 all-to-all-done.t
  60.2 0.0 copy-done
  60.2 0.0 copy-done.1
  60.2 2.4 %shard_map.138 = (f32[16,128,128]{2,1,0:T(8,128)S(1)}, bf16[16,128,128]{2,1,0:T(8,128)(2,1)S(1)}, f32[128,128]{1,0:T(8,128)S(1)}, f32[128,128]{1,0:T(8,128)S(1)}) custom-call(bf16[32,200,128]{2,1,0:T(8,128)(2,1)S(1)} %all-to-all-done.t, bf16[16,4,48,128]{3,2,1,0:T(8,128)(2,1)S(1)} %bitcast.6, f32[3,128]{1,0:T(4,128)S(1)} %copy-done, f32[1,2]{1,0:T(1,128)S(1)} %bitcast.7), custom_call_target="tpu_custom_call" | custom-call | tf_op jit(solution)/shard_map/pallas_call | solution.py:177
  62.6 7.9 %collective-permute-start.1 = (bf16[16,128,128]{2,1,0:T(8,128)(2,1)S(1)}, bf16[16,128,128]{2,1,0:T(8,128)(2,1)S(1)}, u32[]{:S(2)}, u32[]{:S(2)}) collective-permute-start(bf16[16,128,128]{2,1,0:T(8,128)(2,1)S(1)} %get-tuple-element.10), channel_id=1, source_target_pairs={{0,1},{1,0},{2,3},{3,2},{4,5},{5,4},{6,7},{7,6},{8,9},{9,8},{10,11... | collective-permute-start | bytes 1572872 | tf_op jit(solution)/shard_map/ppermute | solution.py:208
  70.5 1.5 %collective-permute-done.1.came = bf16[16,128,128]{2,1,0:T(8,128)(2,1)S(1)} collective-permute-done((bf16[16,128,128]{2,1,0:T(8,128)(2,1)S(1)}, bf16[16,128,128]{2,1,0:T(8,128)(2,1)S(1)}, u32[]{:S(2)}, u32[]{:S(2)}) %collective-permute-start.1) | collective-permute-done | bytes 524320 | tf_op jit(solution)/shard_map/ppermute | solution.py:208
  72.0 0.9 shard_map.139
  72.9 6.3 %all-to-all-start.2 = ((bf16[16,128,128]{2,1,0:T(8,128)(2,1)}), bf16[16,128,128]{2,1,0:T(8,128)(2,1)S(1)}, u32[]{:S(2)}, u32[]{:S(2)}) async-start(bf16[16,128,128]{2,1,0:T(8,128)(2,1)} %shard_map.139), calls=%async_computation.2 | async-start | bytes 1048576 | tf_op jit(solution)/shard_map/all_to_all | solution.py:210
  79.2 3.3 %collective-permute-start.2 = (f32[128,128]{1,0:T(8,128)S(1)}, f32[128,128]{1,0:T(8,128)S(1)}, u32[]{:S(2)}, u32[]{:S(2)}) collective-permute-start(f32[128,128]{1,0:T(8,128)S(1)} %get-tuple-element.12), channel_id=1, source_target_pairs={{0,8},{8,0},{16,24},{24,16},{1,9},{9,1},{17,25},{25,17},{2,10},{10... | collective-permute-start | bytes 196616 | tf_op jit(solution)/shard_map/ppermute | solution.py:211
  82.5 6.2 %collective-permute-done.2.pair = f32[128,128]{1,0:T(8,128)S(1)} collective-permute-done((f32[128,128]{1,0:T(8,128)S(1)}, f32[128,128]{1,0:T(8,128)S(1)}, u32[]{:S(2)}, u32[]{:S(2)}) %collective-permute-start.2) | collective-permute-done | bytes 65568 | tf_op jit(solution)/shard_map/ppermute | solution.py:211
  88.6 1.3 %all-to-all-done.2.m = bf16[16,128,128]{2,1,0:T(8,128)(2,1)S(1)} async-done(((bf16[16,128,128]{2,1,0:T(8,128)(2,1)}), bf16[16,128,128]{2,1,0:T(8,128)(2,1)S(1)}, u32[]{:S(2)}, u32[]{:S(2)}) %all-to-all-start.2) | async-done | bytes 524320 | tf_op jit(solution)/shard_map/all_to_all | solution.py:210
  89.9 0.7 shard_map.141
  (1 shorter events, 0.0 us)
Async XLA Ops:
  1.5 9.4 %all-to-all-start.1 = ((bf16[4,48,128]{2,1,0:T(8,128)(2,1)}), bf16[4,48,128]{2,1,0:T(8,128)(2,1)S(1)}, u32[]{:S(2)}, u32[]{:S(2)}) async-start(bf16[4,48,128]{2,1,0:T(8,128)(2,1)} %shard_map.137), calls=%async_computation.1 | async-start | bytes 98304 | tf_op jit(solution)/shard_map/all_to_all | solution.py:192
  6.5 0.7 collective-permute-start
  7.2 0.6 copy-start.2
  10.0 50.2 %copy-start = (f32[3,128]{1,0:T(4,128)S(1)}, f32[3,128]{1,0:T(4,128)}, u32[]{:S(2)}) copy-start(f32[3,128]{1,0:T(4,128)} %taps.1) | copy-start | bytes 4612
  10.0 50.2 %copy-start.1 = (f32[2]{0:T(128)S(1)}, f32[2]{0:T(128)}, u32[]{:S(2)}) copy-start(f32[2]{0:T(128)} %param.24) | copy-start | bytes 28
  10.9 49.3 %all-to-all-start = ((bf16[32,200,128]{2,1,0:T(8,128)(2,1)}), bf16[32,200,128]{2,1,0:T(8,128)(2,1)S(1)}, u32[]{:S(2)}, u32[]{:S(2)}) async-start(bf16[32,200,128]{2,1,0:T(8,128)(2,1)} %shard_map.136), calls=%async_computation | async-start | bytes 3276800 | tf_op jit(solution)/shard_map/all_to_all | solution.py:194
  62.6 9.4 %collective-permute-start.1 = (bf16[16,128,128]{2,1,0:T(8,128)(2,1)S(1)}, bf16[16,128,128]{2,1,0:T(8,128)(2,1)S(1)}, u32[]{:S(2)}, u32[]{:S(2)}) collective-permute-start(bf16[16,128,128]{2,1,0:T(8,128)(2,1)S(1)} %get-tuple-element.10), channel_id=1, source_target_pairs={{0,1},{1,0},{2,3},{3,2},{4,5},{5,4},{6,7},{7,6},{8,9},{9,8},{10,11... | collective-permute-start | bytes 1572872 | tf_op jit(solution)/shard_map/ppermute | solution.py:208
  72.9 17.0 %all-to-all-start.2 = ((bf16[16,128,128]{2,1,0:T(8,128)(2,1)}), bf16[16,128,128]{2,1,0:T(8,128)(2,1)S(1)}, u32[]{:S(2)}, u32[]{:S(2)}) async-start(bf16[16,128,128]{2,1,0:T(8,128)(2,1)} %shard_map.139), calls=%async_computation.2 | async-start | bytes 1048576 | tf_op jit(solution)/shard_map/all_to_all | solution.py:210
  79.2 9.4 %collective-permute-start.2 = (f32[128,128]{1,0:T(8,128)S(1)}, f32[128,128]{1,0:T(8,128)S(1)}, u32[]{:S(2)}, u32[]{:S(2)}) collective-permute-start(f32[128,128]{1,0:T(8,128)S(1)} %get-tuple-element.12), channel_id=1, source_target_pairs={{0,8},{8,0},{16,24},{24,16},{1,9},{9,1},{17,25},{25,17},{2,10},{10... | collective-permute-start | bytes 196616 | tf_op jit(solution)/shard_map/ppermute | solution.py:211

commit v8 on v6

--- a/solution.py
+++ b/solution.py
@@ -118,22 +118,22 @@
         i = lax.broadcasted_iota(jnp.int32, (TOK, span), 0)
         j = lax.broadcasted_iota(jnp.int32, (TOK, span), 1)
         near = jnp.abs(i + WINDOW - j) <= WINDOW
+        edge_low, edge_high = jnp.where(z == 0, WINDOW, 0), jnp.where(z == ZN - 1, TOK + WINDOW, span)
+        masks = [near & (j >= edge_low)] + [near] * (YN - 2) + [near & (j < edge_high)]
+        scores, tops, weights = [], [], []
         for b in range(YN):
             q = p_scr[WINDOW + TOK * b : WINDOW + TOK * (b + 1), :HALF].astype(BF16)
             k = p_scr[TOK * b : TOK * b + span, HALF:LANES].astype(BF16)
+            scores.append(jnp.where(masks[b], nt_dot(q, k) * (HALF**-0.5), NEGATIVE))
+        for b in range(YN):
+            tops.append(jnp.maximum(jnp.max(scores[b], axis=1, keepdims=True), logit))
+        for b in range(YN):
+            weights.append(jnp.exp(scores[b] - tops[b]))
+        for b in range(YN):
             v = p_scr[TOK * b : TOK * b + span, LANES:].astype(BF16)
-            scores = nt_dot(q, k) * (HALF**-0.5)
-            allowed = near
-            if b == 0:
-                allowed = near & (j >= jnp.where(z == 0, WINDOW, 0))
-            if b == YN - 1:
-                allowed = near & (j < jnp.where(z == ZN - 1, TOK + WINDOW, span))
-            scores = jnp.where(allowed, scores, NEGATIVE)
-            top = jnp.maximum(jnp.max(scores, axis=1, keepdims=True), logit)
-            e = jnp.exp(scores - top)
-            share = jnp.sum(e, axis=1, keepdims=True) + jnp.exp(logit - top)
-            high = e.astype(BF16)
-            low = (e - high.astype(F32)).astype(BF16)
+            share = jnp.sum(weights[b], axis=1, keepdims=True) + jnp.exp(logit - tops[b])
+            high = weights[b].astype(BF16)
+            low = (weights[b] - high.astype(F32)).astype(BF16)
             send(b, ((nn_dot(high, v) + nn_dot(low, v)) * (1.0 / share)).astype(BF16))
 
     @pl.when(y >= 2)

time: 89.7 us -> 89.7 us (level)
  no operation moved by 1% of the time
where the time goes in v8:
time: 89.7 us; the launch traced here: 89.1 us
  starting transfers between devices  38.6 us (43%)
  blocking collectives  34.6 us (39%)
  waiting for transfers between devices  7.77 us (9%)
  Pallas kernels  7.46 us (8%)
    all_gather x1, blocking collectives, on_device(): lax.all_gather(wy.reshape(YN * 40, LANES), 'z', axis=0, tiled=True)  34.6 us
    all_to_all x1, starting transfers between devices, on_device(): message = lax.all_to_all(message, plane, 0, 0, tiled=True)  12.4 us
    ppermute x3, starting transfers between devices, on_device(): lax.ppermute(gates[k], 'y', [(y, (y + k) % YN) for y in range(YN)])  10.7 us
    all_to_all x1, starting transfers between devices, on_device(): gathered_tok = lax.all_to_all(spread, plane, 0, 0, tiled=True)  7.49 us
    pallas_call x5, Pallas kernels, call(): pl.pallas_call(kernel, out_shape=outs, in_specs=specs or [VM] * len(args)...  7.46 us
    all_to_all x1, starting transfers between devices, on_device(): wy = lax.all_to_all(wy, 'y', 0, 0, tiled=True)  7.36 us
    ppermute x3, waiting for transfers between devices, on_device(): lax.ppermute(gates[k], 'y', [(y, (y + k) % YN) for y in range(YN)])  4.61 us
  transfers between devices with their start and end apart: 7, of which 5 were waited for; matrix products, arithmetic and copies ran while one was open for 0% of the time, Pallas kernels for 4%

profile of v8, /device:TPU:1, one launch (start us, length us, event | category | flops | bytes accessed | tf_op | source)
XLA Modules:
  0.0 89.1 jit_solution(15285826721678276803)
XLA Ops:
  0.0 0.7 collective-permute-start
  0.7 1.5 %shard_map.137 = bf16[4,40,128]{2,1,0:T(8,128)(2,1)} custom-call(bf16[16,128]{1,0:T(8,128)(2,1)} %q.1, bf16[16,64]{1,0:T(8,128)(2,1)} %k.1, bf16[16,64]{1,0:T(8,128)(2,1)} %v.1, bf16[16,128]{1,0:T(8,128)(2,1)} %ci.1, bf16[16,128]{1,0:T(8,128)(2,1)} %pre.1, bf16[16,128]{1,0:T(8,128)(2,1)} %post.1, bf16[16,128]{1,0:T(8,128)(2,1)} %ag.1, bf16[16,128]{1,0:T(8,128)(2,1)} %cg.1, ...), custom_call_target="tpu_custom_call" | custom-call | tf_op jit(solution)/shard_map/pallas_call | solution.py:195
  2.2 7.4 %all-to-all-start.1 = ((bf16[4,40,128]{2,1,0:T(8,128)(2,1)}), bf16[4,40,128]{2,1,0:T(8,128)(2,1)S(1)}, u32[]{:S(2)}, u32[]{:S(2)}) async-start(bf16[4,40,128]{2,1,0:T(8,128)(2,1)} %shard_map.137), calls=%async_computation.1 | async-start | bytes 81920 | tf_op jit(solution)/shard_map/all_to_all | solution.py:210
  9.5 0.0 collective-permute-done.edge
  9.5 0.0 copy-start.2
  9.5 0.6 copy-done.2
  10.2 2.2 %shard_map.136 = bf16[32,200,128]{2,1,0:T(8,128)(2,1)} custom-call(bf16[128,128]{1,0:T(8,128)(2,1)} %tok.1, f32[1,128]{1,0:T(1,128)} %bitcast.11, bf16[128,128]{1,0:T(8,128)(2,1)} %copy-done.2), custom_call_target="tpu_custom_call" | custom-call | tf_op jit(solution)/shard_map/pallas_call | solution.py:195
  12.4 0.0 copy-start
  12.4 0.0 copy-start.1
  12.4 1.5 %all-to-all-done.1 = bf16[4,40,128]{2,1,0:T(8,128)(2,1)S(1)} async-done(((bf16[4,40,128]{2,1,0:T(8,128)(2,1)}), bf16[4,40,128]{2,1,0:T(8,128)(2,1)S(1)}, u32[]{:S(2)}, u32[]{:S(2)}) %all-to-all-start.1) | async-done | bytes 40992 | tf_op jit(solution)/shard_map/all_to_all | solution.py:210
  13.9 7.5 %all-to-all-start = ((bf16[32,200,128]{2,1,0:T(8,128)(2,1)}), bf16[32,200,128]{2,1,0:T(8,128)(2,1)S(1)}, u32[]{:S(2)}, u32[]{:S(2)}) async-start(bf16[32,200,128]{2,1,0:T(8,128)(2,1)} %shard_map.136), calls=%async_computation | async-start | bytes 3276800 | tf_op jit(solution)/shard_map/all_to_all | solution.py:212
  21.4 34.6 %all_gather.3 = bf16[2560,128]{1,0:T(8,128)(2,1)S(1)} all-gather(bf16[160,128]{1,0:T(8,128)(2,1)S(1)} %bitcast.8), channel_id=1, replica_groups=mesh['z'=16,'y'=4,'x'=4,'c'=2] {'z'}, dimensions={0}, use_global_device_ids=true | all-gather | bytes 696320 | tf_op jit(solution)/shard_map/all_gather | solution.py:213
  56.0 0.0 all-to-all-done.t
  56.0 0.0 copy-done
  56.0 0.0 copy-done.1
  56.0 2.5 %shard_map.138 = (bf16[32,128,128]{2,1,0:T(8,128)(2,1)}, f32[64,128]{1,0:T(8,128)S(1)}, f32[64,128]{1,0:T(8,128)S(1)}, f32[64,128]{1,0:T(8,128)S(1)}, f32[64,128]{1,0:T(8,128)S(1)}) custom-call(bf16[32,200,128]{2,1,0:T(8,128)(2,1)S(1)} %all-to-all-done.t, bf16[16,4,40,128]{3,2,1,0:T(8,128)(2,1)S(1)} %bitcast.6, f32[3,128]{1,0:T(4,128)S(1)} %copy-done, ...), custom_call_target="tpu_custom_call" | custom-call | tf_op jit(solution)/shard_map/pallas_call | solution.py:195
  58.5 12.4 %all-to-all-start.2 = ((bf16[32,128,128]{2,1,0:T(8,128)(2,1)}), bf16[32,128,128]{2,1,0:T(8,128)(2,1)S(1)}, u32[]{:S(2)}, u32[]{:S(2)}) async-start(bf16[32,128,128]{2,1,0:T(8,128)(2,1)} %get-tuple-element.10), calls=%async_computation.2 | async-start | bytes 2097152 | tf_op jit(solution)/shard_map/all_to_all | solution.py:230
  71.0 3.3 %collective-permute-start.1 = (f32[64,128]{1,0:T(8,128)S(1)}, f32[64,128]{1,0:T(8,128)S(1)}, u32[]{:S(2)}, u32[]{:S(2)}) collective-permute-start(f32[64,128]{1,0:T(8,128)S(1)} %get-tuple-element.12), channel_id=1, source_target_pairs={{0,8},{8,16},{16,24},{24,0},{1,9},{9,17},{17,25},{25,1},{2,10},{10... | collective-permute-start | bytes 98312 | tf_op jit(solution)/shard_map/ppermute | solution.py:232
  74.2 4.3 %collective-permute-start.2 = (f32[64,128]{1,0:T(8,128)S(1)}, f32[64,128]{1,0:T(8,128)S(1)}, u32[]{:S(2)}, u32[]{:S(2)}) collective-permute-start(f32[64,128]{1,0:T(8,128)S(1)} %get-tuple-element.13), channel_id=1, source_target_pairs={{0,16},{8,24},{16,0},{24,8},{1,17},{9,25},{17,1},{25,9},{2,18},{10... | collective-permute-start | bytes 98312 | tf_op jit(solution)/shard_map/ppermute | solution.py:232
  78.6 3.0 %collective-permute-start.3 = (f32[64,128]{1,0:T(8,128)S(1)}, f32[64,128]{1,0:T(8,128)S(1)}, u32[]{:S(2)}, u32[]{:S(2)}) collective-permute-start(f32[64,128]{1,0:T(8,128)S(1)} %get-tuple-element.14), channel_id=1, source_target_pairs={{0,24},{8,0},{16,8},{24,16},{1,25},{9,1},{17,9},{25,17},{2,26},{10... | collective-permute-start | bytes 98312 | tf_op jit(solution)/shard_map/ppermute | solution.py:232
  81.6 0.7 collective-permute-done.1.g_1
  82.4 3.6 %collective-permute-done.2.g_2 = f32[64,128]{1,0:T(8,128)S(1)} collective-permute-done((f32[64,128]{1,0:T(8,128)S(1)}, f32[64,128]{1,0:T(8,128)S(1)}, u32[]{:S(2)}, u32[]{:S(2)}) %collective-permute-start.2) | collective-permute-done | bytes 32800 | tf_op jit(solution)/shard_map/ppermute | solution.py:232
  85.9 0.3 collective-permute-done.3.g_3
  86.3 0.1 shard_map.139.gates
  86.4 1.6 %all-to-all-done.2.m = bf16[32,128,128]{2,1,0:T(8,128)(2,1)S(1)} async-done(((bf16[32,128,128]{2,1,0:T(8,128)(2,1)}), bf16[32,128,128]{2,1,0:T(8,128)(2,1)S(1)}, u32[]{:S(2)}, u32[]{:S(2)}) %all-to-all-start.2) | async-done | bytes 1048608 | tf_op jit(solution)/shard_map/all_to_all | solution.py:230
  88.0 1.1 %shard_map.140 = bf16[128,128]{1,0:T(8,128)(2,1)} custom-call(bf16[32,128,128]{2,1,0:T(8,128)(2,1)S(1)} %all-to-all-done.2.m, f32[2,128,128]{2,1,0:T(8,128)S(1)} %shard_map.139.gates), custom_call_target="tpu_custom_call" | custom-call | tf_op jit(solution)/shard_map/pallas_call | solution.py:195
Async XLA Ops:
  0.0 9.5 %collective-permute-start = (bf16[128,128]{1,0:T(8,128)(2,1)}, bf16[128,128]{1,0:T(8,128)(2,1)S(1)}, u32[]{:S(2)}, u32[]{:S(2)}) collective-permute-start(bf16[128,128]{1,0:T(8,128)(2,1)} %tok.1), channel_id=1, source_target_pairs={{24,32},{56,64},{88,96},{120,128},{152,160},{184,192},{216,224},{2... | collective-permute-start | bytes 98312 | tf_op jit(solution)/shard_map/ppermute | solution.py:208
  2.2 11.7 %all-to-all-start.1 = ((bf16[4,40,128]{2,1,0:T(8,128)(2,1)}), bf16[4,40,128]{2,1,0:T(8,128)(2,1)S(1)}, u32[]{:S(2)}, u32[]{:S(2)}) async-start(bf16[4,40,128]{2,1,0:T(8,128)(2,1)} %shard_map.137), calls=%async_computation.1 | async-start | bytes 81920 | tf_op jit(solution)/shard_map/all_to_all | solution.py:210
  9.5 0.6 copy-start.2
  12.4 43.6 %copy-start = (f32[3,128]{1,0:T(4,128)S(1)}, f32[3,128]{1,0:T(4,128)}, u32[]{:S(2)}) copy-start(f32[3,128]{1,0:T(4,128)} %taps.1) | copy-start | bytes 4612
  12.4 43.6 %copy-start.1 = (f32[2]{0:T(128)S(1)}, f32[2]{0:T(128)}, u32[]{:S(2)}) copy-start(f32[2]{0:T(128)} %param.24) | copy-start | bytes 28
  13.9 42.1 %all-to-all-start = ((bf16[32,200,128]{2,1,0:T(8,128)(2,1)}), bf16[32,200,128]{2,1,0:T(8,128)(2,1)S(1)}, u32[]{:S(2)}, u32[]{:S(2)}) async-start(bf16[32,200,128]{2,1,0:T(8,128)(2,1)} %shard_map.136), calls=%async_computation | async-start | bytes 3276800 | tf_op jit(solution)/shard_map/all_to_all | solution.py:212
  58.5 29.5 %all-to-all-start.2 = ((bf16[32,128,128]{2,1,0:T(8,128)(2,1)}), bf16[32,128,128]{2,1,0:T(8,128)(2,1)S(1)}, u32[]{:S(2)}, u32[]{:S(2)}) async-start(bf16[32,128,128]{2,1,0:T(8,128)(2,1)} %get-tuple-element.10), calls=%async_computation.2 | async-start | bytes 2097152 | tf_op jit(solution)/shard_map/all_to_all | solution.py:230
  71.0 11.4 %collective-permute-start.1 = (f32[64,128]{1,0:T(8,128)S(1)}, f32[64,128]{1,0:T(8,128)S(1)}, u32[]{:S(2)}, u32[]{:S(2)}) collective-permute-start(f32[64,128]{1,0:T(8,128)S(1)} %get-tuple-element.12), channel_id=1, source_target_pairs={{0,8},{8,16},{16,24},{24,0},{1,9},{9,17},{17,25},{25,1},{2,10},{10... | collective-permute-start | bytes 98312 | tf_op jit(solution)/shard_map/ppermute | solution.py:232
  74.2 11.7 %collective-permute-start.2 = (f32[64,128]{1,0:T(8,128)S(1)}, f32[64,128]{1,0:T(8,128)S(1)}, u32[]{:S(2)}, u32[]{:S(2)}) collective-permute-start(f32[64,128]{1,0:T(8,128)S(1)} %get-tuple-element.13), channel_id=1, source_target_pairs={{0,16},{8,24},{16,0},{24,8},{1,17},{9,25},{17,1},{25,9},{2,18},{10... | collective-permute-start | bytes 98312 | tf_op jit(solution)/shard_map/ppermute | solution.py:232
  78.6 7.7 %collective-permute-start.3 = (f32[64,128]{1,0:T(8,128)S(1)}, f32[64,128]{1,0:T(8,128)S(1)}, u32[]{:S(2)}, u32[]{:S(2)}) collective-permute-start(f32[64,128]{1,0:T(8,128)S(1)} %get-tuple-element.14), channel_id=1, source_target_pairs={{0,24},{8,0},{16,8},{24,16},{1,25},{9,1},{17,9},{25,17},{2,26},{10... | collective-permute-start | bytes 98312 | tf_op jit(solution)/shard_map/ppermute | solution.py:232

commit v9 on v8

--- a/solution.py
+++ b/solution.py
@@ -71,7 +71,7 @@
     z = lax.axis_index("z")
     gains = []
     for tp in range(TPN):
-        r = t[tp, SLOT:, :].astype(F32)
+        r = t[YN * tp, SLOT:, :].astype(F32)
         gains.append(r[0:1] + r[1:2] + r[2:3])
     segments = [(0, 0, TOK, WINDOW)]
     segments += [(WINDOW + TOK * b, b, 0, TOK) for b in range(YN)]
@@ -79,11 +79,11 @@
     for at, b, start, count in segments:
         total = jnp.zeros((count, LANES), F32)
         for tp in range(TPN):
-            x = t[b * TPN + tp, start : start + count, :].astype(F32)
+            x = t[YN * tp + b, start : start + count, :].astype(F32)
             total = total + x * x
         scale = lax.rsqrt(jnp.sum(total, axis=1, keepdims=True) / FEATURES + EPSILON)
         for tp in range(TPN):
-            x = t[b * TPN + tp, start : start + count, :].astype(F32)
+            x = t[YN * tp + b, start : start + count, :].astype(F32)
             n_scr[at : at + count, LANES * tp : LANES * (tp + 1)] = (x * scale * gains[tp]).astype(BF16)
     weight = jnp.concatenate(
         [w[:, :, 16 * pair : 16 * pair + 16, :].reshape(FEATURES, LANES) for pair in range(2)], axis=1
@@ -102,12 +102,11 @@
         w_scr[tp] = rows.reshape(LANES, LANES).astype(BF16)
 
     def outgoing(b):
-        part = pl.ds(b * TPN, TPN)
-        return pltpu.make_async_copy(m_scr.at[part], out.at[part], sems.at[b])
+        return pltpu.make_async_copy(m_scr.at[:, b], out.at[:, b], sems.at[b])
 
     def send(b, mixed):
         for tp in range(TPN):
-            m_scr[b * TPN + tp] = jnp.where(left, mixed, w_scr[tp])
+            m_scr[tp, b] = jnp.where(left, mixed, w_scr[tp])
         outgoing(b).start()
 
     @pl.when(y < 2)
@@ -173,7 +172,7 @@
     for branch in range(2):
         mixed, columns = [], []
         for tp in range(TPN):
-            both = joined(m[(2 * branch) * TPN + tp], m[(2 * branch + 1) * TPN + tp], left)
+            both = joined(m[YN * tp + 2 * branch], m[YN * tp + 2 * branch + 1], left)
             mixed.append(both[0])
             columns.append(both[1])
         value = nt_dot(jnp.concatenate(mixed, axis=1), jnp.concatenate(columns, axis=1))
@@ -203,7 +202,7 @@
 
 
 def on_device(tok, gain, q, k, v, ci, pre, post, ag, cg, sink, taps, wa, wc):
-    plane = ("y", "x", "c")
+    plane = ("x", "c", "y")
     edges = [(YN * z + YN - 1, YN * z + YN) for z in range(ZN - 1)]
     edge = lax.ppermute(tok, ("z", "y"), edges + [(b, a) for a, b in edges])
     wy = call(pack_kernel, shaped((YN, 40, LANES)), (q, k, v, ci, pre, post, ag, cg, wa.T, wc.T), limit=60)
@@ -213,7 +212,7 @@
     w = lax.all_gather(wy.reshape(YN * 40, LANES), "z", axis=0, tiled=True).reshape(ZN, YN, 40, LANES)
     message, *gates = call(
         mix_kernel,
-        (shaped((PLANE, TOK, LANES)),) + (shaped((HALF, LANES), F32),) * 4,
+        (shaped((TPN, YN, TOK, LANES)),) + (shaped((HALF, LANES), F32),) * 4,
         (gathered_tok, w, taps, sink.reshape(1, 2)),
         [VM] * 4,
         [
@@ -221,13 +220,13 @@
             pltpu.VMEM((ROWS, 2 * LANES), F32),
             pltpu.VMEM((YN, HALF, LANES), F32),
             pltpu.VMEM((TPN, LANES, LANES), BF16),
-            pltpu.VMEM((PLANE, TOK, LANES), BF16),
+            pltpu.VMEM((TPN, YN, TOK, LANES), BF16),
             pltpu.SemaphoreType.DMA((YN,)),
         ],
         20,
         first=pl.BlockSpec(memory_space=pl.ANY),
     )
-    message = lax.all_to_all(message, plane, 0, 0, tiled=True)
+    message = lax.all_to_all(message.reshape(PLANE, TOK, LANES), plane, 0, 0, tiled=True)
     for k in range(1, YN):
         gates[k] = lax.ppermute(gates[k], "y", [(y, (y + k) % YN) for y in range(YN)])
     gates = call(gate_kernel, shaped((2, TOK, LANES), F32), gates, scratch=[pltpu.VMEM((YN, HALF, LANES), F32)])

time: 89.7 us -> 88.9 us (level)
  no operation moved by 1% of the time
where the time goes in v9:
time: 88.9 us; the launch traced here: 88.3 us
  starting transfers between devices  38.9 us (44%)
  blocking collectives  34.3 us (39%)
  Pallas kernels  7.37 us (8%)
  waiting for transfers between devices  7.12 us (8%)
    all_gather x1, blocking collectives, on_device(): lax.all_gather(wy.reshape(YN * 40, LANES), 'z', axis=0, tiled=True)  34.3 us
    all_to_all x1, starting transfers between devices, on_device(): lax.all_to_all(message.reshape(PLANE, TOK, LANES), plane, 0, 0, tiled=True)  12.7 us
    ppermute x3, starting transfers between devices, on_device(): lax.ppermute(gates[k], 'y', [(y, (y + k) % YN) for y in range(YN)])  10.7 us
    all_to_all x1, starting transfers between devices, on_device(): gathered_tok = lax.all_to_all(spread, plane, 0, 0, tiled=True)  7.51 us
    pallas_call x5, Pallas kernels, call(): pl.pallas_call(kernel, out_shape=outs, in_specs=specs or [VM] * len(args)...  7.37 us
    all_to_all x1, starting transfers between devices, on_device(): wy = lax.all_to_all(wy, 'y', 0, 0, tiled=True)  7.36 us
    ppermute x3, waiting for transfers between devices, on_device(): lax.ppermute(gates[k], 'y', [(y, (y + k) % YN) for y in range(YN)])  4.72 us
  transfers between devices with their start and end apart: 7, of which 5 were waited for; matrix products, arithmetic and copies ran while one was open for 0% of the time, Pallas kernels for 4%

profile of v9, /device:TPU:1, one launch (start us, length us, event | category | flops | bytes accessed | tf_op | source)
XLA Modules:
  0.0 88.3 jit_solution(17709132270704560488)
XLA Ops:
  0.0 0.7 collective-permute-start
  0.7 1.5 %shard_map.137 = bf16[4,40,128]{2,1,0:T(8,128)(2,1)} custom-call(bf16[16,128]{1,0:T(8,128)(2,1)} %q.1, bf16[16,64]{1,0:T(8,128)(2,1)} %k.1, bf16[16,64]{1,0:T(8,128)(2,1)} %v.1, bf16[16,128]{1,0:T(8,128)(2,1)} %ci.1, bf16[16,128]{1,0:T(8,128)(2,1)} %pre.1, bf16[16,128]{1,0:T(8,128)(2,1)} %post.1, bf16[16,128]{1,0:T(8,128)(2,1)} %ag.1, bf16[16,128]{1,0:T(8,128)(2,1)} %cg.1, ...), custom_call_target="tpu_custom_call" | custom-call | tf_op jit(solution)/shard_map/pallas_call | solution.py:194
  2.2 7.4 %all-to-all-start.1 = ((bf16[4,40,128]{2,1,0:T(8,128)(2,1)}), bf16[4,40,128]{2,1,0:T(8,128)(2,1)S(1)}, u32[]{:S(2)}, u32[]{:S(2)}) async-start(bf16[4,40,128]{2,1,0:T(8,128)(2,1)} %shard_map.137), calls=%async_computation.1 | async-start | bytes 81920 | tf_op jit(solution)/shard_map/all_to_all | solution.py:209
  9.5 0.0 collective-permute-done.edge
  9.5 0.0 copy-start.2
  9.5 0.6 copy-done.2
  10.2 2.2 %shard_map.136 = bf16[32,200,128]{2,1,0:T(8,128)(2,1)} custom-call(bf16[128,128]{1,0:T(8,128)(2,1)} %tok.1, f32[1,128]{1,0:T(1,128)} %bitcast.12, bf16[128,128]{1,0:T(8,128)(2,1)} %copy-done.2), custom_call_target="tpu_custom_call" | custom-call | tf_op jit(solution)/shard_map/pallas_call | solution.py:194
  12.4 0.0 copy-start
  12.4 0.0 copy-start.1
  12.4 1.5 %all-to-all-done.1 = bf16[4,40,128]{2,1,0:T(8,128)(2,1)S(1)} async-done(((bf16[4,40,128]{2,1,0:T(8,128)(2,1)}), bf16[4,40,128]{2,1,0:T(8,128)(2,1)S(1)}, u32[]{:S(2)}, u32[]{:S(2)}) %all-to-all-start.1) | async-done | bytes 40992 | tf_op jit(solution)/shard_map/all_to_all | solution.py:209
  13.9 7.5 %all-to-all-start = ((bf16[32,200,128]{2,1,0:T(8,128)(2,1)}), bf16[32,200,128]{2,1,0:T(8,128)(2,1)S(1)}, u32[]{:S(2)}, u32[]{:S(2)}) async-start(bf16[32,200,128]{2,1,0:T(8,128)(2,1)} %shard_map.136), calls=%async_computation | async-start | bytes 3276800 | tf_op jit(solution)/shard_map/all_to_all | solution.py:211
  21.4 34.3 %all_gather.3 = bf16[2560,128]{1,0:T(8,128)(2,1)S(1)} all-gather(bf16[160,128]{1,0:T(8,128)(2,1)S(1)} %bitcast.9), channel_id=1, replica_groups=mesh['z'=16,'y'=4,'x'=4,'c'=2] {'z'}, dimensions={0}, use_global_device_ids=true | all-gather | bytes 696320 | tf_op jit(solution)/shard_map/all_gather | solution.py:212
  55.7 0.0 all-to-all-done.t
  55.7 0.0 copy-done
  55.7 0.0 copy-done.1
  55.7 2.5 %shard_map.138 = (bf16[8,4,128,128]{3,2,1,0:T(8,128)(2,1)}, f32[64,128]{1,0:T(8,128)S(1)}, f32[64,128]{1,0:T(8,128)S(1)}, f32[64,128]{1,0:T(8,128)S(1)}, f32[64,128]{1,0:T(8,128)S(1)}) custom-call(bf16[32,200,128]{2,1,0:T(8,128)(2,1)S(1)} %all-to-all-done.t, bf16[16,4,40,128]{3,2,1,0:T(8,128)(2,1)S(1)} %bitcast.7, f32[3,128]{1,0:T(4,128)S(1)} %copy-done, ...), custom_call_target="tpu_custom_call" | custom-call | tf_op jit(solution)/shard_map/pallas_call | solution.py:194
  58.2 12.7 %all-to-all-start.2 = ((bf16[32,128,128]{2,1,0:T(8,128)(2,1)}), bf16[32,128,128]{2,1,0:T(8,128)(2,1)S(1)}, u32[]{:S(2)}, u32[]{:S(2)}) async-start(bf16[32,128,128]{2,1,0:T(8,128)(2,1)} %bitcast.6), calls=%async_computation.2 | async-start | bytes 2097152 | tf_op jit(solution)/shard_map/all_to_all | solution.py:229
  70.9 3.3 %collective-permute-start.1 = (f32[64,128]{1,0:T(8,128)S(1)}, f32[64,128]{1,0:T(8,128)S(1)}, u32[]{:S(2)}, u32[]{:S(2)}) collective-permute-start(f32[64,128]{1,0:T(8,128)S(1)} %get-tuple-element.12), channel_id=1, source_target_pairs={{0,8},{8,16},{16,24},{24,0},{1,9},{9,17},{17,25},{25,1},{2,10},{10... | collective-permute-start | bytes 98312 | tf_op jit(solution)/shard_map/ppermute | solution.py:231
  74.1 4.3 %collective-permute-start.2 = (f32[64,128]{1,0:T(8,128)S(1)}, f32[64,128]{1,0:T(8,128)S(1)}, u32[]{:S(2)}, u32[]{:S(2)}) collective-permute-start(f32[64,128]{1,0:T(8,128)S(1)} %get-tuple-element.13), channel_id=1, source_target_pairs={{0,16},{8,24},{16,0},{24,8},{1,17},{9,25},{17,1},{25,9},{2,18},{10... | collective-permute-start | bytes 98312 | tf_op jit(solution)/shard_map/ppermute | solution.py:231
  78.4 3.1 %collective-permute-start.3 = (f32[64,128]{1,0:T(8,128)S(1)}, f32[64,128]{1,0:T(8,128)S(1)}, u32[]{:S(2)}, u32[]{:S(2)}) collective-permute-start(f32[64,128]{1,0:T(8,128)S(1)} %get-tuple-element.14), channel_id=1, source_target_pairs={{0,24},{8,0},{16,8},{24,16},{1,25},{9,1},{17,9},{25,17},{2,26},{10... | collective-permute-start | bytes 98312 | tf_op jit(solution)/shard_map/ppermute | solution.py:231
  81.5 0.7 collective-permute-done.1.g_1
  82.2 2.3 %collective-permute-done.2.g_2 = f32[64,128]{1,0:T(8,128)S(1)} collective-permute-done((f32[64,128]{1,0:T(8,128)S(1)}, f32[64,128]{1,0:T(8,128)S(1)}, u32[]{:S(2)}, u32[]{:S(2)}) %collective-permute-start.2) | collective-permute-done | bytes 32800 | tf_op jit(solution)/shard_map/ppermute | solution.py:231
  84.5 1.7 %collective-permute-done.3.g_3 = f32[64,128]{1,0:T(8,128)S(1)} collective-permute-done((f32[64,128]{1,0:T(8,128)S(1)}, f32[64,128]{1,0:T(8,128)S(1)}, u32[]{:S(2)}, u32[]{:S(2)}) %collective-permute-start.3) | collective-permute-done | bytes 32800 | tf_op jit(solution)/shard_map/ppermute | solution.py:231
  86.3 0.1 shard_map.139.gates
  86.4 0.9 all-to-all-done.2.m
  87.3 1.1 %shard_map.140 = bf16[128,128]{1,0:T(8,128)(2,1)} custom-call(bf16[32,128,128]{2,1,0:T(8,128)(2,1)S(1)} %all-to-all-done.2.m, f32[2,128,128]{2,1,0:T(8,128)S(1)} %shard_map.139.gates), custom_call_target="tpu_custom_call" | custom-call | tf_op jit(solution)/shard_map/pallas_call | solution.py:194
Async XLA Ops:
  0.0 9.5 %collective-permute-start = (bf16[128,128]{1,0:T(8,128)(2,1)}, bf16[128,128]{1,0:T(8,128)(2,1)S(1)}, u32[]{:S(2)}, u32[]{:S(2)}) collective-permute-start(bf16[128,128]{1,0:T(8,128)(2,1)} %tok.1), channel_id=1, source_target_pairs={{24,32},{56,64},{88,96},{120,128},{152,160},{184,192},{216,224},{2... | collective-permute-start | bytes 98312 | tf_op jit(solution)/shard_map/ppermute | solution.py:207
  2.2 11.7 %all-to-all-start.1 = ((bf16[4,40,128]{2,1,0:T(8,128)(2,1)}), bf16[4,40,128]{2,1,0:T(8,128)(2,1)S(1)}, u32[]{:S(2)}, u32[]{:S(2)}) async-start(bf16[4,40,128]{2,1,0:T(8,128)(2,1)} %shard_map.137), calls=%async_computation.1 | async-start | bytes 81920 | tf_op jit(solution)/shard_map/all_to_all | solution.py:209
  9.5 0.6 copy-start.2
  12.4 43.3 %copy-start = (f32[3,128]{1,0:T(4,128)S(1)}, f32[3,128]{1,0:T(4,128)}, u32[]{:S(2)}) copy-start(f32[3,128]{1,0:T(4,128)} %taps.1) | copy-start | bytes 4612
  12.4 43.3 %copy-start.1 = (f32[2]{0:T(128)S(1)}, f32[2]{0:T(128)}, u32[]{:S(2)}) copy-start(f32[2]{0:T(128)} %param.24) | copy-start | bytes 28
  13.9 41.8 %all-to-all-start = ((bf16[32,200,128]{2,1,0:T(8,128)(2,1)}), bf16[32,200,128]{2,1,0:T(8,128)(2,1)S(1)}, u32[]{:S(2)}, u32[]{:S(2)}) async-start(bf16[32,200,128]{2,1,0:T(8,128)(2,1)} %shard_map.136), calls=%async_computation | async-start | bytes 3276800 | tf_op jit(solution)/shard_map/all_to_all | solution.py:211
  58.2 29.1 %all-to-all-start.2 = ((bf16[32,128,128]{2,1,0:T(8,128)(2,1)}), bf16[32,128,128]{2,1,0:T(8,128)(2,1)S(1)}, u32[]{:S(2)}, u32[]{:S(2)}) async-start(bf16[32,128,128]{2,1,0:T(8,128)(2,1)} %bitcast.6), calls=%async_computation.2 | async-start | bytes 2097152 | tf_op jit(solution)/shard_map/all_to_all | solution.py:229
  70.9 11.4 %collective-permute-start.1 = (f32[64,128]{1,0:T(8,128)S(1)}, f32[64,128]{1,0:T(8,128)S(1)}, u32[]{:S(2)}, u32[]{:S(2)}) collective-permute-start(f32[64,128]{1,0:T(8,128)S(1)} %get-tuple-element.12), channel_id=1, source_target_pairs={{0,8},{8,16},{16,24},{24,0},{1,9},{9,17},{17,25},{25,1},{2,10},{10... | collective-permute-start | bytes 98312 | tf_op jit(solution)/shard_map/ppermute | solution.py:231
  74.1 10.4 %collective-permute-start.2 = (f32[64,128]{1,0:T(8,128)S(1)}, f32[64,128]{1,0:T(8,128)S(1)}, u32[]{:S(2)}, u32[]{:S(2)}) collective-permute-start(f32[64,128]{1,0:T(8,128)S(1)} %get-tuple-element.13), channel_id=1, source_target_pairs={{0,16},{8,24},{16,0},{24,8},{1,17},{9,25},{17,1},{25,9},{2,18},{10... | collective-permute-start | bytes 98312 | tf_op jit(solution)/shard_map/ppermute | solution.py:231
  78.4 7.8 %collective-permute-start.3 = (f32[64,128]{1,0:T(8,128)S(1)}, f32[64,128]{1,0:T(8,128)S(1)}, u32[]{:S(2)}, u32[]{:S(2)}) collective-permute-start(f32[64,128]{1,0:T(8,128)S(1)} %get-tuple-element.14), channel_id=1, source_target_pairs={{0,24},{8,0},{16,8},{24,16},{1,25},{9,1},{17,9},{25,17},{2,26},{10... | collective-permute-start | bytes 98312 | tf_op jit(solution)/shard_map/ppermute | solution.py:231

commit v10 on v9

--- a/solution.py
+++ b/solution.py
@@ -101,12 +101,17 @@
         rows = jnp.stack([turned(rows.reshape(HALF, LANES)).reshape(TPN, 8, LANES), rows], axis=1)
         w_scr[tp] = rows.reshape(LANES, LANES).astype(BF16)
 
+    for x in range(XN):
+        packed = jnp.where(left[:HALF], turned(w_scr[2 * x + 1])[:HALF], w_scr[2 * x + 1][HALF:])
+        for b in range(YN):
+            m_scr[x, b, TOK:, :] = packed
+
     def outgoing(b):
         return pltpu.make_async_copy(m_scr.at[:, b], out.at[:, b], sems.at[b])
 
     def send(b, mixed):
-        for tp in range(TPN):
-            m_scr[tp, b] = jnp.where(left, mixed, w_scr[tp])
+        for x in range(XN):
+            m_scr[x, b, :TOK, :] = jnp.where(left, mixed, w_scr[2 * x])
         outgoing(b).start()
 
     @pl.when(y < 2)
@@ -166,17 +171,28 @@
         out[branch] = jax.nn.sigmoid(jnp.concatenate(joined(*parts, left), axis=0))
 
 
-def final_kernel(m, gates, out):
+def partial_kernel(m, keep, give):
+    first_core = lax.axis_index("c") == 0
     left = lax.broadcasted_iota(jnp.int32, (TOK, LANES), 1) < HALF
+    for branch in range(2):
+        mixed, even, odd = [], [], []
+        for x in range(XN):
+            a, b = m[YN * x + 2 * branch], m[YN * x + 2 * branch + 1]
+            both = joined(a[:TOK], b[:TOK], left)
+            mixed.append(both[0])
+            even.append(both[1])
+            odd.append(jnp.concatenate(joined(a[TOK:], b[TOK:], left[:HALF]), axis=0))
+        mixed = jnp.concatenate(mixed, axis=1)
+        sums = [nt_dot(mixed, jnp.concatenate(columns, axis=1)) for columns in (even, odd)]
+        keep[branch] = jnp.where(first_core, sums[0], sums[1])
+        give[branch] = jnp.where(first_core, sums[1], sums[0])
+
+
+def final_kernel(keep, came, gates, out):
+    other = 1 - lax.axis_index("c")
     total = jnp.zeros((TOK, LANES), F32)
     for branch in range(2):
-        mixed, columns = [], []
-        for tp in range(TPN):
-            both = joined(m[YN * tp + 2 * branch], m[YN * tp + 2 * branch + 1], left)
-            mixed.append(both[0])
-            columns.append(both[1])
-        value = nt_dot(jnp.concatenate(mixed, axis=1), jnp.concatenate(columns, axis=1))
-        total = total + gates[branch] * value
+        total = total + gates[branch] * (keep[branch] + came[other, branch])
     out[...] = total.astype(BF16)
 
 
@@ -212,7 +228,7 @@
     w = lax.all_gather(wy.reshape(YN * 40, LANES), "z", axis=0, tiled=True).reshape(ZN, YN, 40, LANES)
     message, *gates = call(
         mix_kernel,
-        (shaped((TPN, YN, TOK, LANES)),) + (shaped((HALF, LANES), F32),) * 4,
+        (shaped((XN, YN, TOK + HALF, LANES)),) + (shaped((HALF, LANES), F32),) * 4,
         (gathered_tok, w, taps, sink.reshape(1, 2)),
         [VM] * 4,
         [
@@ -220,17 +236,20 @@
             pltpu.VMEM((ROWS, 2 * LANES), F32),
             pltpu.VMEM((YN, HALF, LANES), F32),
             pltpu.VMEM((TPN, LANES, LANES), BF16),
-            pltpu.VMEM((TPN, YN, TOK, LANES), BF16),
+            pltpu.VMEM((XN, YN, TOK + HALF, LANES), BF16),
             pltpu.SemaphoreType.DMA((YN,)),
         ],
         20,
         first=pl.BlockSpec(memory_space=pl.ANY),
     )
-    message = lax.all_to_all(message.reshape(PLANE, TOK, LANES), plane, 0, 0, tiled=True)
+    message = lax.all_to_all(message.reshape(XN * YN, TOK + HALF, LANES), ("x", "y"), 0, 0, tiled=True)
     for k in range(1, YN):
         gates[k] = lax.ppermute(gates[k], "y", [(y, (y + k) % YN) for y in range(YN)])
     gates = call(gate_kernel, shaped((2, TOK, LANES), F32), gates, scratch=[pltpu.VMEM((YN, HALF, LANES), F32)])
-    return call(final_kernel, shaped((TOK, LANES)), (message, gates))
+    sums = shaped((2, TOK, LANES), F32)
+    keep, give = call(partial_kernel, (sums, sums), (message,))
+    came = lax.all_gather(give, "c")
+    return call(final_kernel, shaped((TOK, LANES)), (keep, came, gates))
 
 
 def solution(mesh):

time: 88.9 us -> 88.4 us (level)
  blocking collectives: 34.3 us -> 42.8 us
  starting transfers between devices: 38.9 us -> 32.2 us
  waiting for transfers between devices: 7.12 us -> 4.84 us
    all_gather x0 -> x1, blocking collectives: none -> 8.49 us  [on_device(): came = lax.all_gather(give, 'c')]
    all_to_all x1, starting transfers between devices: 12.7 us -> 6.02 us  [on_device(): lax.all_to_all(message.reshape(XN * YN, TOK + HALF, LANES), ('x', 'y'), 0...]
    ppermute x3, waiting for transfers between devices: 4.72 us -> 3.3 us  [on_device(): lax.ppermute(gates[k], 'y', [(y, (y + k) % YN) for y in range(YN)])]
    pallas_call x5 -> x6, Pallas kernels: 7.37 us -> 7.26 us  [call(): pl.pallas_call(kernel, out_shape=outs, in_specs=specs or [VM] * len(args)...]
  transfers between devices with their start and end apart: 7 -> 7, of which waited for: 5 -> 2; matrix products, arithmetic and copies ran while one was open for 0% -> 0% of each run, Pallas kernels for 4% -> 4%
where the time goes in v10:
time: 88.4 us; the launch traced here: 87.8 us
  blocking collectives  42.8 us (48%)
  starting transfers between devices  32.2 us (36%)
  Pallas kernels  7.26 us (8%)
  waiting for transfers between devices  4.84 us (5%)
    all_gather x1, blocking collectives, on_device(): lax.all_gather(wy.reshape(YN * 40, LANES), 'z', axis=0, tiled=True)  34.3 us
    ppermute x3, starting transfers between devices, on_device(): lax.ppermute(gates[k], 'y', [(y, (y + k) % YN) for y in range(YN)])  10.7 us
    all_gather x1, blocking collectives, on_device(): came = lax.all_gather(give, 'c')  8.49 us
    all_to_all x1, starting transfers between devices, on_device(): gathered_tok = lax.all_to_all(spread, plane, 0, 0, tiled=True)  7.51 us
    all_to_all x1, starting transfers between devices, on_device(): wy = lax.all_to_all(wy, 'y', 0, 0, tiled=True)  7.36 us
    pallas_call x6, Pallas kernels, call(): pl.pallas_call(kernel, out_shape=outs, in_specs=specs or [VM] * len(args)...  7.26 us
    all_to_all x1, starting transfers between devices, on_device(): lax.all_to_all(message.reshape(XN * YN, TOK + HALF, LANES), ('x', 'y'), 0...  6.02 us
    ppermute x3, waiting for transfers between devices, on_device(): lax.ppermute(gates[k], 'y', [(y, (y + k) % YN) for y in range(YN)])  3.3 us
  transfers between devices with their start and end apart: 7, of which 2 were waited for; matrix products, arithmetic and copies ran while one was open for 0% of the time, Pallas kernels for 4%

profile of v10, /device:TPU:1, one launch (start us, length us, event | category | flops | bytes accessed | tf_op | source)
XLA Modules:
  0.0 87.8 jit_solution(7118115147264179650)
XLA Ops:
  0.0 0.7 collective-permute-start
  0.7 1.5 %shard_map.137 = bf16[4,40,128]{2,1,0:T(8,128)(2,1)} custom-call(bf16[16,128]{1,0:T(8,128)(2,1)} %q.1, bf16[16,64]{1,0:T(8,128)(2,1)} %k.1, bf16[16,64]{1,0:T(8,128)(2,1)} %v.1, bf16[16,128]{1,0:T(8,128)(2,1)} %ci.1, bf16[16,128]{1,0:T(8,128)(2,1)} %pre.1, bf16[16,128]{1,0:T(8,128)(2,1)} %post.1, bf16[16,128]{1,0:T(8,128)(2,1)} %ag.1, bf16[16,128]{1,0:T(8,128)(2,1)} %cg.1, ...), custom_call_target="tpu_custom_call" | custom-call | tf_op jit(solution)/shard_map/pallas_call | solution.py:210
  2.2 7.4 %all-to-all-start.1 = ((bf16[4,40,128]{2,1,0:T(8,128)(2,1)}), bf16[4,40,128]{2,1,0:T(8,128)(2,1)S(1)}, u32[]{:S(2)}, u32[]{:S(2)}) async-start(bf16[4,40,128]{2,1,0:T(8,128)(2,1)} %shard_map.137), calls=%async_computation.1 | async-start | bytes 81920 | tf_op jit(solution)/shard_map/all_to_all | solution.py:225
  9.5 0.0 collective-permute-done.edge
  9.5 0.0 copy-start.2
  9.5 0.6 copy-done.2
  10.2 2.2 %shard_map.136 = bf16[32,200,128]{2,1,0:T(8,128)(2,1)} custom-call(bf16[128,128]{1,0:T(8,128)(2,1)} %tok.1, f32[1,128]{1,0:T(1,128)} %bitcast.14, bf16[128,128]{1,0:T(8,128)(2,1)} %copy-done.2), custom_call_target="tpu_custom_call" | custom-call | tf_op jit(solution)/shard_map/pallas_call | solution.py:210
  12.3 0.0 copy-start
  12.3 0.0 copy-start.1
  12.3 1.5 %all-to-all-done.1 = bf16[4,40,128]{2,1,0:T(8,128)(2,1)S(1)} async-done(((bf16[4,40,128]{2,1,0:T(8,128)(2,1)}), bf16[4,40,128]{2,1,0:T(8,128)(2,1)S(1)}, u32[]{:S(2)}, u32[]{:S(2)}) %all-to-all-start.1) | async-done | bytes 40992 | tf_op jit(solution)/shard_map/all_to_all | solution.py:225
  13.9 7.5 %all-to-all-start = ((bf16[32,200,128]{2,1,0:T(8,128)(2,1)}), bf16[32,200,128]{2,1,0:T(8,128)(2,1)S(1)}, u32[]{:S(2)}, u32[]{:S(2)}) async-start(bf16[32,200,128]{2,1,0:T(8,128)(2,1)} %shard_map.136), calls=%async_computation | async-start | bytes 3276800 | tf_op jit(solution)/shard_map/all_to_all | solution.py:227
  21.4 34.3 %all_gather.9 = bf16[2560,128]{1,0:T(8,128)(2,1)S(1)} all-gather(bf16[160,128]{1,0:T(8,128)(2,1)S(1)} %bitcast.11), channel_id=1, replica_groups=mesh['z'=16,'y'=4,'x'=4,'c'=2] {'z'}, dimensions={0}, use_global_device_ids=true | all-gather | bytes 696320 | tf_op jit(solution)/shard_map/all_gather | solution.py:228
  55.7 0.0 all-to-all-done.t
  55.7 0.0 copy-done
  55.7 0.0 copy-done.1
  55.7 2.4 %shard_map.138 = (bf16[4,4,192,128]{3,2,1,0:T(8,128)(2,1)}, f32[64,128]{1,0:T(8,128)S(1)}, f32[64,128]{1,0:T(8,128)S(1)}, f32[64,128]{1,0:T(8,128)S(1)}, f32[64,128]{1,0:T(8,128)S(1)}) custom-call(bf16[32,200,128]{2,1,0:T(8,128)(2,1)S(1)} %all-to-all-done.t, bf16[16,4,40,128]{3,2,1,0:T(8,128)(2,1)S(1)} %bitcast.8, f32[3,128]{1,0:T(4,128)S(1)} %copy-done, ...), custom_call_target="tpu_custom_call" | custom-call | tf_op jit(solution)/shard_map/pallas_call | solution.py:210
  58.1 6.0 %all-to-all-start.2 = ((bf16[16,192,128]{2,1,0:T(8,128)(2,1)}), bf16[16,192,128]{2,1,0:T(8,128)(2,1)S(1)}, u32[]{:S(2)}, u32[]{:S(2)}) async-start(bf16[16,192,128]{2,1,0:T(8,128)(2,1)} %bitcast.6), calls=%async_computation.2 | async-start | bytes 1572864 | tf_op jit(solution)/shard_map/all_to_all | solution.py:245
  64.1 3.3 %collective-permute-start.1 = (f32[64,128]{1,0:T(8,128)S(1)}, f32[64,128]{1,0:T(8,128)S(1)}, u32[]{:S(2)}, u32[]{:S(2)}) collective-permute-start(f32[64,128]{1,0:T(8,128)S(1)} %get-tuple-element.16), channel_id=1, source_target_pairs={{0,8},{8,16},{16,24},{24,0},{1,9},{9,17},{17,25},{25,1},{2,10},{10... | collective-permute-start | bytes 98312 | tf_op jit(solution)/shard_map/ppermute | solution.py:247
  67.4 4.3 %collective-permute-start.2 = (f32[64,128]{1,0:T(8,128)S(1)}, f32[64,128]{1,0:T(8,128)S(1)}, u32[]{:S(2)}, u32[]{:S(2)}) collective-permute-start(f32[64,128]{1,0:T(8,128)S(1)} %get-tuple-element.17), channel_id=1, source_target_pairs={{0,16},{8,24},{16,0},{24,8},{1,17},{9,25},{17,1},{25,9},{2,18},{10... | collective-permute-start | bytes 98312 | tf_op jit(solution)/shard_map/ppermute | solution.py:247
  71.7 3.1 %collective-permute-start.3 = (f32[64,128]{1,0:T(8,128)S(1)}, f32[64,128]{1,0:T(8,128)S(1)}, u32[]{:S(2)}, u32[]{:S(2)}) collective-permute-start(f32[64,128]{1,0:T(8,128)S(1)} %get-tuple-element.18), channel_id=1, source_target_pairs={{0,24},{8,0},{16,8},{24,16},{1,25},{9,1},{17,9},{25,17},{2,26},{10... | collective-permute-start | bytes 98312 | tf_op jit(solution)/shard_map/ppermute | solution.py:247
  74.8 0.0 collective-permute-done.1.g_1
  74.8 0.0 collective-permute-done.2.g_2
  74.8 3.3 %collective-permute-done.3.g_3 = f32[64,128]{1,0:T(8,128)S(1)} collective-permute-done((f32[64,128]{1,0:T(8,128)S(1)}, f32[64,128]{1,0:T(8,128)S(1)}, u32[]{:S(2)}, u32[]{:S(2)}) %collective-permute-start.3) | collective-permute-done | bytes 32800 | tf_op jit(solution)/shard_map/ppermute | solution.py:247
  78.1 0.1 shard_map.140.gates
  78.2 0.0 all-to-all-done.2.m
  78.2 0.4 shard_map.139
  78.7 8.5 %all-gather = f32[4,128,128]{2,1,0:T(8,128)S(1)} all-gather(f32[2,128,128]{2,1,0:T(8,128)S(1)} %get-tuple-element.14), channel_id=2, replica_groups=mesh['z'=16,'y'=4,'x'=4,'c'=2] {'c'}, dimensions={0}, use_global_device_ids=true | all-gather | bytes 393216 | tf_op jit(solution)/shard_map/all_gather | solution.py:251
  87.2 0.6 shard_map.141
Async XLA Ops:
  0.0 9.5 %collective-permute-start = (bf16[128,128]{1,0:T(8,128)(2,1)}, bf16[128,128]{1,0:T(8,128)(2,1)S(1)}, u32[]{:S(2)}, u32[]{:S(2)}) collective-permute-start(bf16[128,128]{1,0:T(8,128)(2,1)} %tok.1), channel_id=1, source_target_pairs={{24,32},{56,64},{88,96},{120,128},{152,160},{184,192},{216,224},{2... | collective-permute-start | bytes 98312 | tf_op jit(solution)/shard_map/ppermute | solution.py:223
  2.2 11.7 %all-to-all-start.1 = ((bf16[4,40,128]{2,1,0:T(8,128)(2,1)}), bf16[4,40,128]{2,1,0:T(8,128)(2,1)S(1)}, u32[]{:S(2)}, u32[]{:S(2)}) async-start(bf16[4,40,128]{2,1,0:T(8,128)(2,1)} %shard_map.137), calls=%async_computation.1 | async-start | bytes 81920 | tf_op jit(solution)/shard_map/all_to_all | solution.py:225
  9.5 0.6 copy-start.2
  12.3 43.4 %copy-start = (f32[3,128]{1,0:T(4,128)S(1)}, f32[3,128]{1,0:T(4,128)}, u32[]{:S(2)}) copy-start(f32[3,128]{1,0:T(4,128)} %taps.1) | copy-start | bytes 4612
  12.3 43.4 %copy-start.1 = (f32[2]{0:T(128)S(1)}, f32[2]{0:T(128)}, u32[]{:S(2)}) copy-start(f32[2]{0:T(128)} %param.24) | copy-start | bytes 28
  13.9 41.8 %all-to-all-start = ((bf16[32,200,128]{2,1,0:T(8,128)(2,1)}), bf16[32,200,128]{2,1,0:T(8,128)(2,1)S(1)}, u32[]{:S(2)}, u32[]{:S(2)}) async-start(bf16[32,200,128]{2,1,0:T(8,128)(2,1)} %shard_map.136), calls=%async_computation | async-start | bytes 3276800 | tf_op jit(solution)/shard_map/all_to_all | solution.py:227
  58.1 20.1 %all-to-all-start.2 = ((bf16[16,192,128]{2,1,0:T(8,128)(2,1)}), bf16[16,192,128]{2,1,0:T(8,128)(2,1)S(1)}, u32[]{:S(2)}, u32[]{:S(2)}) async-start(bf16[16,192,128]{2,1,0:T(8,128)(2,1)} %bitcast.6), calls=%async_computation.2 | async-start | bytes 1572864 | tf_op jit(solution)/shard_map/all_to_all | solution.py:245
  64.1 10.7 %collective-permute-start.1 = (f32[64,128]{1,0:T(8,128)S(1)}, f32[64,128]{1,0:T(8,128)S(1)}, u32[]{:S(2)}, u32[]{:S(2)}) collective-permute-start(f32[64,128]{1,0:T(8,128)S(1)} %get-tuple-element.16), channel_id=1, source_target_pairs={{0,8},{8,16},{16,24},{24,0},{1,9},{9,17},{17,25},{25,1},{2,10},{10... | collective-permute-start | bytes 98312 | tf_op jit(solution)/shard_map/ppermute | solution.py:247
  67.4 7.4 %collective-permute-start.2 = (f32[64,128]{1,0:T(8,128)S(1)}, f32[64,128]{1,0:T(8,128)S(1)}, u32[]{:S(2)}, u32[]{:S(2)}) collective-permute-start(f32[64,128]{1,0:T(8,128)S(1)} %get-tuple-element.17), channel_id=1, source_target_pairs={{0,16},{8,24},{16,0},{24,8},{1,17},{9,25},{17,1},{25,9},{2,18},{10... | collective-permute-start | bytes 98312 | tf_op jit(solution)/shard_map/ppermute | solution.py:247
  71.7 6.4 %collective-permute-start.3 = (f32[64,128]{1,0:T(8,128)S(1)}, f32[64,128]{1,0:T(8,128)S(1)}, u32[]{:S(2)}, u32[]{:S(2)}) collective-permute-start(f32[64,128]{1,0:T(8,128)S(1)} %get-tuple-element.18), channel_id=1, source_target_pairs={{0,24},{8,0},{16,8},{24,16},{1,25},{9,1},{17,9},{25,17},{2,26},{10... | collective-permute-start | bytes 98312 | tf_op jit(solution)/shard_map/ppermute | solution.py:247

commit v11 on v10

--- a/solution.py
+++ b/solution.py
@@ -104,14 +104,14 @@
     for x in range(XN):
         packed = jnp.where(left[:HALF], turned(w_scr[2 * x + 1])[:HALF], w_scr[2 * x + 1][HALF:])
         for b in range(YN):
-            m_scr[x, b, TOK:, :] = packed
+            m_scr[b, x, TOK:, :] = packed
 
     def outgoing(b):
-        return pltpu.make_async_copy(m_scr.at[:, b], out.at[:, b], sems.at[b])
+        return pltpu.make_async_copy(m_scr.at[b], out.at[b], sems.at[b])
 
     def send(b, mixed):
         for x in range(XN):
-            m_scr[x, b, :TOK, :] = jnp.where(left, mixed, w_scr[2 * x])
+            m_scr[b, x, :TOK, :] = jnp.where(left, mixed, w_scr[2 * x])
         outgoing(b).start()
 
     @pl.when(y < 2)
@@ -177,7 +177,7 @@
     for branch in range(2):
         mixed, even, odd = [], [], []
         for x in range(XN):
-            a, b = m[YN * x + 2 * branch], m[YN * x + 2 * branch + 1]
+            a, b = m[2 * branch * XN + x], m[(2 * branch + 1) * XN + x]
             both = joined(a[:TOK], b[:TOK], left)
             mixed.append(both[0])
             even.append(both[1])
@@ -228,7 +228,7 @@
     w = lax.all_gather(wy.reshape(YN * 40, LANES), "z", axis=0, tiled=True).reshape(ZN, YN, 40, LANES)
     message, *gates = call(
         mix_kernel,
-        (shaped((XN, YN, TOK + HALF, LANES)),) + (shaped((HALF, LANES), F32),) * 4,
+        (shaped((YN, XN, TOK + HALF, LANES)),) + (shaped((HALF, LANES), F32),) * 4,
         (gathered_tok, w, taps, sink.reshape(1, 2)),
         [VM] * 4,
         [
@@ -236,13 +236,13 @@
             pltpu.VMEM((ROWS, 2 * LANES), F32),
             pltpu.VMEM((YN, HALF, LANES), F32),
             pltpu.VMEM((TPN, LANES, LANES), BF16),
-            pltpu.VMEM((XN, YN, TOK + HALF, LANES), BF16),
+            pltpu.VMEM((YN, XN, TOK + HALF, LANES), BF16),
             pltpu.SemaphoreType.DMA((YN,)),
         ],
         20,
         first=pl.BlockSpec(memory_space=pl.ANY),
     )
-    message = lax.all_to_all(message.reshape(XN * YN, TOK + HALF, LANES), ("x", "y"), 0, 0, tiled=True)
+    message = lax.all_to_all(message.reshape(YN * XN, TOK + HALF, LANES), ("y", "x"), 0, 0, tiled=True)
     for k in range(1, YN):
         gates[k] = lax.ppermute(gates[k], "y", [(y, (y + k) % YN) for y in range(YN)])
     gates = call(gate_kernel, shaped((2, TOK, LANES), F32), gates, scratch=[pltpu.VMEM((YN, HALF, LANES), F32)])

time: 88.4 us -> 88.4 us (level)
  blocking collectives: 42.8 us -> 41 us
  waiting for transfers between devices: 4.84 us -> 6.58 us
    all_gather x1, blocking collectives: 8.49 us -> 6.71 us  [on_device(): came = lax.all_gather(give, 'c')]
    ppermute x3, waiting for transfers between devices: 3.3 us -> 5.03 us  [on_device(): lax.ppermute(gates[k], 'y', [(y, (y + k) % YN) for y in range(YN)])]
where the time goes in v11:
time: 88.4 us; the launch traced here: 87.8 us
  blocking collectives  41 us (46%)
  starting transfers between devices  32.2 us (36%)
  Pallas kernels  7.31 us (8%)
  waiting for transfers between devices  6.58 us (7%)
    all_gather x1, blocking collectives, on_device(): lax.all_gather(wy.reshape(YN * 40, LANES), 'z', axis=0, tiled=True)  34.3 us
    ppermute x3, starting transfers between devices, on_device(): lax.ppermute(gates[k], 'y', [(y, (y + k) % YN) for y in range(YN)])  10.7 us
    all_to_all x1, starting transfers between devices, on_device(): gathered_tok = lax.all_to_all(spread, plane, 0, 0, tiled=True)  7.51 us
    all_to_all x1, starting transfers between devices, on_device(): wy = lax.all_to_all(wy, 'y', 0, 0, tiled=True)  7.36 us
    pallas_call x6, Pallas kernels, call(): pl.pallas_call(kernel, out_shape=outs, in_specs=specs or [VM] * len(args)...  7.31 us
    all_gather x1, blocking collectives, on_device(): came = lax.all_gather(give, 'c')  6.71 us
    all_to_all x1, starting transfers between devices, on_device(): lax.all_to_all(message.reshape(YN * XN, TOK + HALF, LANES), ('y', 'x'), 0...  6.02 us
    ppermute x3, waiting for transfers between devices, on_device(): lax.ppermute(gates[k], 'y', [(y, (y + k) % YN) for y in range(YN)])  5.03 us
  transfers between devices with their start and end apart: 7, of which 2 were waited for; matrix products, arithmetic and copies ran while one was open for 0% of the time, Pallas kernels for 4%

profile of v11, /device:TPU:1, one launch (start us, length us, event | category | flops | bytes accessed | tf_op | source)
XLA Modules:
  0.0 87.8 jit_solution(416782235135552415)
XLA Ops:
  0.0 0.7 collective-permute-start
  0.7 1.5 %shard_map.137 = bf16[4,40,128]{2,1,0:T(8,128)(2,1)} custom-call(bf16[16,128]{1,0:T(8,128)(2,1)} %q.1, bf16[16,64]{1,0:T(8,128)(2,1)} %k.1, bf16[16,64]{1,0:T(8,128)(2,1)} %v.1, bf16[16,128]{1,0:T(8,128)(2,1)} %ci.1, bf16[16,128]{1,0:T(8,128)(2,1)} %pre.1, bf16[16,128]{1,0:T(8,128)(2,1)} %post.1, bf16[16,128]{1,0:T(8,128)(2,1)} %ag.1, bf16[16,128]{1,0:T(8,128)(2,1)} %cg.1, ...), custom_call_target="tpu_custom_call" | custom-call | tf_op jit(solution)/shard_map/pallas_call | solution.py:210
  2.2 7.4 %all-to-all-start.1 = ((bf16[4,40,128]{2,1,0:T(8,128)(2,1)}), bf16[4,40,128]{2,1,0:T(8,128)(2,1)S(1)}, u32[]{:S(2)}, u32[]{:S(2)}) async-start(bf16[4,40,128]{2,1,0:T(8,128)(2,1)} %shard_map.137), calls=%async_computation.1 | async-start | bytes 81920 | tf_op jit(solution)/shard_map/all_to_all | solution.py:225
  9.5 0.0 collective-permute-done.edge
  9.5 0.0 copy-start.2
  9.5 0.6 copy-done.2
  10.2 2.2 %shard_map.136 = bf16[32,200,128]{2,1,0:T(8,128)(2,1)} custom-call(bf16[128,128]{1,0:T(8,128)(2,1)} %tok.1, f32[1,128]{1,0:T(1,128)} %bitcast.14, bf16[128,128]{1,0:T(8,128)(2,1)} %copy-done.2), custom_call_target="tpu_custom_call" | custom-call | tf_op jit(solution)/shard_map/pallas_call | solution.py:210
  12.3 0.0 copy-start
  12.3 0.0 copy-start.1
  12.3 1.5 %all-to-all-done.1 = bf16[4,40,128]{2,1,0:T(8,128)(2,1)S(1)} async-done(((bf16[4,40,128]{2,1,0:T(8,128)(2,1)}), bf16[4,40,128]{2,1,0:T(8,128)(2,1)S(1)}, u32[]{:S(2)}, u32[]{:S(2)}) %all-to-all-start.1) | async-done | bytes 40992 | tf_op jit(solution)/shard_map/all_to_all | solution.py:225
  13.9 7.5 %all-to-all-start = ((bf16[32,200,128]{2,1,0:T(8,128)(2,1)}), bf16[32,200,128]{2,1,0:T(8,128)(2,1)S(1)}, u32[]{:S(2)}, u32[]{:S(2)}) async-start(bf16[32,200,128]{2,1,0:T(8,128)(2,1)} %shard_map.136), calls=%async_computation | async-start | bytes 3276800 | tf_op jit(solution)/shard_map/all_to_all | solution.py:227
  21.4 34.3 %all_gather.9 = bf16[2560,128]{1,0:T(8,128)(2,1)S(1)} all-gather(bf16[160,128]{1,0:T(8,128)(2,1)S(1)} %bitcast.11), channel_id=1, replica_groups=mesh['z'=16,'y'=4,'x'=4,'c'=2] {'z'}, dimensions={0}, use_global_device_ids=true | all-gather | bytes 696320 | tf_op jit(solution)/shard_map/all_gather | solution.py:228
  55.7 0.0 all-to-all-done.t
  55.7 0.0 copy-done
  55.7 0.0 copy-done.1
  55.7 2.4 %shard_map.138 = (bf16[4,4,192,128]{3,2,1,0:T(8,128)(2,1)}, f32[64,128]{1,0:T(8,128)S(1)}, f32[64,128]{1,0:T(8,128)S(1)}, f32[64,128]{1,0:T(8,128)S(1)}, f32[64,128]{1,0:T(8,128)S(1)}) custom-call(bf16[32,200,128]{2,1,0:T(8,128)(2,1)S(1)} %all-to-all-done.t, bf16[16,4,40,128]{3,2,1,0:T(8,128)(2,1)S(1)} %bitcast.8, f32[3,128]{1,0:T(4,128)S(1)} %copy-done, ...), custom_call_target="tpu_custom_call" | custom-call | tf_op jit(solution)/shard_map/pallas_call | solution.py:210
  58.1 6.0 %all-to-all-start.2 = ((bf16[16,192,128]{2,1,0:T(8,128)(2,1)}), bf16[16,192,128]{2,1,0:T(8,128)(2,1)S(1)}, u32[]{:S(2)}, u32[]{:S(2)}) async-start(bf16[16,192,128]{2,1,0:T(8,128)(2,1)} %bitcast.6), calls=%async_computation.2 | async-start | bytes 1572864 | tf_op jit(solution)/shard_map/all_to_all | solution.py:245
  64.1 3.3 %collective-permute-start.1 = (f32[64,128]{1,0:T(8,128)S(1)}, f32[64,128]{1,0:T(8,128)S(1)}, u32[]{:S(2)}, u32[]{:S(2)}) collective-permute-start(f32[64,128]{1,0:T(8,128)S(1)} %get-tuple-element.16), channel_id=1, source_target_pairs={{0,8},{8,16},{16,24},{24,0},{1,9},{9,17},{17,25},{25,1},{2,10},{10... | collective-permute-start | bytes 98312 | tf_op jit(solution)/shard_map/ppermute | solution.py:247
  67.4 4.3 %collective-permute-start.2 = (f32[64,128]{1,0:T(8,128)S(1)}, f32[64,128]{1,0:T(8,128)S(1)}, u32[]{:S(2)}, u32[]{:S(2)}) collective-permute-start(f32[64,128]{1,0:T(8,128)S(1)} %get-tuple-element.17), channel_id=1, source_target_pairs={{0,16},{8,24},{16,0},{24,8},{1,17},{9,25},{17,1},{25,9},{2,18},{10... | collective-permute-start | bytes 98312 | tf_op jit(solution)/shard_map/ppermute | solution.py:247
  71.7 3.1 %collective-permute-start.3 = (f32[64,128]{1,0:T(8,128)S(1)}, f32[64,128]{1,0:T(8,128)S(1)}, u32[]{:S(2)}, u32[]{:S(2)}) collective-permute-start(f32[64,128]{1,0:T(8,128)S(1)} %get-tuple-element.18), channel_id=1, source_target_pairs={{0,24},{8,0},{16,8},{24,16},{1,25},{9,1},{17,9},{25,17},{2,26},{10... | collective-permute-start | bytes 98312 | tf_op jit(solution)/shard_map/ppermute | solution.py:247
  74.8 0.0 collective-permute-done.1.g_1
  74.8 0.0 collective-permute-done.2.g_2
  74.8 5.0 %collective-permute-done.3.g_3 = f32[64,128]{1,0:T(8,128)S(1)} collective-permute-done((f32[64,128]{1,0:T(8,128)S(1)}, f32[64,128]{1,0:T(8,128)S(1)}, u32[]{:S(2)}, u32[]{:S(2)}) %collective-permute-start.3) | collective-permute-done | bytes 32800 | tf_op jit(solution)/shard_map/ppermute | solution.py:247
  79.9 0.1 shard_map.140.gates
  80.0 0.0 all-to-all-done.2.m
  80.0 0.5 shard_map.139
  80.5 6.7 %all-gather = f32[4,128,128]{2,1,0:T(8,128)S(1)} all-gather(f32[2,128,128]{2,1,0:T(8,128)S(1)} %get-tuple-element.14), channel_id=2, replica_groups=mesh['z'=16,'y'=4,'x'=4,'c'=2] {'c'}, dimensions={0}, use_global_device_ids=true | all-gather | bytes 393216 | tf_op jit(solution)/shard_map/all_gather | solution.py:251
  87.2 0.6 shard_map.141
Async XLA Ops:
  0.0 9.5 %collective-permute-start = (bf16[128,128]{1,0:T(8,128)(2,1)}, bf16[128,128]{1,0:T(8,128)(2,1)S(1)}, u32[]{:S(2)}, u32[]{:S(2)}) collective-permute-start(bf16[128,128]{1,0:T(8,128)(2,1)} %tok.1), channel_id=1, source_target_pairs={{24,32},{56,64},{88,96},{120,128},{152,160},{184,192},{216,224},{2... | collective-permute-start | bytes 98312 | tf_op jit(solution)/shard_map/ppermute | solution.py:223
  2.2 11.7 %all-to-all-start.1 = ((bf16[4,40,128]{2,1,0:T(8,128)(2,1)}), bf16[4,40,128]{2,1,0:T(8,128)(2,1)S(1)}, u32[]{:S(2)}, u32[]{:S(2)}) async-start(bf16[4,40,128]{2,1,0:T(8,128)(2,1)} %shard_map.137), calls=%async_computation.1 | async-start | bytes 81920 | tf_op jit(solution)/shard_map/all_to_all | solution.py:225
  9.5 0.6 copy-start.2
  12.3 43.4 %copy-start = (f32[3,128]{1,0:T(4,128)S(1)}, f32[3,128]{1,0:T(4,128)}, u32[]{:S(2)}) copy-start(f32[3,128]{1,0:T(4,128)} %taps.1) | copy-start | bytes 4612
  12.3 43.4 %copy-start.1 = (f32[2]{0:T(128)S(1)}, f32[2]{0:T(128)}, u32[]{:S(2)}) copy-start(f32[2]{0:T(128)} %param.24) | copy-start | bytes 28
  13.9 41.8 %all-to-all-start = ((bf16[32,200,128]{2,1,0:T(8,128)(2,1)}), bf16[32,200,128]{2,1,0:T(8,128)(2,1)S(1)}, u32[]{:S(2)}, u32[]{:S(2)}) async-start(bf16[32,200,128]{2,1,0:T(8,128)(2,1)} %shard_map.136), calls=%async_computation | async-start | bytes 3276800 | tf_op jit(solution)/shard_map/all_to_all | solution.py:227
  58.1 21.9 %all-to-all-start.2 = ((bf16[16,192,128]{2,1,0:T(8,128)(2,1)}), bf16[16,192,128]{2,1,0:T(8,128)(2,1)S(1)}, u32[]{:S(2)}, u32[]{:S(2)}) async-start(bf16[16,192,128]{2,1,0:T(8,128)(2,1)} %bitcast.6), calls=%async_computation.2 | async-start | bytes 1572864 | tf_op jit(solution)/shard_map/all_to_all | solution.py:245
  64.1 10.7 %collective-permute-start.1 = (f32[64,128]{1,0:T(8,128)S(1)}, f32[64,128]{1,0:T(8,128)S(1)}, u32[]{:S(2)}, u32[]{:S(2)}) collective-permute-start(f32[64,128]{1,0:T(8,128)S(1)} %get-tuple-element.16), channel_id=1, source_target_pairs={{0,8},{8,16},{16,24},{24,0},{1,9},{9,17},{17,25},{25,1},{2,10},{10... | collective-permute-start | bytes 98312 | tf_op jit(solution)/shard_map/ppermute | solution.py:247
  67.4 7.4 %collective-permute-start.2 = (f32[64,128]{1,0:T(8,128)S(1)}, f32[64,128]{1,0:T(8,128)S(1)}, u32[]{:S(2)}, u32[]{:S(2)}) collective-permute-start(f32[64,128]{1,0:T(8,128)S(1)} %get-tuple-element.17), channel_id=1, source_target_pairs={{0,16},{8,24},{16,0},{24,8},{1,17},{9,25},{17,1},{25,9},{2,18},{10... | collective-permute-start | bytes 98312 | tf_op jit(solution)/shard_map/ppermute | solution.py:247
  71.7 8.1 %collective-permute-start.3 = (f32[64,128]{1,0:T(8,128)S(1)}, f32[64,128]{1,0:T(8,128)S(1)}, u32[]{:S(2)}, u32[]{:S(2)}) collective-permute-start(f32[64,128]{1,0:T(8,128)S(1)} %get-tuple-element.18), channel_id=1, source_target_pairs={{0,24},{8,0},{16,8},{24,16},{1,25},{9,1},{17,9},{25,17},{2,26},{10... | collective-permute-start | bytes 98312 | tf_op jit(solution)/shard_map/ppermute | solution.py:247
